TPU v7x, 512 devices: a whole 4x4x16 slice. The times are simulated.
512 devices in a mesh: sp: 64 (over z, y), tp: 8 (over x, core).
Axes of the slice: x: 4, y: 4, z: 16, core: 2. Of those that a mesh axis runs over, the one named last changes fastest.
Arguments:
- latent: bfloat16 [16384, 2048], P(('sp', 'tp')), may hold values from -6 to 6
- condition: bfloat16 [2048], P('sp'), may hold values from -6 to 6
- context_condition: bfloat16 [2048], P('sp'), may hold values from -6 to 6
- context: bfloat16 [512, 2048], P('sp'), may hold values from -6 to 6
- w_shift: bfloat16 [2048, 2048], P('sp', 'tp'), may hold values from -0.125 to 0.125
- w_scale: bfloat16 [2048, 2048], P('sp', 'tp'), may hold values from -0.125 to 0.125
- w_gate: bfloat16 [2048, 2048], P('sp', 'tp'), may hold values from -0.125 to 0.125
- pre_gain: float32 [2048], replicated, may hold values from 0.1 to 1.9
- post_gain: float32 [2048], replicated, may hold values from 0.1 to 1.9
- query_gain: float32 [128], replicated, may hold values from 0.1 to 5
- key_gain: float32 [128], replicated, may hold values from 0.1 to 5
- w_query: bfloat16 [2048, 2048], P(None, 'tp'), may hold values from -0.125 to 0.125
- w_key: bfloat16 [2048, 1024], P(None, 'tp'), may hold values from -0.125 to 0.125
- w_value: bfloat16 [2048, 1024], P(None, 'tp'), may hold values from -0.125 to 0.125
- w_out: bfloat16 [2048, 2048], P('tp'), may hold values from -0.125 to 0.125
Outputs:
- updated: bfloat16 [16384, 2048], P(('sp', 'tp'))
All inputs are finite; a program needn't handle non-finite values.
Results may differ from a plain program's by a relative error of at most 0.0085.
The roundings to bfloat16 on the way count: a program that leaves them out, or rounds other values in their place, can miss the bound.
Values may be sent and summed in bfloat16 or wider, within the bound.
No kernel may reach another device: no remote copies, remote signals or barrier semaphores. Data moves between devices by JAX's collectives and lax.ppermute only.
A program may use at most 64 MiB of HBM per device.

v0:
```python
import functools
import math

import jax
import jax.numpy as jnp
from jax import lax
from jax.sharding import Mesh
from jax.sharding import PartitionSpec as P

GRID_W = 64
SP = ("sp_0", "sp_1")
SP_TP = ("sp_0", "sp_1", "tp")


def by_axis(value, axes):
    return functools.reduce(lax.psum, axes, value)


def laid_out(blocks, dim):
    blocks = jnp.moveaxis(blocks, 0, dim)
    shape = blocks.shape
    return blocks.reshape(*shape[:dim], shape[dim] * shape[dim + 1], *shape[dim + 2 :])


def from_everyone(value, axis):
    devices = lax.axis_size(axis)
    return lax.all_to_all(
        jnp.broadcast_to(value[None], (devices, *value.shape)), axis, 0, 0, tiled=True
    )


def gathered_copies(value, axis, dim):
    return laid_out(from_everyone(value, axis), dim)


def one_gather(arrays, axis, dims):
    ravelled = jnp.concatenate([a.reshape(-1) for a in arrays])
    lines, at, outs = (lax.all_gather(ravelled, axis), 0, [])
    for a, dim in zip(arrays, dims):
        blocks = lines[:, at : at + a.size].reshape(-1, *a.shape)
        outs.append(laid_out(blocks, dim))
        at += a.size
    return tuple(outs)


def gather_in_order(value, axes, turns):
    blocks = value
    for k in turns:
        blocks = lax.all_gather(blocks, axes[k])
    done = turns[::-1]
    back = [done.index(k) for k in range(len(axes))]
    blocks = blocks.transpose(*back, *range(len(axes), blocks.ndim))
    return blocks.reshape(-1, *value.shape)


def whole_of(value, axes, turns, dim):
    return laid_out(gather_in_order(value, axes, turns), dim)


def split_up(value, dim, devices):
    before, after = (value.shape[:dim], value.shape[dim + 1 :])
    return jnp.moveaxis(value.reshape(*before, devices, -1, *after), dim, 0)


def summed_on_arrival(value, axis, dim):
    blocks = split_up(value, dim, lax.axis_size(axis))
    arrived = lax.all_to_all(blocks, axis, split_axis=0, concat_axis=0, tiled=True)
    return arrived.astype(jnp.float32).sum(axis=0)


def rms(values, gain):
    values = values.astype(jnp.float32)
    return values * lax.rsqrt(jnp.mean(values * values, axis=-1, keepdims=True) + 1e-06) * gain


def rotate_grid(values, positions, grid_width):
    head_dim = values.shape[-1]
    half = head_dim // 2
    quarter = head_dim // 4
    freqs = 10000.0 ** (-jnp.arange(0, half, 2).astype(jnp.float32) / half)
    row_pos = (positions // grid_width).astype(jnp.float32)
    col_pos = (positions % grid_width).astype(jnp.float32)
    pieces = []
    for axis_pos, base in ((row_pos, 0), (col_pos, half)):
        angle = axis_pos[:, None, None] * freqs
        cosine = jnp.cos(angle)
        sine = jnp.sin(angle)
        first = values[..., base : base + quarter]
        second = values[..., base + quarter : base + half]
        pieces = pieces + [first * cosine - second * sine, second * cosine + first * sine]
    return jnp.concatenate(pieces, axis=-1)


def absorb(carry, grouped_query, key_rows, value_rows, offsets, head_dim):
    largest, total, summed = carry
    kv_dev = grouped_query.shape[1]
    key_heads = key_rows.reshape(key_rows.shape[0], kv_dev, head_dim)
    value_heads = value_rows.reshape(value_rows.shape[0], kv_dev, head_dim)
    scores = jnp.einsum(
        "tkgd,skd->kgts", grouped_query, key_heads, preferred_element_type=jnp.float32
    )
    scores = scores * head_dim ** (-0.5) + offsets
    new_largest = jnp.maximum(largest, jnp.max(scores, axis=-1))
    correction = jnp.exp(largest - new_largest)
    terms = jnp.exp(scores - new_largest[..., None])
    total = total * correction + jnp.sum(terms, axis=-1)
    summed = summed * correction[..., None] + jnp.einsum(
        "kgts,skd->kgtd",
        terms.astype(jnp.bfloat16),
        value_heads,
        preferred_element_type=jnp.float32,
    )
    return (new_largest, total, summed)


def absorb_blocks(carry, grouped_query, key_rows, value_rows, offsets, shard_rows, head_dim):
    length = key_rows.shape[0]
    size = length
    shards = length // shard_rows
    factor = 1
    for candidate in range(shards, 0, -1):
        if shards % candidate == 0 and candidate * shard_rows <= 2048:
            factor = candidate
            break
    size = factor * shard_rows
    blocks = length // size
    if blocks == 1:
        return absorb(carry, grouped_query, key_rows, value_rows, offsets, head_dim)

    def step_block(state, inputs):
        return (absorb(state, grouped_query, inputs[0], inputs[1], inputs[2], head_dim), None)

    width = key_rows.shape[1]
    stacked = (
        key_rows.reshape(blocks, size, width),
        value_rows.reshape(blocks, size, width),
        offsets.reshape(blocks, size),
    )
    carry, unused = lax.scan(step_block, carry, stacked)
    return carry


def body(
    latent,
    condition,
    context_condition,
    context,
    w_shift,
    w_scale,
    w_gate,
    pre_gain,
    post_gain,
    query_gain,
    key_gain,
    w_query,
    w_key,
    w_value,
    w_out,
):
    sp_count = lax.axis_size(SP)
    tp_count = lax.axis_size("tp")
    head_dim = query_gain.shape[0]
    heads_dev = w_query.shape[1] // head_dim
    kv_dev = w_key.shape[1] // head_dim
    group = heads_dev // kv_dev
    query_width = w_query.shape[1]
    key_width = w_key.shape[1]
    conds = jax.nn.silu(jnp.stack([condition, context_condition]).astype(jnp.float32)).astype(
        jnp.bfloat16
    )
    partial_mod = tuple(
        (
            jnp.dot(conds, weight, preferred_element_type=jnp.float32)
            for weight in (w_shift, w_scale, w_gate)
        )
    )
    partial_mod = jax.tree.map(lambda part: by_axis(part, SP), partial_mod)
    shift, scale, gate = jax.tree.map(lambda part: gathered_copies(part, "tp", 1), partial_mod)
    normed = (rms(latent, pre_gain) * (1.0 + scale[0]) + shift[0]).astype(jnp.bfloat16)
    normed_context = (rms(context, pre_gain) * (1.0 + scale[1]) + shift[1]).astype(jnp.bfloat16)
    tok_dev = latent.shape[0] * tp_count
    ctx_dev = context.shape[0]
    weights_all = jnp.concatenate([w_query, w_key, w_value], axis=1)
    projected = (
        lambda segment, first_row: jnp.dot(segment, weights_all, preferred_element_type=jnp.float32)
    )(gathered_copies(normed, "tp", 0), jnp.int32(0))
    positions = lax.axis_index(SP) * tok_dev + jnp.arange(tok_dev)
    query = projected[:, :query_width].reshape(tok_dev, heads_dev, head_dim)
    query = rotate_grid(rms(query, query_gain), positions, GRID_W).astype(jnp.bfloat16)
    key = projected[:, query_width : query_width + key_width].reshape(tok_dev, kv_dev, head_dim)
    key = (
        rotate_grid(rms(key, key_gain), positions, GRID_W)
        .astype(jnp.bfloat16)
        .reshape(tok_dev, key_width)
    )
    value = projected[:, query_width + key_width :].astype(jnp.bfloat16)
    grouped_query = query.reshape(tok_dev, kv_dev, group, head_dim)
    weights_kv = jnp.concatenate([w_key, w_value], axis=1)
    lift = math.log(tok_dev * sp_count / (4.0 * ctx_dev * sp_count))
    carry = (
        jnp.full((kv_dev, group, tok_dev), -1e30, jnp.float32),
        jnp.zeros((kv_dev, group, tok_dev), jnp.float32),
        jnp.zeros((kv_dev, group, tok_dev, head_dim), jnp.float32),
    )
    both = jnp.dot(normed_context, weights_kv, preferred_element_type=jnp.float32)
    context_key = rms(
        both[:, :key_width].reshape(normed_context.shape[0], kv_dev, head_dim), key_gain
    )
    context_key = context_key.astype(jnp.bfloat16).reshape(normed_context.shape[0], key_width)
    context_key, context_value = (context_key, both[:, key_width:].astype(jnp.bfloat16))
    context_key, context_value = one_gather((context_key, context_value), SP, (0, 0))
    context_offsets = jnp.full((context_key.shape[0],), lift, jnp.float32)
    carry = absorb_blocks(
        carry,
        grouped_query,
        context_key,
        context_value,
        context_offsets,
        context_key.shape[0],
        head_dim,
    )
    segments = (whole_of(key, SP, (0, 1), 0), whole_of(value, SP, (0, 1), 0))
    length = segments[0].shape[0]
    within = jnp.arange(length) % tok_dev
    offsets = jnp.where(within >= tok_dev, lift, 0.0).astype(jnp.float32)
    largest, total, summed = absorb_blocks(
        carry, grouped_query, segments[0], segments[1], offsets, tok_dev, head_dim
    )
    attended = (
        (summed / total[..., None]).transpose(2, 0, 1, 3).reshape(tok_dev, heads_dev * head_dim)
    )
    attended = attended.astype(jnp.bfloat16)
    mixed = summed_on_arrival(
        jnp.dot(attended, w_out, preferred_element_type=jnp.float32).astype(jnp.bfloat16), "tp", 0
    )
    updated = latent.astype(jnp.float32) + gate[0] * rms(mixed, post_gain)
    return updated.astype(jnp.bfloat16)


def solution(mesh):
    torus = Mesh(mesh.devices.reshape(16, 4, mesh.shape["tp"]), ("sp_0", "sp_1", "tp"))
    placed = (
        P(SP_TP, None),
        P(SP),
        P(SP),
        P(SP, None),
        P(SP, "tp"),
        P(SP, "tp"),
        P(SP, "tp"),
        P(),
        P(),
        P(),
        P(),
        P(None, "tp"),
        P(None, "tp"),
        P(None, "tp"),
        P("tp", None),
    )
    return jax.shard_map(
        body, mesh=torus, in_specs=placed, out_specs=P(SP_TP, None), check_vma=False
    )
```

profile of v0, /device:TPU:1, one launch (start us, length us, event | category | flops | bytes accessed | tf_op | source)
XLA Modules:
  0.0 423.7 jit_solution(1902211752874019034)
XLA Ops:
  9.3 30.7 %all-reduce = (f32[2,256]{1,0:T(2,128)S(1)}, f32[2,256]{1,0:T(2,128)S(1)}, f32[2,256]{1,0:T(2,128)S(1)}) all-reduce(f32[2,256]{1,0:T(2,128)S(1)} %fusion.99, f32[2,256]{1,0:T(2,128)S(1)} %fusion.101, f32[2,256]{1,0:T(2,128)S(1)} %fusion.103), channel_id=1, replica_groups=mesh['sp_0'=16,'sp_1'=4,'tp'=8] {'sp_0'}, use_global_device_ids=true, to_apply=%region_5.6 | all-reduce | flops 1536 | bytes 12288 | tf_op jit(solution)/shard_map/psum | solution.py:16
  40.0 8.8 %all-reduce.1 = (f32[2,256]{1,0:T(2,128)S(1)}, f32[2,256]{1,0:T(2,128)S(1)}, f32[2,256]{1,0:T(2,128)S(1)}) all-reduce(f32[2,256]{1,0:T(2,128)S(1)} %get-tuple-element.66, f32[2,256]{1,0:T(2,128)S(1)} %get-tuple-element.67, f32[2,256]{1,0:T(2,128)S(1)} %get-tuple-element.68), channel_id=1, replica_groups=mesh['sp_0'=16,'sp_1'=4,'tp'=8] {'sp_1'}, use_global_device_ids=true, to_apply=%region_6.7 | all-reduce | flops 1536 | bytes 12288 | tf_op jit(solution)/shard_map/psum | solution.py:16
  49.5 14.0 %all-to-all-start.1 = ((f32[8,2,256]{2,1,0:T(2,128)}), f32[8,2,256]{2,1,0:T(2,128)S(1)}, u32[]{:S(2)}, u32[]{:S(2)}) async-start(f32[8,2,256]{2,1,0:T(2,128)} %broadcast_in_dim.23), calls=%async_computation.1 | async-start | bytes 32768 | tf_op jit(solution)/shard_map/all_to_all | solution.py:27
  64.5 3.6 all-to-all-done.1
  68.8 3.9 all-to-all-start.2
  72.7 4.7 %all-to-all-done.2 = f32[8,2,256]{2,1,0:T(2,128)S(1)} async-done(((f32[8,2,256]{2,1,0:T(2,128)}), f32[8,2,256]{2,1,0:T(2,128)S(1)}, u32[]{:S(2)}, u32[]{:S(2)}) %all-to-all-start.2) | async-done | bytes 16416 | tf_op jit(solution)/shard_map/all_to_all | solution.py:27
  79.5 4.2 all-to-all-start.3
  83.7 15.0 %all-to-all-done.3 = bf16[8,32,2048]{2,1,0:T(8,128)(2,1)S(1)} async-done(((bf16[8,32,2048]{2,1,0:T(8,128)(2,1)}), bf16[8,32,2048]{2,1,0:T(8,128)(2,1)S(1)}, u32[]{:S(2)}, u32[]{:S(2)}) %all-to-all-start.3) | async-done | bytes 1048608 | tf_op jit(solution)/shard_map/all_to_all | solution.py:27
  103.2 51.8 %all-gather.9.cloned.1.call-done = bf16[16,256,128]{2,1,0:T(8,128)(2,1)} async-done(((bf16[1,256,128]{2,1,0:T(8,128)(2,1)}), bf16[16,256,128]{2,1,0:T(8,128)(2,1)}) %all-gather.9.cloned.1.call-update) | async-done | bytes 1048592 | tf_op jit(solution)/shard_map/all_gather | solution.py:49
  155.0 69.7 %all-gather.13.cloned.1.call-done = bf16[4096,128]{1,0:T(8,128)(2,1)} async-done(((bf16[256,128]{1,0:T(8,128)(2,1)}), bf16[4096,128]{1,0:T(8,128)(2,1)}) %all-gather.13.cloned.1.call-update) | async-done | bytes 1048592 | tf_op jit(solution)/shard_map/all_gather | solution.py:49
  225.3 15.3 %all-to-all-start = ((f32[8,2,256]{2,1,0:T(2,128)}), f32[8,2,256]{2,1,0:T(2,128)S(1)}, u32[]{:S(2)}, u32[]{:S(2)}) async-start(f32[8,2,256]{2,1,0:T(2,128)} %broadcast_in_dim.22), calls=%async_computation | async-start | bytes 32768 | tf_op jit(solution)/shard_map/all_to_all | solution.py:27
  243.4 69.4 %all-gather = bf16[131072]{0:T(1024)(128)(2,1)S(1)} all-gather(bf16[2048]{0:T(1024)(128)(2,1)S(1)} %pad_maximum_fusion.2), channel_id=2, replica_groups=mesh['sp_0'=16,'sp_1'=4,'tp'=8] {'sp_0','sp_1'}, dimensions={0}, use_global_device_ids=true | all-gather | bytes 266240 | tf_op jit(solution)/shard_map/all_gather | solution.py:38
  315.4 4.6 %copy.40 = bf16[16,4,256,128]{3,2,1,0:T(8,128)(2,1)} copy(bf16[16,4,256,128]{3,2,0,1:T(8,128)(2,1)} %bitcast.170) | data formatting | bytes 8388608 | tf_op jit(solution)/shard_map/transpose | solution.py:52
  320.0 28.2 %all-gather.15.cloned.1.call-done = bf16[64,256,128]{2,1,0:T(8,128)(2,1)} async-done(((bf16[16,256,128]{2,1,0:T(8,128)(2,1)}), bf16[64,256,128]{2,1,0:T(8,128)(2,1)}) %all-gather.15.cloned.1.call-update) | async-done | bytes 4194320 | tf_op jit(solution)/shard_map/all_gather | solution.py:49
  348.2 4.7 %copy.41 = bf16[16,4,256,128]{3,2,1,0:T(8,128)(2,1)} copy(bf16[16,4,256,128]{3,2,0,1:T(8,128)(2,1)} %bitcast.171) | data formatting | bytes 8388608 | tf_op jit(solution)/shard_map/transpose | solution.py:52
  352.9 41.5 %while.14 = (s32[]{:T(128)}, f32[1,2,256]{2,1,0:T(2,128)S(1)}, f32[1,2,256]{2,1,0:T(2,128)S(1)}, f32[1,2,256,128]{3,2,1,0:T(8,128)S(1)}, bf16[8,2048,128]{2,1,0:...) while((s32[]{:T(128)}, f32[1,2,256]{2,1,0:T(2,128)S(1)}, ...), condition=%wide.region_16.17_spmd, body=%wide.region_13.16_spmd.sunk | while | flops 548537856 | bytes 14361697 | solution.py:139
  354.7 2.4 fusion.126
  359.9 2.4 fusion.126
  365.1 2.4 fusion.126
  370.3 2.4 fusion.126
  375.5 2.4 fusion.126
  385.8 2.4 fusion.126
  396.1 5.1 %all-to-all-start.4 = ((bf16[8,32,2048]{2,1,0:T(8,128)(2,1)}), bf16[8,32,2048]{2,1,0:T(8,128)(2,1)S(1)}, u32[]{:S(2)}, u32[]{:S(2)}) async-start(bf16[8,32,2048]{2,1,0:T(8,128)(2,1)} %bitcast.53), calls=%async_computation.4 | async-start | bytes 2097152 | tf_op jit(solution)/shard_map/all_to_all | solution.py:67
  401.2 15.0 %all-to-all-done.4 = bf16[8,32,2048]{2,1,0:T(8,128)(2,1)S(1)} async-done(((bf16[8,32,2048]{2,1,0:T(8,128)(2,1)}), bf16[8,32,2048]{2,1,0:T(8,128)(2,1)S(1)}, u32[]{:S(2)}, u32[]{:S(2)}) %all-to-all-start.4) | async-done | bytes 1048608 | tf_op jit(solution)/shard_map/all_to_all | solution.py:67
  (135 shorter events, 46.6 us)
Async XLA Ops:
  6.5 388.1 %copy-start = (bf16[256,2048]{1,0:T(8,128)(2,1)S(1)}, bf16[256,2048]{1,0:T(8,128)(2,1)}, u32[]{:S(2)}) copy-start(bf16[256,2048]{1,0:T(8,128)(2,1)} %param.31) | copy-start | bytes 3145732
  49.5 18.7 %all-to-all-start.1 = ((f32[8,2,256]{2,1,0:T(2,128)}), f32[8,2,256]{2,1,0:T(2,128)S(1)}, u32[]{:S(2)}, u32[]{:S(2)}) async-start(f32[8,2,256]{2,1,0:T(2,128)} %broadcast_in_dim.23), calls=%async_computation.1 | async-start | bytes 32768 | tf_op jit(solution)/shard_map/all_to_all | solution.py:27
  68.8 8.6 %all-to-all-start.2 = ((f32[8,2,256]{2,1,0:T(2,128)}), f32[8,2,256]{2,1,0:T(2,128)S(1)}, u32[]{:S(2)}, u32[]{:S(2)}) async-start(f32[8,2,256]{2,1,0:T(2,128)} %broadcast_in_dim.24), calls=%async_computation.2 | async-start | bytes 32768 | tf_op jit(solution)/shard_map/all_to_all | solution.py:27
  79.5 19.2 %all-to-all-start.3 = ((bf16[8,32,2048]{2,1,0:T(8,128)(2,1)}), bf16[8,32,2048]{2,1,0:T(8,128)(2,1)S(1)}, u32[]{:S(2)}, u32[]{:S(2)}) async-start(bf16[8,32,2048]{2,1,0:T(8,128)(2,1)} %broadcast_in_dim.25), calls=%async_computation.3 | async-start | bytes 2097152 | tf_op jit(solution)/shard_map/all_to_all | solution.py:27
  83.7 17.5 %copy-start.5 = (f32[128]{0:T(128)S(1)}, f32[128]{0:T(128)}, u32[]{:S(2)}) copy-start(f32[128]{0:T(128)} %param.27) | copy-start | bytes 1540
  83.7 71.2 %all-gather.9.cloned.1.call-start = ((), (), s32[]{:S(2)}) async-start(), calls=%async_computation.5 | async-start | bytes 1114112 | tf_op jit(solution)/shard_map/all_gather | solution.py:49
  98.7 141.9 %copy-start.2 = (bf16[8,2048]{1,0:T(8,128)(2,1)S(1)}, bf16[8,2048]{1,0:T(8,128)(2,1)}, u32[]{:S(2)}) copy-start(bf16[8,2048]{1,0:T(8,128)(2,1)} %param.20) | copy-start | bytes 98308
  98.7 143.1 %copy-start.4 = (f32[2048]{0:T(1024)S(1)}, f32[2048]{0:T(1024)}, u32[]{:S(2)}) copy-start(f32[2048]{0:T(1024)} %param.24) | copy-start | bytes 24580
  101.0 140.8 %copy-start.7 = (bf16[2048,128]{1,0:T(8,128)(2,1)S(1)}, bf16[2048,128]{1,0:T(8,128)(2,1)}, u32[]{:S(2)}) copy-start(bf16[2048,128]{1,0:T(8,128)(2,1)} %param.30) | copy-start | bytes 1572868
  102.3 211.3 %copy-start.6 = (f32[128]{0:T(128)S(1)}, f32[128]{0:T(128)}, u32[]{:S(2)}) copy-start(f32[128]{0:T(128)} %param.26) | copy-start | bytes 1540
  102.4 122.4 %all-gather.13.cloned.1.call-start = ((), (), s32[]{:S(2)}) async-start(), calls=%async_computation.7 | async-start | bytes 1114112 | tf_op jit(solution)/shard_map/all_gather | solution.py:49
  103.1 212.2 %all-gather.11.cloned.1.call-start = ((), (), s32[]{:S(2)}) async-start(), calls=%async_computation.6 | async-start | bytes 5242880 | tf_op jit(solution)/shard_map/all_gather | solution.py:49
  155.0 193.3 %all-gather.15.cloned.1.call-start = ((), (), s32[]{:S(2)}) async-start(), calls=%async_computation.8 | async-start | bytes 5242880 | tf_op jit(solution)/shard_map/all_gather | solution.py:49
  225.3 170.7 %all-to-all-start = ((f32[8,2,256]{2,1,0:T(2,128)}), f32[8,2,256]{2,1,0:T(2,128)S(1)}, u32[]{:S(2)}, u32[]{:S(2)}) async-start(f32[8,2,256]{2,1,0:T(2,128)} %broadcast_in_dim.22), calls=%async_computation | async-start | bytes 32768 | tf_op jit(solution)/shard_map/all_to_all | solution.py:27
  394.4 22.0 %copy-start.1 = (bf16[32,2048]{1,0:T(8,128)(2,1)S(1)}, bf16[32,2048]{1,0:T(8,128)(2,1)}, u32[]{:S(2)}) copy-start(bf16[32,2048]{1,0:T(8,128)(2,1)} %param.17) | copy-start | bytes 393220
  394.4 22.0 %copy-start.3 = (f32[2048]{0:T(1024)S(1)}, f32[2048]{0:T(1024)}, u32[]{:S(2)}) copy-start(f32[2048]{0:T(1024)} %param.25) | copy-start | bytes 24580
  396.1 20.1 %all-to-all-start.4 = ((bf16[8,32,2048]{2,1,0:T(8,128)(2,1)}), bf16[8,32,2048]{2,1,0:T(8,128)(2,1)S(1)}, u32[]{:S(2)}, u32[]{:S(2)}) async-start(bf16[8,32,2048]{2,1,0:T(8,128)(2,1)} %bitcast.53), calls=%async_computation.4 | async-start | bytes 2097152 | tf_op jit(solution)/shard_map/all_to_all | solution.py:67
Sparse Core Ops, SparseCore 0:
  102.5 52.4 all-gather.8
  157.0 67.6 all-gather.12
  226.8 63.0 all-gather.10
  291.9 56.2 all-gather.14
where the time goes:
time: 425 us; the launch traced here: 424 us
  waiting for transfers between devices  188 us (44%)
  blocking collectives  109 us (26%)
  starting transfers between devices  42.6 us (10%)
  matrix products  42.3 us (10%)
  local copies, waits for them, and re-layouts  14.5 us (3%)
  other arithmetic  13.5 us (3%)
  between operations  13.5 us (3%)
    all_gather x4, waiting for transfers between devices, gather_in_order(): blocks = lax.all_gather(blocks, axes[k])  150 us
    all_gather x1, blocking collectives, one_gather(): lines, at, outs = (lax.all_gather(ravelled, axis), 0, [])  69.4 us
    psum x2, blocking collectives, by_axis(): return functools.reduce(lax.psum, axes, value)  39.6 us
    all_to_all x4, starting transfers between devices, from_everyone(): lax.all_to_all(jnp.broadcast_to(value[None], (devices, *value.shape)), ax...  37.4 us
    all_to_all x4, waiting for transfers between devices, from_everyone(): lax.all_to_all(jnp.broadcast_to(value[None], (devices, *value.shape)), ax...  23.2 us
    dot_general x9, matrix products, absorb(): jnp.einsum('kgts,skd->kgtd', terms.astype(jnp.bfloat16), value_heads, pre...  19.9 us
    all_to_all x1, waiting for transfers between devices, summed_on_arrival(): lax.all_to_all(blocks, axis, split_axis=0, concat_axis=0, tiled=True)  15 us
    dot_general x9, matrix products, absorb(): jnp.einsum('tkgd,skd->kgts', grouped_query, key_heads, preferred_element_...  14.7 us
  transfers between devices with their start and end apart: 9, of which 7 were waited for; matrix products, arithmetic and copies ran while one was open for 14% of the time, Pallas kernels for 0%

commit v1 on v0

v1 whole, which is shorter than its diff:
```python
import functools
import math

import jax
import jax.numpy as jnp
from jax import lax
from jax.experimental import pallas as pl
from jax.experimental.pallas import tpu as pltpu
from jax.sharding import Mesh
from jax.sharding import PartitionSpec as P

GRID_W = 64
LOG2E = math.log2(math.e)
ALL = ("z", "y", "tp")
F32 = jnp.float32
BF16 = jnp.bfloat16

STAGES = [[(s, 1), (-s, -1)] for s in range(1, 8)] + [[(8, 1)]]


def from_everyone(value, axes):
    devices = lax.axis_size(axes)
    return lax.all_to_all(
        jnp.broadcast_to(value[None], (devices, *value.shape)), axes, 0, 0, tiled=True
    )


def rms_rows(values):
    return values * lax.rsqrt(jnp.mean(values * values, axis=-1, keepdims=True) + 1e-06)


def rms(values, gain):
    values = values.astype(F32)
    return rms_rows(values) * gain


def rotation_tables(positions, grid_width, head_dim):
    half = head_dim // 2
    quarter = head_dim // 4
    lane = jnp.arange(head_dim)
    j = (lane % quarter).astype(F32)
    freqs = 10000.0 ** (-(2.0 * j) / half)
    row_pos = (positions // grid_width).astype(F32)[:, None]
    col_pos = (positions % grid_width).astype(F32)[:, None]
    angle = jnp.where(lane[None] < half, row_pos, col_pos) * freqs[None]
    first = ((lane % half) < quarter)[None]
    sine = jnp.sin(angle)
    return (
        jnp.cos(angle),
        jnp.where(first, -sine, 0.0),
        jnp.where(first, 0.0, sine),
    )


def project_kernel(lat, ctx, gain, mods, wq, wk, wv, qg, kg, cos, sa, sb, q_out, msg):
    rows = lat.shape[0]
    ctx_rows = ctx.shape[0]
    head_dim = kg.shape[1]
    quarter = head_dim // 4
    g = gain[...]
    x = rms_rows(lat[...].astype(F32)) * g
    x = (x * (1.0 + mods[1:2]) + mods[0:1]).astype(BF16)
    c = rms_rows(ctx[...].astype(F32)) * g
    c = (c * (1.0 + mods[3:4]) + mods[2:3]).astype(BF16)

    def turned(v, gain_row):
        v = rms_rows(v) * gain_row
        up = pltpu.roll(v, head_dim - quarter, 1)
        down = pltpu.roll(v, quarter, 1)
        return v * cos[...] + up * sa[...] + down * sb[...]

    both = jnp.concatenate([x, c], axis=0)
    k = jnp.dot(both, wk[...], preferred_element_type=F32)
    v = jnp.dot(both, wv[...], preferred_element_type=F32)
    msg[0:rows] = turned(k[:rows], kg[...]).astype(BF16)
    msg[rows : 2 * rows] = v[:rows].astype(BF16)
    tail = jnp.concatenate([rms_rows(k[rows:]) * kg[...], v[rows:]], axis=0)
    msg[2 * rows : 2 * rows + 2 * ctx_rows] = tail.astype(BF16)
    q = jnp.dot(x, wq[...], preferred_element_type=F32)
    for h in range(q.shape[1] // head_dim):
        qh = turned(q[:, h * head_dim : (h + 1) * head_dim], qg[...])
        q_out[:, h * rows : (h + 1) * rows] = jnp.transpose(qh).astype(BF16)


def attend_kernel(*refs, blocks, keys, has_ctx, first, last, factor, lift):
    refs = list(refs)
    q = refs.pop(0)
    kv = [refs.pop(0) for _ in range(blocks)]
    ctx = refs.pop(0) if has_ctx else None
    if not first:
        m_in, l_in, acc_in = refs.pop(0), refs.pop(0), refs.pop(0)
    qv = q[0]
    scores = [jnp.dot(r[0:keys], qv, preferred_element_type=F32) for r in kv]
    largest = functools.reduce(jnp.maximum, [jnp.max(s, axis=0, keepdims=True) for s in scores])
    largest = largest * factor
    values = [r[keys : 2 * keys] for r in kv]
    if has_ctx:
        half = ctx.shape[0] // 2
        cs = jnp.dot(ctx[0:half], qv, preferred_element_type=F32) * factor + lift
        largest = jnp.maximum(largest, jnp.max(cs, axis=0, keepdims=True))
    if not first:
        largest = jnp.maximum(largest, m_in[0])
        fade = jnp.exp2(m_in[0] - largest)
        total = l_in[0] * fade
        acc = acc_in[0] * fade
    else:
        total = jnp.zeros_like(largest)
        acc = None
    terms = [jnp.exp2(s * factor - largest) for s in scores]
    if has_ctx:
        terms.append(jnp.exp2(cs - largest))
        values.append(ctx[half : 2 * half])
    for p, v in zip(terms, values):
        total = total + jnp.sum(p, axis=0, keepdims=True)
        part = lax.dot_general(
            v, p.astype(BF16), (((0,), (0,)), ((), ())), preferred_element_type=F32
        )
        acc = part if acc is None else acc + part
    if last:
        (out,) = refs
        dim = acc.shape[0]
        out[0, 0:dim] = (acc / total).astype(BF16)
        lse = largest + jnp.log2(total)
        hi = lse.astype(BF16).astype(F32)
        mid = (lse - hi).astype(BF16).astype(F32)
        low = lse - hi - mid
        row = lax.broadcasted_iota(jnp.int32, (16, lse.shape[1]), 0)
        packed = jnp.where(row == 0, hi, jnp.where(row == 1, mid, jnp.where(row == 2, low, 0.0)))
        out[0, dim : dim + 16] = packed.astype(BF16)
    else:
        m_out, l_out, acc_out = refs
        m_out[0] = largest
        l_out[0] = total
        acc_out[0] = acc


def attend(q_all, messages, ctx, carry, last, keys, factor, lift):
    parts, dim, width = q_all.shape
    first = carry is None
    full = lambda a: pl.BlockSpec(a.shape, lambda i: (0,) * a.ndim)
    part = lambda n: pl.BlockSpec((1, n, width), lambda i: (i, 0, 0))
    operands = [q_all, *messages]
    specs = [part(dim)] + [full(a) for a in messages]
    if ctx is not None:
        operands.append(ctx)
        specs.append(full(ctx))
    if not first:
        operands += list(carry)
        specs += [part(1), part(1), part(dim)]
    if last:
        out_shape = (jax.ShapeDtypeStruct((parts, dim + 16, width), BF16),)
        out_specs = (part(dim + 16),)
    else:
        out_shape = (
            jax.ShapeDtypeStruct((parts, 1, width), F32),
            jax.ShapeDtypeStruct((parts, 1, width), F32),
            jax.ShapeDtypeStruct((parts, dim, width), F32),
        )
        out_specs = (part(1), part(1), part(dim))
    all_keys = keys * len(messages) + (0 if ctx is None else ctx.shape[0] // 2)
    return pl.pallas_call(
        functools.partial(
            attend_kernel,
            blocks=len(messages),
            keys=keys,
            has_ctx=ctx is not None,
            first=first,
            last=last,
            factor=factor,
            lift=lift,
        ),
        grid=(parts,),
        in_specs=specs,
        out_specs=out_specs,
        out_shape=out_shape,
        cost_estimate=pl.CostEstimate(
            flops=4 * all_keys * parts * width * dim,
            bytes_accessed=2 * parts * width * dim * 4,
            transcendentals=all_keys * parts * width,
        ),
        name="attend",
    )(*operands)


def merge_kernel(parts, w_out, out):
    count, rows, width = parts.shape
    dim = rows - 16
    tail = [parts[i, dim : dim + 16].astype(F32) for i in range(count)]
    lse = [t[0:1] + t[1:2] + t[2:3] for t in tail]
    top = functools.reduce(jnp.maximum, lse)
    share = [jnp.exp2(v - top) for v in lse]
    whole = functools.reduce(jnp.add, share)
    merged = functools.reduce(
        jnp.add, [parts[i, 0:dim].astype(F32) * share[i] for i in range(count)]
    )
    merged = (merged / whole).astype(BF16)
    heads = w_out.shape[0] // dim
    rows = width // heads
    stacked = jnp.concatenate(
        [merged[:, h * rows : (h + 1) * rows] for h in range(heads)], axis=0
    )
    out[...] = lax.dot_general(
        stacked, w_out[...], (((0,), (0,)), ((), ())), preferred_element_type=F32
    ).astype(BF16)


def body(
    latent,
    condition,
    context_condition,
    context,
    w_shift,
    w_scale,
    w_gate,
    pre_gain,
    post_gain,
    query_gain,
    key_gain,
    w_query,
    w_key,
    w_value,
    w_out,
):
    tp_count = lax.axis_size("tp")
    z_count = lax.axis_size("z")
    y_count = lax.axis_size("y")
    model = latent.shape[1]
    head_dim = query_gain.shape[0]
    tok_dev = latent.shape[0] * tp_count
    ctx_dev = context.shape[0]
    heads_dev = w_query.shape[1] // head_dim
    factor = head_dim ** (-0.5) * LOG2E
    lift = math.log(tok_dev / (4.0 * ctx_dev)) * LOG2E

    gathered = from_everyone(latent, "tp").reshape(tok_dev, model)

    conds = jax.nn.silu(jnp.stack([condition, context_condition]).astype(F32)).astype(BF16)
    shift_part, scale_part, gate_part = (
        jnp.dot(conds, weight, preferred_element_type=F32) for weight in (w_shift, w_scale, w_gate)
    )
    partial_mod = jnp.concatenate(
        [shift_part[0:1], scale_part[0:1], shift_part[1:2], scale_part[1:2], gate_part[0:1]], axis=0
    )
    partial_mod = from_everyone(partial_mod, "z").sum(axis=0)
    pieces = from_everyone(partial_mod, ("y", "tp"))
    mods = pieces.reshape(y_count, tp_count, *partial_mod.shape).sum(axis=0)
    mods = mods.transpose(1, 0, 2).reshape(partial_mod.shape[0], model)

    positions = (lax.axis_index("z") * y_count + lax.axis_index("y")) * tok_dev + jnp.arange(tok_dev)
    cos, sa, sb = rotation_tables(positions, GRID_W, head_dim)
    msg_rows = 2 * tok_dev + 2 * ctx_dev
    query, message = pl.pallas_call(
        project_kernel,
        out_shape=(
            jax.ShapeDtypeStruct((head_dim, heads_dev * tok_dev), BF16),
            jax.ShapeDtypeStruct((msg_rows, head_dim), BF16),
        ),
        cost_estimate=pl.CostEstimate(
            flops=2 * tok_dev * model * 4 * head_dim,
            bytes_accessed=2 * model * (4 * head_dim + tok_dev),
            transcendentals=0,
        ),
        name="project",
    )(
        gathered,
        context,
        pre_gain[None],
        mods[0:4],
        w_query,
        w_key,
        w_value,
        query_gain[None],
        key_gain[None],
        cos,
        sa,
        sb,
    )

    def receive(value, hop):
        turn = [((i + hop) % z_count, i) for i in range(z_count)]
        return lax.ppermute(value, "z", turn)

    q_all = from_everyone(query, "y")
    held = {0: message}
    carry = None
    waiting = [message]
    for stage in STAGES:
        arrived = {d: receive(held[d - hop], hop) for d, hop in stage}
        carry = attend(q_all, waiting, None, carry, False, tok_dev, factor, lift)
        held.update(arrived)
        waiting = list(arrived.values())
    tails = [held[d][2 * tok_dev :] for d in sorted(held)]
    ctx = jnp.concatenate([t[:ctx_dev] for t in tails] + [t[ctx_dev:] for t in tails], axis=0)
    (partials,) = attend(q_all, waiting, ctx, carry, True, tok_dev, factor, lift)
    returned = lax.all_to_all(partials, "y", 0, 0, tiled=True)
    mixed = pl.pallas_call(
        merge_kernel,
        out_shape=jax.ShapeDtypeStruct((tok_dev, model), BF16),
        cost_estimate=pl.CostEstimate(
            flops=2 * tok_dev * model * heads_dev * head_dim,
            bytes_accessed=4 * tok_dev * model,
            transcendentals=0,
        ),
        name="merge",
    )(returned, w_out)
    arrived = lax.all_to_all(mixed.reshape(tp_count, -1, model), "tp", 0, 0, tiled=True)
    mixed = arrived.astype(F32).sum(axis=0)
    updated = latent.astype(F32) + mods[4] * rms(mixed, post_gain)
    return updated.astype(BF16)


def solution(mesh):
    tp_count = mesh.shape["tp"]
    torus = Mesh(mesh.devices.reshape(16, 4, tp_count), ALL)
    sp = ("z", "y")
    placed = (
        P(ALL, None),
        P(sp),
        P(sp),
        P(sp, None),
        P(sp, "tp"),
        P(sp, "tp"),
        P(sp, "tp"),
        P(),
        P(),
        P(),
        P(),
        P(None, "tp"),
        P(None, "tp"),
        P(None, "tp"),
        P("tp", None),
    )
    return jax.shard_map(
        body, mesh=torus, in_specs=placed, out_specs=P(ALL, None), check_vma=False
    )
```

time: 425 us -> 240 us (0.56)
  waiting for transfers between devices: 188 us -> 30.2 us
  Pallas kernels: 0 us -> 53.3 us
  blocking collectives: 109 us -> 58.5 us
  matrix products: 42.3 us -> 1.79 us
  starting transfers between devices: 42.6 us -> 65.7 us
  between operations: 13.5 us -> 0.48 us
  local copies, waits for them, and re-layouts: 14.5 us -> 25 us
  other arithmetic: 13.5 us -> 3.12 us
    all_gather x4 -> x0, waiting for transfers between devices: 150 us -> none  [gather_in_order(): blocks = lax.all_gather(blocks, axes[k])]
    all_gather x1 -> x0, blocking collectives: 69.4 us -> none  [one_gather(): lines, at, outs = (lax.all_gather(ravelled, axis), 0, [])]
    all_to_all x0 -> x3, blocking collectives: none -> 58.5 us  [the longest x2 47 us: from_everyone(): lax.all_to_all(jnp.broadcast_to(value[None], (devices, *value.shape)), ax...]
    pallas_call x0 -> x11, Pallas kernels: none -> 53.3 us  [the longest x9 46.1 us: attend(): pl.pallas_call(functools.partial(attend_kernel, blocks=len(messages), key...]
    ppermute x0 -> x15, starting transfers between devices: none -> 47.3 us  [receive(): return lax.ppermute(value, 'z', turn)]
    dot_general x24 -> x3, matrix products: 42.3 us -> 1.79 us  [body(): jnp.dot(conds, weight, preferred_element_type=F32)]
    psum x2 -> x0, blocking collectives: 39.6 us -> none  [by_axis(): return functools.reduce(lax.psum, axes, value)]
    all_to_all x4 -> x2, starting transfers between devices: 37.4 us -> 7.07 us  [from_everyone(): lax.all_to_all(jnp.broadcast_to(value[None], (devices, *value.shape)), ax...]
  transfers between devices with their start and end apart: 9 -> 18, of which waited for: 7 -> 5; matrix products, arithmetic and copies ran while one was open for 14% -> 5% of each run, Pallas kernels for 0% -> 17%
where the time goes in v1:
time: 240 us; the launch traced here: 238 us
  starting transfers between devices  65.7 us (27%)
  blocking collectives  58.5 us (24%)
  Pallas kernels  53.3 us (22%)
  waiting for transfers between devices  30.2 us (13%)
  local copies, waits for them, and re-layouts  25 us (10%)
  other arithmetic  3.12 us (1%)
    ppermute x15, starting transfers between devices, receive(): return lax.ppermute(value, 'z', turn)  47.3 us
    all_to_all x2, blocking collectives, from_everyone(): lax.all_to_all(jnp.broadcast_to(value[None], (devices, *value.shape)), ax...  47 us
    pallas_call x9, Pallas kernels, attend(): pl.pallas_call(functools.partial(attend_kernel, blocks=len(messages), key...  46.1 us
    unnamed x76, local copies, waits for them, and re-layouts  22.1 us
    all_to_all x1, waiting for transfers between devices, body(): lax.all_to_all(mixed.reshape(tp_count, -1, model), 'tp', 0, 0, tiled=True)  15 us
    all_to_all x2, waiting for transfers between devices, from_everyone(): lax.all_to_all(jnp.broadcast_to(value[None], (devices, *value.shape)), ax...  13 us
    all_to_all x1, blocking collectives, body(): returned = lax.all_to_all(partials, 'y', 0, 0, tiled=True)  11.5 us
    all_to_all x1, starting transfers between devices, body(): lax.all_to_all(mixed.reshape(tp_count, -1, model), 'tp', 0, 0, tiled=True)  11.3 us
  transfers between devices with their start and end apart: 18, of which 5 were waited for; matrix products, arithmetic and copies ran while one was open for 5% of the time, Pallas kernels for 17%

profile of v1, /device:TPU:1, one launch (start us, length us, event | category | flops | bytes accessed | tf_op | source)
XLA Modules:
  0.0 238.1 jit_solution(6728875861983105848)
XLA Ops:
  2.6 27.5 %all_to_all.30 = f32[16,5,256]{2,1,0:T(8,128)S(1)} all-to-all(f32[16,5,256]{2,1,0:T(8,128)S(1)} %broadcast_in_dim.86), channel_id=1, replica_groups=mesh['z'=16,'y'=4,'tp'=8] {'z'}, dimensions={0} | all-to-all | bytes 163840 | tf_op jit(solution)/shard_map/all_to_all | solution.py:23
  30.1 19.5 %all_to_all.31 = f32[32,5,256]{2,1,0:T(8,128)S(1)} all-to-all(f32[32,5,256]{2,1,0:T(8,128)S(1)} %broadcast_in_dim.87), channel_id=1, replica_groups=mesh['z'=16,'y'=4,'tp'=8] {'y','tp'}, dimensions={0} | all-to-all | bytes 327680 | tf_op jit(solution)/shard_map/all_to_all | solution.py:23
  50.8 3.6 %all-to-all-start.2 = ((bf16[8,32,2048]{2,1,0:T(8,128)(2,1)}), bf16[8,32,2048]{2,1,0:T(8,128)(2,1)S(1)}, u32[]{:S(2)}, u32[]{:S(2)}) async-start(bf16[8,32,2048]{2,1,0:T(8,128)(2,1)} %broadcast_in_dim.88), calls=%async_computation.2 | async-start | bytes 2097152 | tf_op jit(solution)/shard_map/all_to_all | solution.py:23
  56.4 13.0 %all-to-all-done.2 = bf16[8,32,2048]{2,1,0:T(8,128)(2,1)S(1)} async-done(((bf16[8,32,2048]{2,1,0:T(8,128)(2,1)}), bf16[8,32,2048]{2,1,0:T(8,128)(2,1)S(1)}, u32[]{:S(2)}, u32[]{:S(2)}) %all-to-all-start.2) | async-done | bytes 1048608 | tf_op jit(solution)/shard_map/all_to_all | solution.py:23
  70.4 4.3 %project.1 = (bf16[128,512]{1,0:T(8,128)(2,1)}, bf16[528,128]{1,0:T(8,128)(2,1)}) custom-call(bf16[256,2048]{1,0:T(8,128)(2,1)} %bitcast.22, bf16[8,2048]{1,0:T(8,128)(2,1)} %ctx.1, f32[1,2048]{1,0:T(1,128)} %bitcast.29, f32[4,2048]{1,0:T(4,128)} %bitcast.27, bf16[2048,256]{1,0:T(8,128)(2,1)} %wq.1, bf16[2048,128]{1,0:T(8,128)(2,1)} %wk.1, ...), custom_call_target="tpu_custom_call" | custom-call | flops 536870912 | bytes 3145728 | tf_op jit(solution)/shard_map/project/pallas_call | solution.py:252
  77.6 3.5 %collective-permute-start = (bf16[528,128]{1,0:T(8,128)(2,1)}, bf16[528,128]{1,0:T(8,128)(2,1)S(1)}, u32[]{:S(2)}, u32[]{:S(2)}) collective-permute-start(bf16[528,128]{1,0:T(8,128)(2,1)} %get-tuple-element.32.refs_1_), channel_id=1, source_target_pairs={{32,0},{64,32},{96,64},{128,96},{160,128},{192,160},{224,192},{256... | collective-permute-start | bytes 405512 | tf_op jit(solution)/shard_map/ppermute | solution.py:281
  84.1 4.6 %collective-permute-start.1 = (bf16[528,128]{1,0:T(8,128)(2,1)S(1)}, bf16[528,128]{1,0:T(8,128)(2,1)S(1)}, u32[]{:S(2)}, u32[]{:S(2)}) collective-permute-start(bf16[528,128]{1,0:T(8,128)(2,1)S(1)} %collective-permute-done.refs_1_), channel_id=1, source_target_pairs={{32,0},{64,32},{96,64},{128,96},{160,128},{192,160},{224,192},{256... | collective-permute-start | bytes 405512 | tf_op jit(solution)/shard_map/ppermute | solution.py:281
  95.8 4.6 %collective-permute-start.2 = (bf16[528,128]{1,0:T(8,128)(2,1)S(1)}, bf16[528,128]{1,0:T(8,128)(2,1)S(1)}, u32[]{:S(2)}, u32[]{:S(2)}) collective-permute-start(bf16[528,128]{1,0:T(8,128)(2,1)S(1)} %collective-permute-done.1.refs_1_), channel_id=1, source_target_pairs={{32,0},{64,32},{96,64},{128,96},{160,128},{192,160},{224,192},{256... | collective-permute-start | bytes 405512 | tf_op jit(solution)/shard_map/ppermute | solution.py:281
  103.1 4.6 %collective-permute-start.3 = (bf16[528,128]{1,0:T(8,128)(2,1)S(1)}, bf16[528,128]{1,0:T(8,128)(2,1)S(1)}, u32[]{:S(2)}, u32[]{:S(2)}) collective-permute-start(bf16[528,128]{1,0:T(8,128)(2,1)S(1)} %collective-permute-done.2.refs_1_), channel_id=1, source_target_pairs={{32,0},{64,32},{96,64},{128,96},{160,128},{192,160},{224,192},{256... | collective-permute-start | bytes 405512 | tf_op jit(solution)/shard_map/ppermute | solution.py:281
  110.0 4.6 %collective-permute-start.4 = (bf16[528,128]{1,0:T(8,128)(2,1)S(1)}, bf16[528,128]{1,0:T(8,128)(2,1)S(1)}, u32[]{:S(2)}, u32[]{:S(2)}) collective-permute-start(bf16[528,128]{1,0:T(8,128)(2,1)S(1)} %collective-permute-done.3.refs_1_), channel_id=1, source_target_pairs={{32,0},{64,32},{96,64},{128,96},{160,128},{192,160},{224,192},{256... | collective-permute-start | bytes 405512 | tf_op jit(solution)/shard_map/ppermute | solution.py:281
  115.4 4.3 %attend.9 = (f32[4,1,512]{2,1,0:T(1,128)}, f32[4,1,512]{2,1,0:T(1,128)}, f32[4,128,512]{2,1,0:T(8,128)}) custom-call(bf16[4,128,512]{2,1,0:T(8,128)(2,1)} %copy-done.2, bf16[528,128]{1,0:T(8,128)(2,1)} %get-tuple-element.32.refs_1_), custom_call_target="tpu_custom_call" | custom-call | flops 268435456 | bytes 2097152 | tf_op jit(solution)/shard_map/attend/pallas_call | solution.py:161
  121.7 5.3 %attend.10 = (f32[4,1,512]{2,1,0:T(1,128)}, f32[4,1,512]{2,1,0:T(1,128)}, f32[4,128,512]{2,1,0:T(8,128)}) custom-call(bf16[4,128,512]{2,1,0:T(8,128)(2,1)} %copy-done.2, bf16[528,128]{1,0:T(8,128)(2,1)} %copy-done.7, bf16[528,128]{1,0:T(8,128)(2,1)} %copy-done.8, f32[4,1,512]{2,1,0:T(1,128)} %get-tuple-element.33.refs_3_, ...), custom_call_target="tpu_custom_call" | custom-call | flops 536870912 | bytes 2097152 | tf_op jit(solution)/shard_map/attend/pallas_call | solution.py:161
  127.0 5.3 %attend.11 = (f32[4,1,512]{2,1,0:T(1,128)}, f32[4,1,512]{2,1,0:T(1,128)}, f32[4,128,512]{2,1,0:T(8,128)}) custom-call(bf16[4,128,512]{2,1,0:T(8,128)(2,1)} %copy-done.2, bf16[528,128]{1,0:T(8,128)(2,1)} %copy-done.9, bf16[528,128]{1,0:T(8,128)(2,1)} %copy-done.10, f32[4,1,512]{2,1,0:T(1,128)} %get-tuple-element.36.refs_3_, ...), custom_call_target="tpu_custom_call" | custom-call | flops 536870912 | bytes 2097152 | tf_op jit(solution)/shard_map/attend/pallas_call | solution.py:161
  132.3 4.6 %collective-permute-start.5 = (bf16[528,128]{1,0:T(8,128)(2,1)S(1)}, bf16[528,128]{1,0:T(8,128)(2,1)S(1)}, u32[]{:S(2)}, u32[]{:S(2)}) collective-permute-start(bf16[528,128]{1,0:T(8,128)(2,1)S(1)} %collective-permute-done.4.refs_1_), channel_id=1, source_target_pairs={{32,0},{64,32},{96,64},{128,96},{160,128},{192,160},{224,192},{256... | collective-permute-start | bytes 405512 | tf_op jit(solution)/shard_map/ppermute | solution.py:281
  136.9 5.3 %attend.12 = (f32[4,1,512]{2,1,0:T(1,128)}, f32[4,1,512]{2,1,0:T(1,128)}, f32[4,128,512]{2,1,0:T(8,128)}) custom-call(bf16[4,128,512]{2,1,0:T(8,128)(2,1)} %copy-done.2, bf16[528,128]{1,0:T(8,128)(2,1)} %copy-done.11, bf16[528,128]{1,0:T(8,128)(2,1)} %copy-done.12, f32[4,1,512]{2,1,0:T(1,128)} %get-tuple-element.39.refs_3_, ...), custom_call_target="tpu_custom_call" | custom-call | flops 536870912 | bytes 2097152 | tf_op jit(solution)/shard_map/attend/pallas_call | solution.py:161
  144.2 5.3 %attend.13 = (f32[4,1,512]{2,1,0:T(1,128)}, f32[4,1,512]{2,1,0:T(1,128)}, f32[4,128,512]{2,1,0:T(8,128)}) custom-call(bf16[4,128,512]{2,1,0:T(8,128)(2,1)} %copy-done.2, bf16[528,128]{1,0:T(8,128)(2,1)} %copy-done.13, bf16[528,128]{1,0:T(8,128)(2,1)} %copy-done.15, f32[4,1,512]{2,1,0:T(1,128)} %get-tuple-element.42.refs_3_, ...), custom_call_target="tpu_custom_call" | custom-call | flops 536870912 | bytes 2097152 | tf_op jit(solution)/shard_map/attend/pallas_call | solution.py:161
  149.5 5.3 %attend.14 = (f32[4,1,512]{2,1,0:T(1,128)}, f32[4,1,512]{2,1,0:T(1,128)}, f32[4,128,512]{2,1,0:T(8,128)}) custom-call(bf16[4,128,512]{2,1,0:T(8,128)(2,1)} %copy-done.2, bf16[528,128]{1,0:T(8,128)(2,1)} %copy-done.14, bf16[528,128]{1,0:T(8,128)(2,1)} %copy-done.16, f32[4,1,512]{2,1,0:T(1,128)} %get-tuple-element.45.refs_3_, ...), custom_call_target="tpu_custom_call" | custom-call | flops 536870912 | bytes 2097152 | tf_op jit(solution)/shard_map/attend/pallas_call | solution.py:161
  154.8 4.6 %collective-permute-start.6 = (bf16[528,128]{1,0:T(8,128)(2,1)S(1)}, bf16[528,128]{1,0:T(8,128)(2,1)S(1)}, u32[]{:S(2)}, u32[]{:S(2)}) collective-permute-start(bf16[528,128]{1,0:T(8,128)(2,1)S(1)} %collective-permute-done.5.refs_1_), channel_id=1, source_target_pairs={{32,0},{64,32},{96,64},{128,96},{160,128},{192,160},{224,192},{256... | collective-permute-start | bytes 405512 | tf_op jit(solution)/shard_map/ppermute | solution.py:281
  159.4 5.3 %attend.15 = (f32[4,1,512]{2,1,0:T(1,128)}, f32[4,1,512]{2,1,0:T(1,128)}, f32[4,128,512]{2,1,0:T(8,128)}) custom-call(bf16[4,128,512]{2,1,0:T(8,128)(2,1)} %copy-done.2, bf16[528,128]{1,0:T(8,128)(2,1)} %copy-done.17, bf16[528,128]{1,0:T(8,128)(2,1)} %collective-permute-done.13.refs_2_, f32[4,1,512]{2,1,0:T(1,128)} %get-tuple-element.48.refs_3_, ...), custom_call_target="tpu_custom_call" | custom-call | flops 536870912 | bytes 2097152 | tf_op jit(solution)/shard_map/attend/pallas_call | solution.py:161
  175.4 5.3 %attend.16 = (f32[4,1,512]{2,1,0:T(1,128)}, f32[4,1,512]{2,1,0:T(1,128)}, f32[4,128,512]{2,1,0:T(8,128)}) custom-call(bf16[4,128,512]{2,1,0:T(8,128)(2,1)} %copy-done.2, bf16[528,128]{1,0:T(8,128)(2,1)} %copy-done.18, bf16[528,128]{1,0:T(8,128)(2,1)} %copy-done.19, f32[4,1,512]{2,1,0:T(1,128)} %get-tuple-element.51.refs_3_, ...), custom_call_target="tpu_custom_call" | custom-call | flops 536870912 | bytes 2097152 | tf_op jit(solution)/shard_map/attend/pallas_call | solution.py:161
  191.6 4.7 %attend.17 = bf16[4,144,512]{2,1,0:T(8,128)(2,1)} custom-call(bf16[4,128,512]{2,1,0:T(8,128)(2,1)} %copy-done.2, bf16[528,128]{1,0:T(8,128)(2,1)} %copy-done.4, bf16[256,128]{1,0:T(8,128)(2,1)} %copy-done.5, f32[4,1,512]{2,1,0:T(1,128)} %get-tuple-element.54.refs_3_, f32[4,1,512]{2,1,0:T(1,128)} %get-tuple-element.55.refs_4_, ...), custom_call_target="tpu_custom_call" | custom-call | flops 402653184 | bytes 2097152 | tf_op jit(solution)/shard_map/attend/pallas_call | solution.py:161
  196.3 11.5 %all_to_all.32.parts = bf16[4,144,512]{2,1,0:T(8,128)(2,1)} all-to-all(bf16[4,144,512]{2,1,0:T(8,128)(2,1)} %attend.17), channel_id=1, replica_groups=mesh['z'=16,'y'=4,'tp'=8] {'y'}, dimensions={0} | all-to-all | bytes 1179648 | tf_op jit(solution)/shard_map/all_to_all | solution.py:295
  210.7 11.3 %all-to-all-start.5 = ((bf16[8,32,2048]{2,1,0:T(8,128)(2,1)}), bf16[8,32,2048]{2,1,0:T(8,128)(2,1)S(1)}, u32[]{:S(2)}, u32[]{:S(2)}) async-start(bf16[8,32,2048]{2,1,0:T(8,128)(2,1)} %bitcast.23), calls=%async_computation.5 | async-start | bytes 2097152 | tf_op jit(solution)/shard_map/all_to_all | solution.py:306
  222.0 15.0 %all-to-all-done.5 = bf16[8,32,2048]{2,1,0:T(8,128)(2,1)S(1)} async-done(((bf16[8,32,2048]{2,1,0:T(8,128)(2,1)}), bf16[8,32,2048]{2,1,0:T(8,128)(2,1)S(1)}, u32[]{:S(2)}, u32[]{:S(2)}) %all-to-all-start.5) | async-done | bytes 1048608 | tf_op jit(solution)/shard_map/all_to_all | solution.py:306
  (123 shorter events, 54.9 us)
Async XLA Ops:
  0.0 49.7 %copy-start.3 = (bf16[32,2048]{1,0:T(8,128)(2,1)S(1)}, bf16[32,2048]{1,0:T(8,128)(2,1)}, u32[]{:S(2)}) copy-start(bf16[32,2048]{1,0:T(8,128)(2,1)} %param.15) | copy-start | bytes 393220
  50.8 18.6 %all-to-all-start.2 = ((bf16[8,32,2048]{2,1,0:T(8,128)(2,1)}), bf16[8,32,2048]{2,1,0:T(8,128)(2,1)S(1)}, u32[]{:S(2)}, u32[]{:S(2)}) async-start(bf16[8,32,2048]{2,1,0:T(8,128)(2,1)} %broadcast_in_dim.88), calls=%async_computation.2 | async-start | bytes 2097152 | tf_op jit(solution)/shard_map/all_to_all | solution.py:23
  74.7 7.5 %collective-permute-start.8 = (bf16[528,128]{1,0:T(8,128)(2,1)}, bf16[528,128]{1,0:T(8,128)(2,1)S(1)}, u32[]{:S(2)}, u32[]{:S(2)}) collective-permute-start(bf16[528,128]{1,0:T(8,128)(2,1)} %get-tuple-element.32.refs_1_), channel_id=1, source_target_pairs={{480,0},{0,32},{32,64},{64,96},{96,128},{128,160},{160,192},{192,2... | collective-permute-start | bytes 405512 | tf_op jit(solution)/shard_map/ppermute | solution.py:281
  77.6 6.4 %collective-permute-start = (bf16[528,128]{1,0:T(8,128)(2,1)}, bf16[528,128]{1,0:T(8,128)(2,1)S(1)}, u32[]{:S(2)}, u32[]{:S(2)}) collective-permute-start(bf16[528,128]{1,0:T(8,128)(2,1)} %get-tuple-element.32.refs_1_), channel_id=1, source_target_pairs={{32,0},{64,32},{96,64},{128,96},{160,128},{192,160},{224,192},{256... | collective-permute-start | bytes 405512 | tf_op jit(solution)/shard_map/ppermute | solution.py:281
  82.1 37.6 %copy-start.8 = (bf16[528,128]{1,0:T(8,128)(2,1)}, bf16[528,128]{1,0:T(8,128)(2,1)S(1)}, u32[]{:S(2)}) copy-start(bf16[528,128]{1,0:T(8,128)(2,1)S(1)} %collective-permute-done.8.refs_2_) | copy-start | bytes 405508
  82.1 11.7 %collective-permute-start.9 = (bf16[528,128]{1,0:T(8,128)(2,1)S(1)}, bf16[528,128]{1,0:T(8,128)(2,1)S(1)}, u32[]{:S(2)}, u32[]{:S(2)}) collective-permute-start(bf16[528,128]{1,0:T(8,128)(2,1)S(1)} %collective-permute-done.8.refs_2_), channel_id=1, source_target_pairs={{480,0},{0,32},{32,64},{64,96},{96,128},{128,160},{160,192},{192,2... | collective-permute-start | bytes 405512 | tf_op jit(solution)/shard_map/ppermute | solution.py:281
  84.1 35.7 %copy-start.7 = (bf16[528,128]{1,0:T(8,128)(2,1)}, bf16[528,128]{1,0:T(8,128)(2,1)S(1)}, u32[]{:S(2)}) copy-start(bf16[528,128]{1,0:T(8,128)(2,1)S(1)} %collective-permute-done.refs_1_) | copy-start | bytes 405508
  84.1 11.7 %collective-permute-start.1 = (bf16[528,128]{1,0:T(8,128)(2,1)S(1)}, bf16[528,128]{1,0:T(8,128)(2,1)S(1)}, u32[]{:S(2)}, u32[]{:S(2)}) collective-permute-start(bf16[528,128]{1,0:T(8,128)(2,1)S(1)} %collective-permute-done.refs_1_), channel_id=1, source_target_pairs={{32,0},{64,32},{96,64},{128,96},{160,128},{192,160},{224,192},{256... | collective-permute-start | bytes 405512 | tf_op jit(solution)/shard_map/ppermute | solution.py:281
  90.4 24.2 %all-to-all-start.3 = ((bf16[4,128,512]{2,1,0:T(8,128)(2,1)}), bf16[4,128,512]{2,1,0:T(8,128)(2,1)S(1)}, u32[]{:S(2)}, u32[]{:S(2)}) async-start(bf16[4,128,512]{2,1,0:T(8,128)(2,1)} %broadcast_in_dim.97), calls=%async_computation.3 | async-start | bytes 1048576 | tf_op jit(solution)/shard_map/all_to_all | solution.py:23
  93.9 7.3 %collective-permute-start.10 = (bf16[528,128]{1,0:T(8,128)(2,1)S(1)}, bf16[528,128]{1,0:T(8,128)(2,1)S(1)}, u32[]{:S(2)}, u32[]{:S(2)}) collective-permute-start(bf16[528,128]{1,0:T(8,128)(2,1)S(1)} %collective-permute-done.9.refs_2_), channel_id=1, source_target_pairs={{480,0},{0,32},{32,64},{64,96},{96,128},{128,160},{160,192},{192,2... | collective-permute-start | bytes 405512 | tf_op jit(solution)/shard_map/ppermute | solution.py:281
  95.8 7.2 %collective-permute-start.2 = (bf16[528,128]{1,0:T(8,128)(2,1)S(1)}, bf16[528,128]{1,0:T(8,128)(2,1)S(1)}, u32[]{:S(2)}, u32[]{:S(2)}) collective-permute-start(bf16[528,128]{1,0:T(8,128)(2,1)S(1)} %collective-permute-done.1.refs_1_), channel_id=1, source_target_pairs={{32,0},{64,32},{96,64},{128,96},{160,128},{192,160},{224,192},{256... | collective-permute-start | bytes 405512 | tf_op jit(solution)/shard_map/ppermute | solution.py:281
  101.2 35.8 %copy-start.12 = (bf16[528,128]{1,0:T(8,128)(2,1)}, bf16[528,128]{1,0:T(8,128)(2,1)S(1)}, u32[]{:S(2)}) copy-start(bf16[528,128]{1,0:T(8,128)(2,1)S(1)} %collective-permute-done.10.refs_2_) | copy-start | bytes 405508
  101.2 7.0 %collective-permute-start.11 = (bf16[528,128]{1,0:T(8,128)(2,1)S(1)}, bf16[528,128]{1,0:T(8,128)(2,1)S(1)}, u32[]{:S(2)}, u32[]{:S(2)}) collective-permute-start(bf16[528,128]{1,0:T(8,128)(2,1)S(1)} %collective-permute-done.10.refs_2_), channel_id=1, source_target_pairs={{480,0},{0,32},{32,64},{64,96},{96,128},{128,160},{160,192},{192,2... | collective-permute-start | bytes 405512 | tf_op jit(solution)/shard_map/ppermute | solution.py:281
  103.1 33.9 %copy-start.11 = (bf16[528,128]{1,0:T(8,128)(2,1)}, bf16[528,128]{1,0:T(8,128)(2,1)S(1)}, u32[]{:S(2)}) copy-start(bf16[528,128]{1,0:T(8,128)(2,1)S(1)} %collective-permute-done.2.refs_1_) | copy-start | bytes 405508
  103.1 6.9 %collective-permute-start.3 = (bf16[528,128]{1,0:T(8,128)(2,1)S(1)}, bf16[528,128]{1,0:T(8,128)(2,1)S(1)}, u32[]{:S(2)}, u32[]{:S(2)}) collective-permute-start(bf16[528,128]{1,0:T(8,128)(2,1)S(1)} %collective-permute-done.2.refs_1_), channel_id=1, source_target_pairs={{32,0},{64,32},{96,64},{128,96},{160,128},{192,160},{224,192},{256... | collective-permute-start | bytes 405512 | tf_op jit(solution)/shard_map/ppermute | solution.py:281
  108.1 34.2 %copy-start.15 = (bf16[528,128]{1,0:T(8,128)(2,1)}, bf16[528,128]{1,0:T(8,128)(2,1)S(1)}, u32[]{:S(2)}) copy-start(bf16[528,128]{1,0:T(8,128)(2,1)S(1)} %collective-permute-done.11.refs_2_) | copy-start | bytes 405508
  108.1 11.6 %collective-permute-start.12 = (bf16[528,128]{1,0:T(8,128)(2,1)S(1)}, bf16[528,128]{1,0:T(8,128)(2,1)S(1)}, u32[]{:S(2)}, u32[]{:S(2)}) collective-permute-start(bf16[528,128]{1,0:T(8,128)(2,1)S(1)} %collective-permute-done.11.refs_2_), channel_id=1, source_target_pairs={{480,0},{0,32},{32,64},{64,96},{96,128},{128,160},{160,192},{192,2... | collective-permute-start | bytes 405512 | tf_op jit(solution)/shard_map/ppermute | solution.py:281
  110.0 22.3 %collective-permute-start.4 = (bf16[528,128]{1,0:T(8,128)(2,1)S(1)}, bf16[528,128]{1,0:T(8,128)(2,1)S(1)}, u32[]{:S(2)}, u32[]{:S(2)}) collective-permute-start(bf16[528,128]{1,0:T(8,128)(2,1)S(1)} %collective-permute-done.3.refs_1_), channel_id=1, source_target_pairs={{32,0},{64,32},{96,64},{128,96},{160,128},{192,160},{224,192},{256... | collective-permute-start | bytes 405512 | tf_op jit(solution)/shard_map/ppermute | solution.py:281
  119.8 22.5 %collective-permute-start.13 = (bf16[528,128]{1,0:T(8,128)(2,1)S(1)}, bf16[528,128]{1,0:T(8,128)(2,1)}, u32[]{:S(2)}, u32[]{:S(2)}) collective-permute-start(bf16[528,128]{1,0:T(8,128)(2,1)S(1)} %collective-permute-done.12.refs_2_), channel_id=1, source_target_pairs={{480,0},{0,32},{32,64},{64,96},{96,128},{128,160},{160,192},{192,2... | collective-permute-start | bytes 405512 | tf_op jit(solution)/shard_map/ppermute | solution.py:281
  132.3 22.5 %collective-permute-start.5 = (bf16[528,128]{1,0:T(8,128)(2,1)S(1)}, bf16[528,128]{1,0:T(8,128)(2,1)S(1)}, u32[]{:S(2)}, u32[]{:S(2)}) collective-permute-start(bf16[528,128]{1,0:T(8,128)(2,1)S(1)} %collective-permute-done.4.refs_1_), channel_id=1, source_target_pairs={{32,0},{64,32},{96,64},{128,96},{160,128},{192,160},{224,192},{256... | collective-permute-start | bytes 405512 | tf_op jit(solution)/shard_map/ppermute | solution.py:281
  142.3 22.4 %collective-permute-start.14 = (bf16[528,128]{1,0:T(8,128)(2,1)}, bf16[528,128]{1,0:T(8,128)(2,1)S(1)}, u32[]{:S(2)}, u32[]{:S(2)}) collective-permute-start(bf16[528,128]{1,0:T(8,128)(2,1)} %collective-permute-done.13.refs_2_), channel_id=1, source_target_pairs={{480,0},{0,32},{32,64},{64,96},{96,128},{128,160},{160,192},{192,2... | collective-permute-start | bytes 405512 | tf_op jit(solution)/shard_map/ppermute | solution.py:281
  154.8 18.7 %collective-permute-start.6 = (bf16[528,128]{1,0:T(8,128)(2,1)S(1)}, bf16[528,128]{1,0:T(8,128)(2,1)S(1)}, u32[]{:S(2)}, u32[]{:S(2)}) collective-permute-start(bf16[528,128]{1,0:T(8,128)(2,1)S(1)} %collective-permute-done.5.refs_1_), channel_id=1, source_target_pairs={{32,0},{64,32},{96,64},{128,96},{160,128},{192,160},{224,192},{256... | collective-permute-start | bytes 405512 | tf_op jit(solution)/shard_map/ppermute | solution.py:281
  173.5 7.3 %collective-permute-start.7 = (bf16[528,128]{1,0:T(8,128)(2,1)S(1)}, bf16[528,128]{1,0:T(8,128)(2,1)S(1)}, u32[]{:S(2)}, u32[]{:S(2)}) collective-permute-start(bf16[528,128]{1,0:T(8,128)(2,1)S(1)} %collective-permute-done.6.refs_1_), channel_id=1, source_target_pairs={{32,0},{64,32},{96,64},{128,96},{160,128},{192,160},{224,192},{256... | collective-permute-start | bytes 405512 | tf_op jit(solution)/shard_map/ppermute | solution.py:281
  210.7 26.3 %all-to-all-start.5 = ((bf16[8,32,2048]{2,1,0:T(8,128)(2,1)}), bf16[8,32,2048]{2,1,0:T(8,128)(2,1)S(1)}, u32[]{:S(2)}, u32[]{:S(2)}) async-start(bf16[8,32,2048]{2,1,0:T(8,128)(2,1)} %bitcast.23), calls=%async_computation.5 | async-start | bytes 2097152 | tf_op jit(solution)/shard_map/all_to_all | solution.py:306
  (14 other events, 172.2 us)

commit v2 on v1

v2 whole, which is shorter than its diff:
```python
import functools
import math

import jax
import jax.numpy as jnp
from jax import lax
from jax.experimental import pallas as pl
from jax.experimental.pallas import tpu as pltpu
from jax.sharding import Mesh
from jax.sharding import PartitionSpec as P

GRID_W = 64
LOG2E = math.log2(math.e)
TP = ("x", "c")
ALL = ("z", "y", *TP)
F32 = jnp.float32
BF16 = jnp.bfloat16


def from_everyone(value, axes):
    devices = lax.axis_size(axes)
    return lax.all_to_all(
        jnp.broadcast_to(value[None], (devices, *value.shape)), axes, 0, 0, tiled=True
    )


def rms_rows(values):
    return values * lax.rsqrt(jnp.mean(values * values, axis=-1, keepdims=True) + 1e-06)


def rms(values, gain):
    values = values.astype(F32)
    return rms_rows(values) * gain


def rotation_tables(positions, grid_width, head_dim):
    half = head_dim // 2
    quarter = head_dim // 4
    lane = jnp.arange(head_dim)
    j = (lane % quarter).astype(F32)
    freqs = 10000.0 ** (-(2.0 * j) / half)
    row_pos = (positions // grid_width).astype(F32)[:, None]
    col_pos = (positions % grid_width).astype(F32)[:, None]
    angle = jnp.where(lane[None] < half, row_pos, col_pos) * freqs[None]
    first = ((lane % half) < quarter)[None]
    sine = jnp.sin(angle)
    return (
        jnp.cos(angle),
        jnp.where(first, -sine, 0.0),
        jnp.where(first, 0.0, sine),
    )


def project_kernel(place, *refs):
    mine, other = refs[:4], refs[4]
    ctx, gain, mods, wq, wk, wv, qg, kg, cos, sa, sb, q_out, msg, lat = refs[5:]
    rows = lat.shape[0]
    part = mine[0].shape[0]
    for h in range(4):
        at = jax.lax.rem(place[0] + h, 4) * 2
        lat[pl.ds(pl.multiple_of((at + place[1]) * part, part), part)] = mine[h][...]
        lat[pl.ds(pl.multiple_of((at + 1 - place[1]) * part, part), part)] = other[
            h * part : (h + 1) * part
        ]
    ctx_rows = ctx.shape[0]
    head_dim = kg.shape[1]
    quarter = head_dim // 4
    g = gain[...]
    x = rms_rows(lat[...].astype(F32)) * g
    x = (x * (1.0 + mods[1:2]) + mods[0:1]).astype(BF16)
    c = rms_rows(ctx[...].astype(F32)) * g
    c = (c * (1.0 + mods[3:4]) + mods[2:3]).astype(BF16)

    def turned(v, gain_row):
        v = rms_rows(v) * gain_row
        up = pltpu.roll(v, head_dim - quarter, 1)
        down = pltpu.roll(v, quarter, 1)
        return v * cos[...] + up * sa[...] + down * sb[...]

    both = jnp.concatenate([x, c], axis=0)
    k = jnp.dot(both, wk[...], preferred_element_type=F32)
    v = jnp.dot(both, wv[...], preferred_element_type=F32)
    msg[0:rows] = turned(k[:rows], kg[...]).astype(BF16)
    msg[rows : 2 * rows] = v[:rows].astype(BF16)
    tail = jnp.concatenate([rms_rows(k[rows:]) * kg[...], v[rows:]], axis=0)
    msg[2 * rows : 2 * rows + 2 * ctx_rows] = tail.astype(BF16)
    q = jnp.dot(x, wq[...], preferred_element_type=F32)
    for h in range(q.shape[1] // head_dim):
        qh = turned(q[:, h * head_dim : (h + 1) * head_dim], qg[...])
        qt = jnp.transpose(qh).astype(BF16)
        for i in range(q_out.shape[0]):
            q_out[i, :, h * rows : (h + 1) * rows] = qt


def attend_kernel(*refs, counts, keys, extra, first, last, factor, lift):
    refs = list(refs)
    q = refs.pop(0)
    span = 2 * (keys + extra)
    blocks = []
    for count in counts:
        ref = refs.pop(0)
        blocks += [(ref, i * span) for i in range(count)]
    if not first:
        m_in, l_in, acc_in = refs.pop(0), refs.pop(0), refs.pop(0)
    tails = [ref[at + 2 * keys : at + span].astype(F32) for ref, at in blocks]
    ctx_key = jnp.concatenate([t[:extra] for t in tails], axis=0).astype(BF16)
    ctx_value = jnp.concatenate([t[extra:] for t in tails], axis=0).astype(BF16)

    def tile(i, unused):
        qv = q[i]
        scores = [
            jnp.dot(ref[at : at + keys], qv, preferred_element_type=F32) for ref, at in blocks
        ]
        largest = functools.reduce(
            jnp.maximum, [jnp.max(s, axis=0, keepdims=True) for s in scores]
        )
        ctx_scores = jnp.dot(ctx_key, qv, preferred_element_type=F32) * factor + lift
        largest = jnp.maximum(largest * factor, jnp.max(ctx_scores, axis=0, keepdims=True))
        if not first:
            largest = jnp.maximum(largest, m_in[i])
        terms = jnp.exp2(ctx_scores - largest)
        total = jnp.sum(terms, axis=0, keepdims=True)
        acc = weighted(ctx_value, terms)
        if not first:
            fade = jnp.exp2(m_in[i] - largest)
            total = total + l_in[i] * fade
            acc = acc + acc_in[i] * fade
        for s, (ref, at) in zip(scores, blocks):
            terms = jnp.exp2(s * factor - largest)
            total = total + jnp.sum(terms, axis=0, keepdims=True)
            acc = acc + weighted(ref[at + keys : at + 2 * keys], terms)
        if last:
            (out,) = refs
            dim = acc.shape[0]
            out[i, 0:dim] = (acc / total).astype(BF16)
            lse = largest + jnp.log2(total)
            hi = lse.astype(BF16).astype(F32)
            mid = (lse - hi).astype(BF16).astype(F32)
            low = lse - hi - mid
            row = lax.broadcasted_iota(jnp.int32, (16, lse.shape[1]), 0)
            packed = jnp.where(
                row == 0, hi, jnp.where(row == 1, mid, jnp.where(row == 2, low, 0.0))
            )
            out[i, dim : dim + 16] = packed.astype(BF16)
        else:
            m_out, l_out, acc_out = refs
            m_out[i] = largest
            l_out[i] = total
            acc_out[i] = acc
        return unused

    lax.fori_loop(0, q.shape[0], tile, 0)


def weighted(values, terms):
    return lax.dot_general(
        values, terms.astype(BF16), (((0,), (0,)), ((), ())), preferred_element_type=F32
    )


def attend(q_all, bundles, carry, last, keys, extra, factor, lift):
    parts, dim, width = q_all.shape
    first = carry is None
    counts = tuple(b.shape[0] // (2 * (keys + extra)) for b in bundles)
    operands = [q_all, *bundles] + ([] if first else list(carry))
    if last:
        out_shape = (jax.ShapeDtypeStruct((parts, dim + 16, width), BF16),)
    else:
        out_shape = (
            jax.ShapeDtypeStruct((parts, 1, width), F32),
            jax.ShapeDtypeStruct((parts, 1, width), F32),
            jax.ShapeDtypeStruct((parts, dim, width), F32),
        )
    whole = pl.BlockSpec(memory_space=pltpu.VMEM)
    all_keys = (keys + extra) * sum(counts)
    return pl.pallas_call(
        functools.partial(
            attend_kernel,
            counts=counts,
            keys=keys,
            extra=extra,
            first=first,
            last=last,
            factor=factor,
            lift=lift,
        ),
        in_specs=[whole] * len(operands),
        out_specs=tuple([whole] * len(out_shape)),
        out_shape=out_shape,
        cost_estimate=pl.CostEstimate(
            flops=4 * all_keys * parts * width * dim,
            bytes_accessed=2 * parts * width * dim * 4,
            transcendentals=all_keys * parts * width,
        ),
        name="attend",
    )(*operands)


def merge_kernel(parts, w_out, out):
    count, rows, width = parts.shape
    dim = rows - 16
    tail = [parts[i, dim : dim + 16].astype(F32) for i in range(count)]
    lse = [t[0:1] + t[1:2] + t[2:3] for t in tail]
    top = functools.reduce(jnp.maximum, lse)
    share = [jnp.exp2(v - top) for v in lse]
    whole = functools.reduce(jnp.add, share)
    merged = functools.reduce(
        jnp.add, [parts[i, 0:dim].astype(F32) * share[i] for i in range(count)]
    )
    merged = (merged / whole).astype(BF16)
    heads = w_out.shape[0] // dim
    rows = width // heads
    stacked = jnp.concatenate(
        [merged[:, h * rows : (h + 1) * rows] for h in range(heads)], axis=0
    )
    out[...] = lax.dot_general(
        stacked, w_out[...], (((0,), (0,)), ((), ())), preferred_element_type=F32
    ).astype(BF16)


def body(
    latent,
    condition,
    context_condition,
    context,
    w_shift,
    w_scale,
    w_gate,
    pre_gain,
    post_gain,
    query_gain,
    key_gain,
    w_query,
    w_key,
    w_value,
    w_out,
):
    tp_count = lax.axis_size(TP)
    y_count = lax.axis_size("y")
    model = latent.shape[1]
    head_dim = query_gain.shape[0]
    tok_dev = latent.shape[0] * tp_count
    ctx_dev = context.shape[0]
    heads_dev = w_query.shape[1] // head_dim
    factor = head_dim ** (-0.5) * LOG2E
    lift = math.log(tok_dev / (4.0 * ctx_dev)) * LOG2E

    def receive(value, axis, hop):
        size = lax.axis_size(axis)
        return lax.ppermute(value, axis, [((i + hop) % size, i) for i in range(size)])

    mine = [latent] + [receive(latent, "x", h) for h in (1, 2, 3)]
    other = receive(jnp.concatenate(mine, axis=0), "c", 1)

    conds = jax.nn.silu(jnp.stack([condition, context_condition]).astype(F32)).astype(BF16)
    shift_part, scale_part, gate_part = (
        jnp.dot(conds, weight, preferred_element_type=F32) for weight in (w_shift, w_scale, w_gate)
    )
    partial_mod = jnp.concatenate(
        [shift_part[0:1], scale_part[0:1], shift_part[1:2], scale_part[1:2], gate_part[0:1]], axis=0
    )
    partial_mod = from_everyone(partial_mod, "z")
    partial_mod = partial_mod.sum(axis=0)
    pieces = from_everyone(partial_mod, ("y", *TP))
    mods = pieces.reshape(y_count, tp_count, *partial_mod.shape).sum(axis=0)
    mods = mods.transpose(1, 0, 2).reshape(partial_mod.shape[0], model)

    positions = (lax.axis_index("z") * y_count + lax.axis_index("y")) * tok_dev + jnp.arange(tok_dev)
    cos, sa, sb = rotation_tables(positions, GRID_W, head_dim)
    msg_rows = 2 * tok_dev + 2 * ctx_dev
    whole = pl.BlockSpec(memory_space=pltpu.VMEM)
    place = jnp.stack([lax.axis_index("x"), lax.axis_index("c")]).astype(jnp.int32)
    query, message = pl.pallas_call(
        project_kernel,
        in_specs=[pl.BlockSpec(memory_space=pltpu.SMEM)] + [whole] * 16,
        out_specs=(whole, whole),
        scratch_shapes=[pltpu.VMEM((tok_dev, model), BF16)],
        out_shape=(
            jax.ShapeDtypeStruct((y_count, head_dim, heads_dev * tok_dev), BF16),
            jax.ShapeDtypeStruct((msg_rows, head_dim), BF16),
        ),
        cost_estimate=pl.CostEstimate(
            flops=2 * tok_dev * model * 4 * head_dim,
            bytes_accessed=2 * model * (4 * head_dim + tok_dev),
            transcendentals=0,
        ),
        name="project",
    )(
        place,
        *mine,
        other,
        context,
        pre_gain[None],
        mods[0:4],
        w_query,
        w_key,
        w_value,
        query_gain[None],
        key_gain[None],
        cos,
        sa,
        sb,
    )

    far_up, far_down = receive(message, "z", 5), receive(message, "z", -5)
    up, down = receive(message, "z", 1), receive(message, "z", -1)
    q_all = lax.all_to_all(query, "y", 0, 0, tiled=True)
    ups = receive(jnp.concatenate([up, far_up, far_down], axis=0), "z", 1)
    downs = receive(jnp.concatenate([down, far_down, far_up], axis=0), "z", -1)
    opposite = receive(far_up, "z", 3)
    last_ups = receive(ups[: 2 * msg_rows], "z", 1)
    last_downs = receive(downs[: 2 * msg_rows], "z", -1)
    shared = (tok_dev, ctx_dev, factor, lift)
    carry = attend(q_all, [message, up, down, far_up, far_down], None, False, *shared)
    carry = attend(q_all, [ups, downs], carry, False, *shared)
    (partials,) = attend(q_all, [opposite, last_ups, last_downs], carry, True, *shared)
    returned = lax.all_to_all(partials, "y", 0, 0, tiled=True)
    mixed = pl.pallas_call(
        merge_kernel,
        out_shape=jax.ShapeDtypeStruct((tok_dev, model), BF16),
        cost_estimate=pl.CostEstimate(
            flops=2 * tok_dev * model * heads_dev * head_dim,
            bytes_accessed=4 * tok_dev * model,
            transcendentals=0,
        ),
        name="merge",
    )(returned, w_out)
    arrived = lax.all_to_all(mixed.reshape(tp_count, -1, model), TP, 0, 0, tiled=True)
    mixed = arrived.astype(F32).sum(axis=0)
    updated = latent.astype(F32) + mods[4] * rms(mixed, post_gain)
    return updated.astype(BF16)


def solution(mesh):
    torus = Mesh(mesh.devices.reshape(16, 4, 4, 2), ALL)
    sp = ("z", "y")
    placed = (
        P(ALL, None),
        P(sp),
        P(sp),
        P(sp, None),
        P(sp, TP),
        P(sp, TP),
        P(sp, TP),
        P(),
        P(),
        P(),
        P(),
        P(None, TP),
        P(None, TP),
        P(None, TP),
        P(TP, None),
    )
    return jax.shard_map(body, mesh=torus, in_specs=placed, out_specs=P(ALL, None), check_vma=False)
```

time: 240 us -> 186 us (0.78)
  blocking collectives: 58.5 us -> 11.6 us
  Pallas kernels: 53.3 us -> 31.9 us
  starting transfers between devices: 65.7 us -> 86.4 us
  local copies, waits for them, and re-layouts: 25 us -> 4.55 us
  waiting for transfers between devices: 30.2 us -> 42.4 us
    all_to_all x2 -> x0, blocking collectives: 47 us -> none  [from_everyone(): lax.all_to_all(jnp.broadcast_to(value[None], (devices, *value.shape)), ax...]
    pallas_call x10 -> x4, Pallas kernels: 50.4 us -> 29 us  [the longest x3 24.4 us: attend(): pl.pallas_call(functools.partial(attend_kernel, counts=counts, keys=keys,...]
    unnamed x76 -> x39, local copies, waits for them, and re-layouts: 22.1 us -> 3.1 us
    all_to_all x2, starting transfers between devices: 7.07 us -> 25.2 us  [from_everyone(): lax.all_to_all(jnp.broadcast_to(value[None], (devices, *value.shape)), ax...]
    ppermute x15 -> x13, waiting for transfers between devices: 2.19 us -> 13.4 us  [receive(): lax.ppermute(value, axis, [((i + hop) % size, i) for i in range(size)])]
    ppermute x15 -> x13, starting transfers between devices: 47.3 us -> 48.8 us  [receive(): lax.ppermute(value, axis, [((i + hop) % size, i) for i in range(size)])]
    all_to_all x1 -> x2, starting transfers between devices: 11.3 us -> 12.4 us  [the longest x1 8.95 us: body(): lax.all_to_all(mixed.reshape(tp_count, -1, model), TP, 0, 0, tiled=True)]
    all_to_all x1 -> x2, waiting for transfers between devices: 15 us -> 15 us  [the longest x1 15 us: body(): lax.all_to_all(mixed.reshape(tp_count, -1, model), TP, 0, 0, tiled=True)]
  transfers between devices with their start and end apart: 18 -> 17, of which waited for: 5 -> 6; matrix products, arithmetic and copies ran while one was open for 5% -> 4% of each run, Pallas kernels for 17% -> 9%
where the time goes in v2:
time: 186 us; the launch traced here: 184 us
  starting transfers between devices  86.4 us (46%)
  waiting for transfers between devices  42.4 us (23%)
  Pallas kernels  31.9 us (17%)
  blocking collectives  11.6 us (6%)
  other arithmetic  4.93 us (3%)
  local copies, waits for them, and re-layouts  4.55 us (2%)
    ppermute x13, starting transfers between devices, receive(): lax.ppermute(value, axis, [((i + hop) % size, i) for i in range(size)])  48.8 us
    all_to_all x2, starting transfers between devices, from_everyone(): lax.all_to_all(jnp.broadcast_to(value[None], (devices, *value.shape)), ax...  25.2 us
    pallas_call x3, Pallas kernels, attend(): pl.pallas_call(functools.partial(attend_kernel, counts=counts, keys=keys,...  24.4 us
    all_to_all x1, waiting for transfers between devices, body(): lax.all_to_all(mixed.reshape(tp_count, -1, model), TP, 0, 0, tiled=True)  15 us
    all_to_all x2, waiting for transfers between devices, from_everyone(): lax.all_to_all(jnp.broadcast_to(value[None], (devices, *value.shape)), ax...  14 us
    ppermute x13, waiting for transfers between devices, receive(): lax.ppermute(value, axis, [((i + hop) % size, i) for i in range(size)])  13.4 us
    all_to_all x1, blocking collectives, body(): returned = lax.all_to_all(partials, 'y', 0, 0, tiled=True)  11.6 us
    all_to_all x1, starting transfers between devices, body(): lax.all_to_all(mixed.reshape(tp_count, -1, model), TP, 0, 0, tiled=True)  8.95 us
  transfers between devices with their start and end apart: 17, of which 6 were waited for; matrix products, arithmetic and copies ran while one was open for 4% of the time, Pallas kernels for 9%

profile of v2, /device:TPU:1, one launch (start us, length us, event | category | flops | bytes accessed | tf_op | source)
XLA Modules:
  0.0 183.9 jit_solution(8237924089362220578)
XLA Ops:
  0.0 5.3 %collective-permute-start = (bf16[32,2048]{1,0:T(8,128)(2,1)}, bf16[32,2048]{1,0:T(8,128)(2,1)S(1)}, u32[]{:S(2)}, u32[]{:S(2)}) collective-permute-start(bf16[32,2048]{1,0:T(8,128)(2,1)} %refs_0_.1), channel_id=1, source_target_pairs={{2,0},{4,2},{6,4},{0,6},{3,1},{5,3},{7,5},{1,7},{10,8},{12,10},{14... | collective-permute-start | bytes 393224 | tf_op jit(solution)/shard_map/ppermute | solution.py:250
  13.5 14.9 %all-to-all-start = ((f32[16,5,256]{2,1,0:T(8,128)}), f32[16,5,256]{2,1,0:T(8,128)S(1)}, u32[]{:S(2)}, u32[]{:S(2)}) async-start(f32[16,5,256]{2,1,0:T(8,128)} %broadcast_in_dim.74), calls=%async_computation | async-start | bytes 262144 | tf_op jit(solution)/shard_map/all_to_all | solution.py:22
  29.6 3.7 %collective-permute-start.3 = (bf16[128,2048]{1,0:T(8,128)(2,1)S(1)}, bf16[128,2048]{1,0:T(8,128)(2,1)S(1)}, u32[]{:S(2)}, u32[]{:S(2)}) collective-permute-start(bf16[128,2048]{1,0:T(8,128)(2,1)S(1)} %pad_maximum_fusion), channel_id=1, source_target_pairs={{1,0},{0,1},{3,2},{2,3},{5,4},{4,5},{7,6},{6,7},{9,8},{8,9},{11,10... | collective-permute-start | bytes 1572872 | tf_op jit(solution)/shard_map/ppermute | solution.py:250
  33.3 7.1 %all-to-all-done = f32[16,5,256]{2,1,0:T(8,128)S(1)} async-done(((f32[16,5,256]{2,1,0:T(8,128)}), f32[16,5,256]{2,1,0:T(8,128)S(1)}, u32[]{:S(2)}, u32[]{:S(2)}) %all-to-all-start) | async-done | bytes 81952 | tf_op jit(solution)/shard_map/all_to_all | solution.py:22
  41.1 10.3 %all-to-all-start.1 = ((f32[32,5,256]{2,1,0:T(8,128)}), f32[32,5,256]{2,1,0:T(8,128)S(1)}, u32[]{:S(2)}, u32[]{:S(2)}) async-start(f32[32,5,256]{2,1,0:T(8,128)} %broadcast_in_dim.75), calls=%async_computation.1 | async-start | bytes 524288 | tf_op jit(solution)/shard_map/all_to_all | solution.py:22
  53.4 6.9 %all-to-all-done.1 = f32[32,5,256]{2,1,0:T(8,128)S(1)} async-done(((f32[32,5,256]{2,1,0:T(8,128)}), f32[32,5,256]{2,1,0:T(8,128)S(1)}, u32[]{:S(2)}, u32[]{:S(2)}) %all-to-all-start.1) | async-done | bytes 163872 | tf_op jit(solution)/shard_map/all_to_all | solution.py:22
  61.8 4.6 %project.1 = (bf16[4,128,512]{2,1,0:T(8,128)(2,1)}, bf16[528,128]{1,0:T(8,128)(2,1)}) custom-call(s32[2]{0:T(128)} %pad_add_fusion.place, bf16[32,2048]{1,0:T(8,128)(2,1)} %refs_0_.1, bf16[32,2048]{1,0:T(8,128)(2,1)} %copy-done.4, bf16[32,2048]{1,0:T(8,128)(2,1)} %copy-done.5, bf16[32,2048]{1,0:T(8,128)(2,1)} %copy-done.6, bf16[128,2048]{1,0:T(8,128)(2,1)} %copy-done.3, ...), custom_call_target="tpu_custom_call" | custom-call | flops 536870912 | bytes 3145728 | tf_op jit(solution)/shard_map/project/pallas_call | solution.py:273
  66.3 3.5 %collective-permute-start.4 = (bf16[528,128]{1,0:T(8,128)(2,1)}, bf16[528,128]{1,0:T(8,128)(2,1)S(1)}, u32[]{:S(2)}, u32[]{:S(2)}) collective-permute-start(bf16[528,128]{1,0:T(8,128)(2,1)} %get-tuple-element.14.refs_1_), channel_id=1, source_target_pairs={{160,0},{192,32},{224,64},{256,96},{288,128},{320,160},{352,192},{... | collective-permute-start | bytes 405512 | tf_op jit(solution)/shard_map/ppermute | solution.py:250
  69.8 2.7 %collective-permute-start.10 = (bf16[528,128]{1,0:T(8,128)(2,1)}, bf16[528,128]{1,0:T(8,128)(2,1)S(1)}, u32[]{:S(2)}, u32[]{:S(2)}) collective-permute-start(bf16[528,128]{1,0:T(8,128)(2,1)} %get-tuple-element.14.refs_1_), channel_id=1, source_target_pairs={{480,0},{0,32},{32,64},{64,96},{96,128},{128,160},{160,192},{192,2... | collective-permute-start | bytes 405512 | tf_op jit(solution)/shard_map/ppermute | solution.py:250
  72.5 3.8 %collective-permute-start.6 = (bf16[528,128]{1,0:T(8,128)(2,1)}, bf16[528,128]{1,0:T(8,128)(2,1)S(1)}, u32[]{:S(2)}, u32[]{:S(2)}) collective-permute-start(bf16[528,128]{1,0:T(8,128)(2,1)} %get-tuple-element.14.refs_1_), channel_id=1, source_target_pairs={{32,0},{64,32},{96,64},{128,96},{160,128},{192,160},{224,192},{256... | collective-permute-start | bytes 405512 | tf_op jit(solution)/shard_map/ppermute | solution.py:250
  76.4 5.8 %collective-permute-start.7 = (bf16[528,128]{1,0:T(8,128)(2,1)}, bf16[528,128]{1,0:T(8,128)(2,1)S(1)}, u32[]{:S(2)}, u32[]{:S(2)}) collective-permute-start(bf16[528,128]{1,0:T(8,128)(2,1)} %get-tuple-element.14.refs_1_), channel_id=1, source_target_pairs={{352,0},{384,32},{416,64},{448,96},{480,128},{0,160},{32,192},{64,... | collective-permute-start | bytes 405512 | tf_op jit(solution)/shard_map/ppermute | solution.py:250
  82.1 6.4 %collective-permute-done.4.refs_4_ = bf16[528,128]{1,0:T(8,128)(2,1)S(1)} collective-permute-done((bf16[528,128]{1,0:T(8,128)(2,1)}, bf16[528,128]{1,0:T(8,128)(2,1)S(1)}, u32[]{:S(2)}, u32[]{:S(2)}) %collective-permute-start.4) | collective-permute-done | bytes 135200 | tf_op jit(solution)/shard_map/ppermute | solution.py:250
  88.5 6.7 %collective-permute-done.7.refs_5_ = bf16[528,128]{1,0:T(8,128)(2,1)S(1)} collective-permute-done((bf16[528,128]{1,0:T(8,128)(2,1)}, bf16[528,128]{1,0:T(8,128)(2,1)S(1)}, u32[]{:S(2)}, u32[]{:S(2)}) %collective-permute-start.7) | collective-permute-done | bytes 135200 | tf_op jit(solution)/shard_map/ppermute | solution.py:250
  95.3 6.4 %collective-permute-start.11 = (bf16[1584,128]{1,0:T(8,128)(2,1)S(1)}, bf16[1584,128]{1,0:T(8,128)(2,1)S(1)}, u32[]{:S(2)}, u32[]{:S(2)}) collective-permute-start(bf16[1584,128]{1,0:T(8,128)(2,1)S(1)} %get-tuple-element.21), channel_id=1, source_target_pairs={{480,0},{0,32},{32,64},{64,96},{96,128},{128,160},{160,192},{192,2... | collective-permute-start | bytes 1216520 | tf_op jit(solution)/shard_map/ppermute | solution.py:250
  103.7 3.5 %all-to-all-start.2 = ((bf16[4,128,512]{2,1,0:T(8,128)(2,1)}), bf16[4,128,512]{2,1,0:T(8,128)(2,1)S(1)}, u32[]{:S(2)}, u32[]{:S(2)}) async-start(bf16[4,128,512]{2,1,0:T(8,128)(2,1)} %get-tuple-element.13), calls=%async_computation.2 | async-start | bytes 1048576 | tf_op jit(solution)/shard_map/all_to_all | solution.py:307
  107.2 4.5 %collective-permute-start.5 = (bf16[528,128]{1,0:T(8,128)(2,1)S(1)}, bf16[528,128]{1,0:T(8,128)(2,1)S(1)}, u32[]{:S(2)}, u32[]{:S(2)}) collective-permute-start(bf16[528,128]{1,0:T(8,128)(2,1)S(1)} %collective-permute-done.4.refs_4_), channel_id=1, source_target_pairs={{96,0},{128,32},{160,64},{192,96},{224,128},{256,160},{288,192},{3... | collective-permute-start | bytes 405512 | tf_op jit(solution)/shard_map/ppermute | solution.py:250
  114.2 4.1 %collective-permute-start.9 = (bf16[1056,128]{1,0:T(8,128)(2,1)S(1)}, bf16[1056,128]{1,0:T(8,128)(2,1)S(1)}, u32[]{:S(2)}, u32[]{:S(2)}) collective-permute-start(bf16[1056,128]{1,0:T(8,128)(2,1)S(1)} %slice.49), channel_id=1, source_target_pairs={{32,0},{64,32},{96,64},{128,96},{160,128},{192,160},{224,192},{256... | collective-permute-start | bytes 811016 | tf_op jit(solution)/shard_map/ppermute | solution.py:250
  119.1 7.4 %attend.3 = (f32[4,1,512]{2,1,0:T(1,128)}, f32[4,1,512]{2,1,0:T(1,128)}, f32[4,128,512]{2,1,0:T(8,128)}) custom-call(bf16[4,128,512]{2,1,0:T(8,128)(2,1)} %copy-done.2, bf16[528,128]{1,0:T(8,128)(2,1)} %get-tuple-element.14.refs_1_, bf16[528,128]{1,0:T(8,128)(2,1)} %copy-done.11, bf16[528,128]{1,0:T(8,128)(2,1)} %copy-done.10, bf16[528,128]{1,0:T(8,128)(2,1)} %copy-done.9, ...), custom_call_target="tpu_custom_call" | custom-call | flops 1384120320 | bytes 2097152 | tf_op jit(solution)/shard_map/attend/pallas_call | solution.py:176
  126.5 9.0 %attend.4 = (f32[4,1,512]{2,1,0:T(1,128)}, f32[4,1,512]{2,1,0:T(1,128)}, f32[4,128,512]{2,1,0:T(8,128)}) custom-call(bf16[4,128,512]{2,1,0:T(8,128)(2,1)} %copy-done.2, bf16[1584,128]{1,0:T(8,128)(2,1)} %copy-done.8, bf16[1584,128]{1,0:T(8,128)(2,1)} %copy-done.7, f32[4,1,512]{2,1,0:T(1,128)} %get-tuple-element.15.refs_3_, ...), custom_call_target="tpu_custom_call" | custom-call | flops 1660944384 | bytes 2097152 | tf_op jit(solution)/shard_map/attend/pallas_call | solution.py:176
  136.4 8.0 %attend.5 = bf16[4,144,512]{2,1,0:T(8,128)(2,1)} custom-call(bf16[4,128,512]{2,1,0:T(8,128)(2,1)} %copy-done.2, bf16[528,128]{1,0:T(8,128)(2,1)} %copy-done.16, bf16[1056,128]{1,0:T(8,128)(2,1)} %copy-done.15, bf16[1056,128]{1,0:T(8,128)(2,1)} %copy-done.14, f32[4,1,512]{2,1,0:T(1,128)} %get-tuple-element.18.refs_4_, ...), custom_call_target="tpu_custom_call" | custom-call | flops 1384120320 | bytes 2097152 | tf_op jit(solution)/shard_map/attend/pallas_call | solution.py:176
  144.4 11.6 %all_to_all.25.parts = bf16[4,144,512]{2,1,0:T(8,128)(2,1)} all-to-all(bf16[4,144,512]{2,1,0:T(8,128)(2,1)} %attend.5), channel_id=1, replica_groups=mesh['z'=16,'y'=4,'x'=4,'c'=2] {'y'}, dimensions={0} | all-to-all | bytes 1179648 | tf_op jit(solution)/shard_map/all_to_all | solution.py:317
  156.0 3.0 %merge.1 = bf16[256,2048]{1,0:T(8,128)(2,1)} custom-call(bf16[4,144,512]{2,1,0:T(8,128)(2,1)} %all_to_all.25.parts, bf16[256,2048]{1,0:T(8,128)(2,1)} %w_out.1), custom_call_target="tpu_custom_call" | custom-call | flops 268435456 | bytes 2097152 | tf_op jit(solution)/shard_map/merge/pallas_call | solution.py:318
  158.9 9.0 %all-to-all-start.4 = ((bf16[8,32,2048]{2,1,0:T(8,128)(2,1)}), bf16[8,32,2048]{2,1,0:T(8,128)(2,1)S(1)}, u32[]{:S(2)}, u32[]{:S(2)}) async-start(bf16[8,32,2048]{2,1,0:T(8,128)(2,1)} %bitcast.23), calls=%async_computation.4 | async-start | bytes 2097152 | tf_op jit(solution)/shard_map/all_to_all | solution.py:328
  167.9 15.0 %all-to-all-done.4 = bf16[8,32,2048]{2,1,0:T(8,128)(2,1)S(1)} async-done(((bf16[8,32,2048]{2,1,0:T(8,128)(2,1)}), bf16[8,32,2048]{2,1,0:T(8,128)(2,1)S(1)}, u32[]{:S(2)}, u32[]{:S(2)}) %all-to-all-start.4) | async-done | bytes 1048608 | tf_op jit(solution)/shard_map/all_to_all | solution.py:328
  (78 shorter events, 20.6 us)
Async XLA Ops:
  0.0 28.5 %collective-permute-start = (bf16[32,2048]{1,0:T(8,128)(2,1)}, bf16[32,2048]{1,0:T(8,128)(2,1)S(1)}, u32[]{:S(2)}, u32[]{:S(2)}) collective-permute-start(bf16[32,2048]{1,0:T(8,128)(2,1)} %refs_0_.1), channel_id=1, source_target_pairs={{2,0},{4,2},{6,4},{0,6},{3,1},{5,3},{7,5},{1,7},{10,8},{12,10},{14... | collective-permute-start | bytes 393224 | tf_op jit(solution)/shard_map/ppermute | solution.py:250
  5.3 23.1 %collective-permute-start.1 = (bf16[32,2048]{1,0:T(8,128)(2,1)}, bf16[32,2048]{1,0:T(8,128)(2,1)S(1)}, u32[]{:S(2)}, u32[]{:S(2)}) collective-permute-start(bf16[32,2048]{1,0:T(8,128)(2,1)} %refs_0_.1), channel_id=1, source_target_pairs={{4,0},{6,2},{0,4},{2,6},{5,1},{7,3},{1,5},{3,7},{12,8},{14,10},{8,... | collective-permute-start | bytes 393224 | tf_op jit(solution)/shard_map/ppermute | solution.py:250
  7.8 20.7 %collective-permute-start.2 = (bf16[32,2048]{1,0:T(8,128)(2,1)}, bf16[32,2048]{1,0:T(8,128)(2,1)S(1)}, u32[]{:S(2)}, u32[]{:S(2)}) collective-permute-start(bf16[32,2048]{1,0:T(8,128)(2,1)} %refs_0_.1), channel_id=1, source_target_pairs={{6,0},{0,2},{2,4},{4,6},{7,1},{1,3},{3,5},{5,7},{14,8},{8,10},{10,... | collective-permute-start | bytes 393224 | tf_op jit(solution)/shard_map/ppermute | solution.py:250
  13.5 26.9 %all-to-all-start = ((f32[16,5,256]{2,1,0:T(8,128)}), f32[16,5,256]{2,1,0:T(8,128)S(1)}, u32[]{:S(2)}, u32[]{:S(2)}) async-start(f32[16,5,256]{2,1,0:T(8,128)} %broadcast_in_dim.74), calls=%async_computation | async-start | bytes 262144 | tf_op jit(solution)/shard_map/all_to_all | solution.py:22
  28.5 24.3 %copy-start.4 = (bf16[32,2048]{1,0:T(8,128)(2,1)}, bf16[32,2048]{1,0:T(8,128)(2,1)S(1)}, u32[]{:S(2)}) copy-start(bf16[32,2048]{1,0:T(8,128)(2,1)S(1)} %collective-permute-done.refs_1_) | copy-start | bytes 393220
  28.5 24.3 %copy-start.5 = (bf16[32,2048]{1,0:T(8,128)(2,1)}, bf16[32,2048]{1,0:T(8,128)(2,1)S(1)}, u32[]{:S(2)}) copy-start(bf16[32,2048]{1,0:T(8,128)(2,1)S(1)} %collective-permute-done.1.refs_2_) | copy-start | bytes 393220
  28.5 24.2 %copy-start.6 = (bf16[32,2048]{1,0:T(8,128)(2,1)}, bf16[32,2048]{1,0:T(8,128)(2,1)S(1)}, u32[]{:S(2)}) copy-start(bf16[32,2048]{1,0:T(8,128)(2,1)S(1)} %collective-permute-done.2.refs_3_) | copy-start | bytes 393220
  29.6 31.4 %collective-permute-start.3 = (bf16[128,2048]{1,0:T(8,128)(2,1)S(1)}, bf16[128,2048]{1,0:T(8,128)(2,1)S(1)}, u32[]{:S(2)}, u32[]{:S(2)}) collective-permute-start(bf16[128,2048]{1,0:T(8,128)(2,1)S(1)} %pad_maximum_fusion), channel_id=1, source_target_pairs={{1,0},{0,1},{3,2},{2,3},{5,4},{4,5},{7,6},{6,7},{9,8},{8,9},{11,10... | collective-permute-start | bytes 1572872 | tf_op jit(solution)/shard_map/ppermute | solution.py:250
  41.1 19.2 %all-to-all-start.1 = ((f32[32,5,256]{2,1,0:T(8,128)}), f32[32,5,256]{2,1,0:T(8,128)S(1)}, u32[]{:S(2)}, u32[]{:S(2)}) async-start(f32[32,5,256]{2,1,0:T(8,128)} %broadcast_in_dim.75), calls=%async_computation.1 | async-start | bytes 524288 | tf_op jit(solution)/shard_map/all_to_all | solution.py:22
  66.3 22.2 %collective-permute-start.4 = (bf16[528,128]{1,0:T(8,128)(2,1)}, bf16[528,128]{1,0:T(8,128)(2,1)S(1)}, u32[]{:S(2)}, u32[]{:S(2)}) collective-permute-start(bf16[528,128]{1,0:T(8,128)(2,1)} %get-tuple-element.14.refs_1_), channel_id=1, source_target_pairs={{160,0},{192,32},{224,64},{256,96},{288,128},{320,160},{352,192},{... | collective-permute-start | bytes 405512 | tf_op jit(solution)/shard_map/ppermute | solution.py:250
  69.8 18.7 %collective-permute-start.10 = (bf16[528,128]{1,0:T(8,128)(2,1)}, bf16[528,128]{1,0:T(8,128)(2,1)S(1)}, u32[]{:S(2)}, u32[]{:S(2)}) collective-permute-start(bf16[528,128]{1,0:T(8,128)(2,1)} %get-tuple-element.14.refs_1_), channel_id=1, source_target_pairs={{480,0},{0,32},{32,64},{64,96},{96,128},{128,160},{160,192},{192,2... | collective-permute-start | bytes 405512 | tf_op jit(solution)/shard_map/ppermute | solution.py:250
  72.5 16.0 %collective-permute-start.6 = (bf16[528,128]{1,0:T(8,128)(2,1)}, bf16[528,128]{1,0:T(8,128)(2,1)S(1)}, u32[]{:S(2)}, u32[]{:S(2)}) collective-permute-start(bf16[528,128]{1,0:T(8,128)(2,1)} %get-tuple-element.14.refs_1_), channel_id=1, source_target_pairs={{32,0},{64,32},{96,64},{128,96},{160,128},{192,160},{224,192},{256... | collective-permute-start | bytes 405512 | tf_op jit(solution)/shard_map/ppermute | solution.py:250
  76.4 18.9 %collective-permute-start.7 = (bf16[528,128]{1,0:T(8,128)(2,1)}, bf16[528,128]{1,0:T(8,128)(2,1)S(1)}, u32[]{:S(2)}, u32[]{:S(2)}) collective-permute-start(bf16[528,128]{1,0:T(8,128)(2,1)} %get-tuple-element.14.refs_1_), channel_id=1, source_target_pairs={{352,0},{384,32},{416,64},{448,96},{480,128},{0,160},{32,192},{64,... | collective-permute-start | bytes 405512 | tf_op jit(solution)/shard_map/ppermute | solution.py:250
  88.5 18.7 %copy-start.9 = (bf16[528,128]{1,0:T(8,128)(2,1)}, bf16[528,128]{1,0:T(8,128)(2,1)S(1)}, u32[]{:S(2)}) copy-start(bf16[528,128]{1,0:T(8,128)(2,1)S(1)} %collective-permute-done.4.refs_4_) | copy-start | bytes 405508
  88.5 15.2 %copy-start.11 = (bf16[528,128]{1,0:T(8,128)(2,1)}, bf16[528,128]{1,0:T(8,128)(2,1)S(1)}, u32[]{:S(2)}) copy-start(bf16[528,128]{1,0:T(8,128)(2,1)S(1)} %collective-permute-done.6.refs_2_) | copy-start | bytes 405508
  95.3 16.4 %collective-permute-start.11 = (bf16[1584,128]{1,0:T(8,128)(2,1)S(1)}, bf16[1584,128]{1,0:T(8,128)(2,1)S(1)}, u32[]{:S(2)}, u32[]{:S(2)}) collective-permute-start(bf16[1584,128]{1,0:T(8,128)(2,1)S(1)} %get-tuple-element.21), channel_id=1, source_target_pairs={{480,0},{0,32},{32,64},{64,96},{96,128},{128,160},{160,192},{192,2... | collective-permute-start | bytes 1216520 | tf_op jit(solution)/shard_map/ppermute | solution.py:250
  101.8 12.4 %collective-permute-start.8 = (bf16[1584,128]{1,0:T(8,128)(2,1)S(1)}, bf16[1584,128]{1,0:T(8,128)(2,1)S(1)}, u32[]{:S(2)}, u32[]{:S(2)}) collective-permute-start(bf16[1584,128]{1,0:T(8,128)(2,1)S(1)} %get-tuple-element.22), channel_id=1, source_target_pairs={{32,0},{64,32},{96,64},{128,96},{160,128},{192,160},{224,192},{256... | collective-permute-start | bytes 1216520 | tf_op jit(solution)/shard_map/ppermute | solution.py:250
  103.7 14.6 %all-to-all-start.2 = ((bf16[4,128,512]{2,1,0:T(8,128)(2,1)}), bf16[4,128,512]{2,1,0:T(8,128)(2,1)S(1)}, u32[]{:S(2)}, u32[]{:S(2)}) async-start(bf16[4,128,512]{2,1,0:T(8,128)(2,1)} %get-tuple-element.13), calls=%async_computation.2 | async-start | bytes 1048576 | tf_op jit(solution)/shard_map/all_to_all | solution.py:307
  107.2 28.3 %collective-permute-start.5 = (bf16[528,128]{1,0:T(8,128)(2,1)S(1)}, bf16[528,128]{1,0:T(8,128)(2,1)S(1)}, u32[]{:S(2)}, u32[]{:S(2)}) collective-permute-start(bf16[528,128]{1,0:T(8,128)(2,1)S(1)} %collective-permute-done.4.refs_4_), channel_id=1, source_target_pairs={{96,0},{128,32},{160,64},{192,96},{224,128},{256,160},{288,192},{3... | collective-permute-start | bytes 405512 | tf_op jit(solution)/shard_map/ppermute | solution.py:250
  111.8 23.8 %collective-permute-start.12 = (bf16[1056,128]{1,0:T(8,128)(2,1)S(1)}, bf16[1056,128]{1,0:T(8,128)(2,1)S(1)}, u32[]{:S(2)}, u32[]{:S(2)}) collective-permute-start(bf16[1056,128]{1,0:T(8,128)(2,1)S(1)} %slice.50), channel_id=1, source_target_pairs={{480,0},{0,32},{32,64},{64,96},{96,128},{128,160},{160,192},{192,2... | collective-permute-start | bytes 811016 | tf_op jit(solution)/shard_map/ppermute | solution.py:250
  114.2 21.3 %collective-permute-start.9 = (bf16[1056,128]{1,0:T(8,128)(2,1)S(1)}, bf16[1056,128]{1,0:T(8,128)(2,1)S(1)}, u32[]{:S(2)}, u32[]{:S(2)}) collective-permute-start(bf16[1056,128]{1,0:T(8,128)(2,1)S(1)} %slice.49), channel_id=1, source_target_pairs={{32,0},{64,32},{96,64},{128,96},{160,128},{192,160},{224,192},{256... | collective-permute-start | bytes 811016 | tf_op jit(solution)/shard_map/ppermute | solution.py:250
  158.9 24.0 %all-to-all-start.4 = ((bf16[8,32,2048]{2,1,0:T(8,128)(2,1)}), bf16[8,32,2048]{2,1,0:T(8,128)(2,1)S(1)}, u32[]{:S(2)}, u32[]{:S(2)}) async-start(bf16[8,32,2048]{2,1,0:T(8,128)(2,1)} %bitcast.23), calls=%async_computation.4 | async-start | bytes 2097152 | tf_op jit(solution)/shard_map/all_to_all | solution.py:328
  167.9 15.3 %copy-start.1 = (bf16[32,2048]{1,0:T(8,128)(2,1)S(1)}, bf16[32,2048]{1,0:T(8,128)(2,1)}, u32[]{:S(2)}) copy-start(bf16[32,2048]{1,0:T(8,128)(2,1)} %refs_0_.1) | copy-start | bytes 393220
  167.9 15.3 %copy-start.13 = (f32[2048]{0:T(1024)S(1)}, f32[2048]{0:T(1024)}, u32[]{:S(2)}) copy-start(f32[2048]{0:T(1024)} %param.23) | copy-start | bytes 24580
  (10 other events, 65.6 us)

commit v3 on v2

--- a/solution.py
+++ b/solution.py
@@ -15,6 +15,14 @@
 ALL = ("z", "y", *TP)
 F32 = jnp.float32
 BF16 = jnp.bfloat16
+
+
+def room(mebibytes):
+    return pltpu.CompilerParams(vmem_limit_bytes=mebibytes << 20)
+
+
+def near(*arrays):
+    return [pltpu.with_memory_space_constraint(a, pltpu.VMEM) for a in arrays]
 
 
 def from_everyone(value, axes):
@@ -51,9 +59,29 @@
     )
 
 
+def modulation_kernel(cond, ctx_cond, w_shift, w_scale, w_gate, out):
+    both = jnp.concatenate([cond[...].astype(F32), ctx_cond[...].astype(F32)], axis=0)
+    both = jax.nn.silu(both).astype(BF16)
+    shift, scale, gate = (
+        jnp.dot(both, w[...], preferred_element_type=F32) for w in (w_shift, w_scale, w_gate)
+    )
+    rows = jnp.concatenate([shift[0:1], scale[0:1], shift[1:2], scale[1:2], gate[0:1]], axis=0)
+    for i in range(out.shape[0]):
+        out[i] = rows
+
+
+def turned(v, gain_row, cos, sa, sb):
+    head_dim = v.shape[1]
+    quarter = head_dim // 4
+    v = rms_rows(v) * gain_row
+    up = pltpu.roll(v, head_dim - quarter, 1)
+    down = pltpu.roll(v, quarter, 1)
+    return v * cos[...] + up * sa[...] + down * sb[...]
+
+
 def project_kernel(place, *refs):
     mine, other = refs[:4], refs[4]
-    ctx, gain, mods, wq, wk, wv, qg, kg, cos, sa, sb, q_out, msg, lat = refs[5:]
+    pieces, ctx, gain, wk, wv, kg, cos, sa, sb, msg, normed, gate, lat = refs[5:]
     rows = lat.shape[0]
     part = mine[0].shape[0]
     for h in range(4):
@@ -62,31 +90,39 @@
         lat[pl.ds(pl.multiple_of((at + 1 - place[1]) * part, part), part)] = other[
             h * part : (h + 1) * part
         ]
+    slots = 2 * 4
+    mods = jnp.concatenate(
+        [
+            functools.reduce(
+                jnp.add, [pieces[y * slots + t] for y in range(pieces.shape[0] // slots)]
+            )
+            for t in range(slots)
+        ],
+        axis=1,
+    )
+    gate[...] = mods[4:5]
     ctx_rows = ctx.shape[0]
-    head_dim = kg.shape[1]
-    quarter = head_dim // 4
     g = gain[...]
     x = rms_rows(lat[...].astype(F32)) * g
     x = (x * (1.0 + mods[1:2]) + mods[0:1]).astype(BF16)
+    normed[...] = x
     c = rms_rows(ctx[...].astype(F32)) * g
     c = (c * (1.0 + mods[3:4]) + mods[2:3]).astype(BF16)
-
-    def turned(v, gain_row):
-        v = rms_rows(v) * gain_row
-        up = pltpu.roll(v, head_dim - quarter, 1)
-        down = pltpu.roll(v, quarter, 1)
-        return v * cos[...] + up * sa[...] + down * sb[...]
-
     both = jnp.concatenate([x, c], axis=0)
     k = jnp.dot(both, wk[...], preferred_element_type=F32)
     v = jnp.dot(both, wv[...], preferred_element_type=F32)
-    msg[0:rows] = turned(k[:rows], kg[...]).astype(BF16)
+    msg[0:rows] = turned(k[:rows], kg[...], cos, sa, sb).astype(BF16)
     msg[rows : 2 * rows] = v[:rows].astype(BF16)
     tail = jnp.concatenate([rms_rows(k[rows:]) * kg[...], v[rows:]], axis=0)
     msg[2 * rows : 2 * rows + 2 * ctx_rows] = tail.astype(BF16)
-    q = jnp.dot(x, wq[...], preferred_element_type=F32)
+
+
+def query_kernel(normed, wq, qg, cos, sa, sb, q_out):
+    rows = normed.shape[0]
+    head_dim = qg.shape[1]
+    q = jnp.dot(normed[...], wq[...], preferred_element_type=F32)
     for h in range(q.shape[1] // head_dim):
-        qh = turned(q[:, h * head_dim : (h + 1) * head_dim], qg[...])
+        qh = turned(q[:, h * head_dim : (h + 1) * head_dim], qg[...], cos, sa, sb)
         qt = jnp.transpose(qh).astype(BF16)
         for i in range(q_out.shape[0]):
             q_out[i, :, h * rows : (h + 1) * rows] = qt
@@ -106,8 +142,14 @@
     ctx_key = jnp.concatenate([t[:extra] for t in tails], axis=0).astype(BF16)
     ctx_value = jnp.concatenate([t[extra:] for t in tails], axis=0).astype(BF16)
 
+    wide = 2
+    width = q.shape[2]
+
+    def both(ref, i):
+        return jnp.concatenate([ref[wide * i + w] for w in range(wide)], axis=1)
+
     def tile(i, unused):
-        qv = q[i]
+        qv = both(q, i)
         scores = [
             jnp.dot(ref[at : at + keys], qv, preferred_element_type=F32) for ref, at in blocks
         ]
@@ -117,22 +159,21 @@
         ctx_scores = jnp.dot(ctx_key, qv, preferred_element_type=F32) * factor + lift
         largest = jnp.maximum(largest * factor, jnp.max(ctx_scores, axis=0, keepdims=True))
         if not first:
-            largest = jnp.maximum(largest, m_in[i])
+            before = both(m_in, i)
+            largest = jnp.maximum(largest, before)
         terms = jnp.exp2(ctx_scores - largest)
         total = jnp.sum(terms, axis=0, keepdims=True)
         acc = weighted(ctx_value, terms)
         if not first:
-            fade = jnp.exp2(m_in[i] - largest)
-            total = total + l_in[i] * fade
-            acc = acc + acc_in[i] * fade
+            fade = jnp.exp2(before - largest)
+            total = total + both(l_in, i) * fade
+            acc = acc + both(acc_in, i) * fade
         for s, (ref, at) in zip(scores, blocks):
             terms = jnp.exp2(s * factor - largest)
             total = total + jnp.sum(terms, axis=0, keepdims=True)
             acc = acc + weighted(ref[at + keys : at + 2 * keys], terms)
         if last:
-            (out,) = refs
-            dim = acc.shape[0]
-            out[i, 0:dim] = (acc / total).astype(BF16)
+            acc = acc / total
             lse = largest + jnp.log2(total)
             hi = lse.astype(BF16).astype(F32)
             mid = (lse - hi).astype(BF16).astype(F32)
@@ -141,15 +182,21 @@
             packed = jnp.where(
                 row == 0, hi, jnp.where(row == 1, mid, jnp.where(row == 2, low, 0.0))
             )
-            out[i, dim : dim + 16] = packed.astype(BF16)
-        else:
-            m_out, l_out, acc_out = refs
-            m_out[i] = largest
-            l_out[i] = total
-            acc_out[i] = acc
+        for w in range(wide):
+            at = slice(w * width, (w + 1) * width)
+            if last:
+                (out,) = refs
+                dim = acc.shape[0]
+                out[wide * i + w, 0:dim] = acc[:, at].astype(BF16)
+                out[wide * i + w, dim : dim + 16] = packed[:, at].astype(BF16)
+            else:
+                m_out, l_out, acc_out = refs
+                m_out[wide * i + w] = largest[:, at]
+                l_out[wide * i + w] = total[:, at]
+                acc_out[wide * i + w] = acc[:, at]
         return unused
 
-    lax.fori_loop(0, q.shape[0], tile, 0)
+    lax.fori_loop(0, q.shape[0] // wide, tile, 0, unroll=True)
 
 
 def weighted(values, terms):
@@ -167,9 +214,9 @@
         out_shape = (jax.ShapeDtypeStruct((parts, dim + 16, width), BF16),)
     else:
         out_shape = (
-            jax.ShapeDtypeStruct((parts, 1, width), F32),
-            jax.ShapeDtypeStruct((parts, 1, width), F32),
-            jax.ShapeDtypeStruct((parts, dim, width), F32),
+            pltpu.VMEM((parts, 1, width), F32),
+            pltpu.VMEM((parts, 1, width), F32),
+            pltpu.VMEM((parts, dim, width), F32),
         )
     whole = pl.BlockSpec(memory_space=pltpu.VMEM)
     all_keys = (keys + extra) * sum(counts)
@@ -192,8 +239,9 @@
             bytes_accessed=2 * parts * width * dim * 4,
             transcendentals=all_keys * parts * width,
         ),
+        compiler_params=room(32),
         name="attend",
-    )(*operands)
+    )(*near(*operands))
 
 
 def merge_kernel(parts, w_out, out):
@@ -249,71 +297,84 @@
         size = lax.axis_size(axis)
         return lax.ppermute(value, axis, [((i + hop) % size, i) for i in range(size)])
 
-    mine = [latent] + [receive(latent, "x", h) for h in (1, 2, 3)]
-    other = receive(jnp.concatenate(mine, axis=0), "c", 1)
-
-    conds = jax.nn.silu(jnp.stack([condition, context_condition]).astype(F32)).astype(BF16)
-    shift_part, scale_part, gate_part = (
-        jnp.dot(conds, weight, preferred_element_type=F32) for weight in (w_shift, w_scale, w_gate)
-    )
-    partial_mod = jnp.concatenate(
-        [shift_part[0:1], scale_part[0:1], shift_part[1:2], scale_part[1:2], gate_part[0:1]], axis=0
-    )
-    partial_mod = from_everyone(partial_mod, "z")
+    whole = pl.BlockSpec(memory_space=pltpu.VMEM)
+    partial_mod = pl.pallas_call(
+        modulation_kernel,
+        in_specs=[whole] * 5,
+        out_specs=whole,
+        out_shape=jax.ShapeDtypeStruct((lax.axis_size("z"), 5, w_shift.shape[1]), F32),
+        compiler_params=room(16),
+        name="modulation",
+    )(condition[None], context_condition[None], w_shift, w_scale, w_gate)
+    partial_mod = lax.all_to_all(partial_mod, "z", 0, 0, tiled=True)
     partial_mod = partial_mod.sum(axis=0)
     pieces = from_everyone(partial_mod, ("y", *TP))
-    mods = pieces.reshape(y_count, tp_count, *partial_mod.shape).sum(axis=0)
-    mods = mods.transpose(1, 0, 2).reshape(partial_mod.shape[0], model)
+    mine = [latent] + [receive(latent, "x", h) for h in (1, 2, 3)]
+    other = jnp.concatenate(mine, axis=0)
+    other = receive(other, "c", 1)
 
     positions = (lax.axis_index("z") * y_count + lax.axis_index("y")) * tok_dev + jnp.arange(tok_dev)
     cos, sa, sb = rotation_tables(positions, GRID_W, head_dim)
     msg_rows = 2 * tok_dev + 2 * ctx_dev
-    whole = pl.BlockSpec(memory_space=pltpu.VMEM)
     place = jnp.stack([lax.axis_index("x"), lax.axis_index("c")]).astype(jnp.int32)
-    query, message = pl.pallas_call(
+    message, normed, gate = pl.pallas_call(
         project_kernel,
-        in_specs=[pl.BlockSpec(memory_space=pltpu.SMEM)] + [whole] * 16,
-        out_specs=(whole, whole),
+        in_specs=[pl.BlockSpec(memory_space=pltpu.SMEM)] + [whole] * 14,
+        out_specs=(whole, whole, whole),
+        out_shape=(
+            jax.ShapeDtypeStruct((msg_rows, head_dim), BF16),
+            pltpu.VMEM((tok_dev, model), BF16),
+            jax.ShapeDtypeStruct((1, model), F32),
+        ),
         scratch_shapes=[pltpu.VMEM((tok_dev, model), BF16)],
-        out_shape=(
-            jax.ShapeDtypeStruct((y_count, head_dim, heads_dev * tok_dev), BF16),
-            jax.ShapeDtypeStruct((msg_rows, head_dim), BF16),
-        ),
         cost_estimate=pl.CostEstimate(
-            flops=2 * tok_dev * model * 4 * head_dim,
-            bytes_accessed=2 * model * (4 * head_dim + tok_dev),
+            flops=2 * tok_dev * model * 2 * head_dim,
+            bytes_accessed=2 * model * (2 * head_dim + tok_dev),
             transcendentals=0,
         ),
+        compiler_params=room(24),
         name="project",
     )(
         place,
-        *mine,
-        other,
-        context,
-        pre_gain[None],
-        mods[0:4],
-        w_query,
-        w_key,
-        w_value,
-        query_gain[None],
-        key_gain[None],
-        cos,
-        sa,
-        sb,
-    )
-
-    far_up, far_down = receive(message, "z", 5), receive(message, "z", -5)
+        *near(
+            *mine,
+            other,
+            pieces,
+            context,
+            pre_gain[None],
+            w_key,
+            w_value,
+            key_gain[None],
+            cos,
+            sa,
+            sb,
+        ),
+    )
+    query = pl.pallas_call(
+        query_kernel,
+        in_specs=[whole] * 6,
+        out_specs=whole,
+        out_shape=jax.ShapeDtypeStruct((y_count, head_dim, heads_dev * tok_dev), BF16),
+        cost_estimate=pl.CostEstimate(
+            flops=2 * tok_dev * model * 2 * head_dim,
+            bytes_accessed=2 * model * (2 * head_dim + tok_dev),
+            transcendentals=0,
+        ),
+        compiler_params=room(16),
+        name="query",
+    )(*near(normed, w_query, query_gain[None], cos, sa, sb))
+
+    far_up, far_down = receive(message, "z", 6), receive(message, "z", -5)
     up, down = receive(message, "z", 1), receive(message, "z", -1)
     q_all = lax.all_to_all(query, "y", 0, 0, tiled=True)
     ups = receive(jnp.concatenate([up, far_up, far_down], axis=0), "z", 1)
-    downs = receive(jnp.concatenate([down, far_down, far_up], axis=0), "z", -1)
-    opposite = receive(far_up, "z", 3)
-    last_ups = receive(ups[: 2 * msg_rows], "z", 1)
+    downs = receive(jnp.concatenate([far_up, far_down, down], axis=0), "z", -1)
+    last_ups = receive(ups, "z", 1)
     last_downs = receive(downs[: 2 * msg_rows], "z", -1)
     shared = (tok_dev, ctx_dev, factor, lift)
     carry = attend(q_all, [message, up, down, far_up, far_down], None, False, *shared)
     carry = attend(q_all, [ups, downs], carry, False, *shared)
-    (partials,) = attend(q_all, [opposite, last_ups, last_downs], carry, True, *shared)
+    (partials,) = attend(q_all, [last_ups, last_downs], carry, True, *shared)
     returned = lax.all_to_all(partials, "y", 0, 0, tiled=True)
     mixed = pl.pallas_call(
         merge_kernel,
@@ -323,11 +384,14 @@
             bytes_accessed=4 * tok_dev * model,
             transcendentals=0,
         ),
+        in_specs=[whole, whole],
+        out_specs=whole,
+        compiler_params=room(16),
         name="merge",
-    )(returned, w_out)
+    )(*near(returned, w_out))
     arrived = lax.all_to_all(mixed.reshape(tp_count, -1, model), TP, 0, 0, tiled=True)
     mixed = arrived.astype(F32).sum(axis=0)
-    updated = latent.astype(F32) + mods[4] * rms(mixed, post_gain)
+    updated = latent.astype(F32) + gate * rms(mixed, post_gain)
     return updated.astype(BF16)
 
 
@@ -351,4 +415,6 @@
         P(None, TP),
         P(TP, None),
     )
-    return jax.shard_map(body, mesh=torus, in_specs=placed, out_specs=P(ALL, None), check_vma=False)
+    return jax.shard_map(
+        body, mesh=torus, in_specs=placed, out_specs=P(ALL, None), check_vma=False
+    )

time: 186 us -> 162 us (0.87)
  blocking collectives: 11.6 us -> 31.2 us
  starting transfers between devices: 86.4 us -> 71.5 us
  Pallas kernels: 31.9 us -> 18.1 us
  waiting for transfers between devices: 42.4 us -> 31.3 us
    all_to_all x0 -> x1, blocking collectives: none -> 21.4 us  [body(): lax.all_to_all(mixed.reshape(tp_count, -1, model), TP, 0, 0, tiled=True)]
    all_to_all x2 -> x1, starting transfers between devices: 25.2 us -> 10.3 us  [from_everyone(): lax.all_to_all(jnp.broadcast_to(value[None], (devices, *value.shape)), ax...]
    pallas_call x3, Pallas kernels: 24.4 us -> 13.4 us  [attend(): pl.pallas_call(functools.partial(attend_kernel, counts=counts, keys=keys,...]
    all_to_all x1, waiting for transfers between devices: 15 us -> 7.07 us  [body(): partial_mod = lax.all_to_all(partial_mod, 'z', 0, 0, tiled=True)]
    ppermute x13 -> x12, starting transfers between devices: 48.8 us -> 42.8 us  [receive(): lax.ppermute(value, axis, [((i + hop) % size, i) for i in range(size)])]
    all_to_all x1, starting transfers between devices: 8.95 us -> 14.9 us  [body(): partial_mod = lax.all_to_all(partial_mod, 'z', 0, 0, tiled=True)]
    all_to_all x2 -> x1, waiting for transfers between devices: 14 us -> 8.23 us  [from_everyone(): lax.all_to_all(jnp.broadcast_to(value[None], (devices, *value.shape)), ax...]
    pallas_call x1, Pallas kernels: 4.56 us -> 1.78 us  [body(): pl.pallas_call(project_kernel, in_specs=[pl.BlockSpec(memory_space=pltpu....]
  transfers between devices with their start and end apart: 17 -> 15, of which waited for: 6 -> 6; matrix products, arithmetic and copies ran while one was open for 4% -> 2% of each run, Pallas kernels for 9% -> 7%
where the time goes in v3:
time: 162 us; the launch traced here: 161 us
  starting transfers between devices  71.5 us (44%)
  waiting for transfers between devices  31.3 us (19%)
  blocking collectives  31.2 us (19%)
  Pallas kernels  18.1 us (11%)
  local copies, waits for them, and re-layouts  4.67 us (3%)
  other arithmetic  3.57 us (2%)
    ppermute x12, starting transfers between devices, receive(): lax.ppermute(value, axis, [((i + hop) % size, i) for i in range(size)])  42.8 us
    all_to_all x1, blocking collectives, body(): lax.all_to_all(mixed.reshape(tp_count, -1, model), TP, 0, 0, tiled=True)  21.4 us
    ppermute x12, waiting for transfers between devices, receive(): lax.ppermute(value, axis, [((i + hop) % size, i) for i in range(size)])  16 us
    all_to_all x1, starting transfers between devices, body(): partial_mod = lax.all_to_all(partial_mod, 'z', 0, 0, tiled=True)  14.9 us
    pallas_call x3, Pallas kernels, attend(): pl.pallas_call(functools.partial(attend_kernel, counts=counts, keys=keys,...  13.4 us
    all_to_all x1, starting transfers between devices, from_everyone(): lax.all_to_all(jnp.broadcast_to(value[None], (devices, *value.shape)), ax...  10.3 us
    all_to_all x1, blocking collectives, body(): returned = lax.all_to_all(partials, 'y', 0, 0, tiled=True)  9.8 us
    all_to_all x1, waiting for transfers between devices, from_everyone(): lax.all_to_all(jnp.broadcast_to(value[None], (devices, *value.shape)), ax...  8.23 us
  transfers between devices with their start and end apart: 15, of which 6 were waited for; matrix products, arithmetic and copies ran while one was open for 2% of the time, Pallas kernels for 7%

profile of v3, /device:TPU:1, one launch (start us, length us, event | category | flops | bytes accessed | tf_op | source)
XLA Modules:
  0.0 160.8 jit_solution(2162562504278907079)
XLA Ops:
  0.0 5.2 %collective-permute-start = (bf16[32,2048]{1,0:T(8,128)(2,1)}, bf16[32,2048]{1,0:T(8,128)(2,1)S(1)}, u32[]{:S(2)}, u32[]{:S(2)}) collective-permute-start(bf16[32,2048]{1,0:T(8,128)(2,1)} %refs_0_.1), channel_id=1, source_target_pairs={{2,0},{4,2},{6,4},{0,6},{3,1},{5,3},{7,5},{1,7},{10,8},{12,10},{14... | collective-permute-start | bytes 393224 | tf_op jit(solution)/shard_map/ppermute | solution.py:298
  5.2 2.4 %collective-permute-start.1 = (bf16[32,2048]{1,0:T(8,128)(2,1)}, bf16[32,2048]{1,0:T(8,128)(2,1)S(1)}, u32[]{:S(2)}, u32[]{:S(2)}) collective-permute-start(bf16[32,2048]{1,0:T(8,128)(2,1)} %refs_0_.1), channel_id=1, source_target_pairs={{4,0},{6,2},{0,4},{2,6},{5,1},{7,3},{1,5},{3,7},{12,8},{14,10},{8,... | collective-permute-start | bytes 393224 | tf_op jit(solution)/shard_map/ppermute | solution.py:298
  7.6 2.5 %collective-permute-start.2 = (bf16[32,2048]{1,0:T(8,128)(2,1)}, bf16[32,2048]{1,0:T(8,128)(2,1)S(1)}, u32[]{:S(2)}, u32[]{:S(2)}) collective-permute-start(bf16[32,2048]{1,0:T(8,128)(2,1)} %refs_0_.1), channel_id=1, source_target_pairs={{6,0},{0,2},{2,4},{4,6},{7,1},{1,3},{3,5},{5,7},{14,8},{8,10},{10,... | collective-permute-start | bytes 393224 | tf_op jit(solution)/shard_map/ppermute | solution.py:298
  14.4 14.9 %all-to-all-start = ((f32[16,5,256]{2,1,0:T(8,128)}), f32[16,5,256]{2,1,0:T(8,128)S(1)}, u32[]{:S(2)}, u32[]{:S(2)}) async-start(f32[16,5,256]{2,1,0:T(8,128)} %modulation.1), calls=%async_computation | async-start | bytes 262144 | tf_op jit(solution)/shard_map/all_to_all | solution.py:309
  30.5 3.7 %collective-permute-start.3 = (bf16[128,2048]{1,0:T(8,128)(2,1)S(1)}, bf16[128,2048]{1,0:T(8,128)(2,1)S(1)}, u32[]{:S(2)}, u32[]{:S(2)}) collective-permute-start(bf16[128,2048]{1,0:T(8,128)(2,1)S(1)} %pad_maximum_fusion), channel_id=1, source_target_pairs={{1,0},{0,1},{3,2},{2,3},{5,4},{4,5},{7,6},{6,7},{9,8},{8,9},{11,10... | collective-permute-start | bytes 1572872 | tf_op jit(solution)/shard_map/ppermute | solution.py:298
  34.2 7.1 %all-to-all-done = f32[16,5,256]{2,1,0:T(8,128)S(1)} async-done(((f32[16,5,256]{2,1,0:T(8,128)}), f32[16,5,256]{2,1,0:T(8,128)S(1)}, u32[]{:S(2)}, u32[]{:S(2)}) %all-to-all-start) | async-done | bytes 81952 | tf_op jit(solution)/shard_map/all_to_all | solution.py:309
  42.1 10.3 %all-to-all-start.1 = ((f32[32,5,256]{2,1,0:T(8,128)}), f32[32,5,256]{2,1,0:T(8,128)S(1)}, u32[]{:S(2)}, u32[]{:S(2)}) async-start(f32[32,5,256]{2,1,0:T(8,128)} %broadcast_in_dim.76), calls=%async_computation.1 | async-start | bytes 524288 | tf_op jit(solution)/shard_map/all_to_all | solution.py:30
  53.0 8.2 %all-to-all-done.1.refs_5_ = f32[32,5,256]{2,1,0:T(8,128)S(1)} async-done(((f32[32,5,256]{2,1,0:T(8,128)}), f32[32,5,256]{2,1,0:T(8,128)S(1)}, u32[]{:S(2)}, u32[]{:S(2)}) %all-to-all-start.1) | async-done | bytes 163872 | tf_op jit(solution)/shard_map/all_to_all | solution.py:30
  63.1 3.9 %collective-permute-start.4 = (bf16[528,128]{1,0:T(8,128)(2,1)S(1)}, bf16[528,128]{1,0:T(8,128)(2,1)S(1)}, u32[]{:S(2)}, u32[]{:S(2)}) collective-permute-start(bf16[528,128]{1,0:T(8,128)(2,1)S(1)} %get-tuple-element.16.refs_1_), channel_id=1, source_target_pairs={{32,0},{64,32},{96,64},{128,96},{160,128},{192,160},{224,192},{256... | collective-permute-start | bytes 405512 | tf_op jit(solution)/shard_map/ppermute | solution.py:298
  67.0 2.0 %collective-permute-start.5 = (bf16[528,128]{1,0:T(8,128)(2,1)S(1)}, bf16[528,128]{1,0:T(8,128)(2,1)S(1)}, u32[]{:S(2)}, u32[]{:S(2)}) collective-permute-start(bf16[528,128]{1,0:T(8,128)(2,1)S(1)} %get-tuple-element.16.refs_1_), channel_id=1, source_target_pairs={{192,0},{224,32},{256,64},{288,96},{320,128},{352,160},{384,192},{... | collective-permute-start | bytes 405512 | tf_op jit(solution)/shard_map/ppermute | solution.py:298
  69.1 7.8 %collective-permute-start.6 = (bf16[528,128]{1,0:T(8,128)(2,1)S(1)}, bf16[528,128]{1,0:T(8,128)(2,1)S(1)}, u32[]{:S(2)}, u32[]{:S(2)}) collective-permute-start(bf16[528,128]{1,0:T(8,128)(2,1)S(1)} %get-tuple-element.16.refs_1_), channel_id=1, source_target_pairs={{352,0},{384,32},{416,64},{448,96},{480,128},{0,160},{32,192},{64,... | collective-permute-start | bytes 405512 | tf_op jit(solution)/shard_map/ppermute | solution.py:298
  76.9 3.4 %collective-permute-start.9 = (bf16[528,128]{1,0:T(8,128)(2,1)S(1)}, bf16[528,128]{1,0:T(8,128)(2,1)S(1)}, u32[]{:S(2)}, u32[]{:S(2)}) collective-permute-start(bf16[528,128]{1,0:T(8,128)(2,1)S(1)} %get-tuple-element.16.refs_1_), channel_id=1, source_target_pairs={{480,0},{0,32},{32,64},{64,96},{96,128},{128,160},{160,192},{192,2... | collective-permute-start | bytes 405512 | tf_op jit(solution)/shard_map/ppermute | solution.py:298
  80.2 10.0 %collective-permute-done.5.refs_4_ = bf16[528,128]{1,0:T(8,128)(2,1)S(1)} collective-permute-done((bf16[528,128]{1,0:T(8,128)(2,1)S(1)}, bf16[528,128]{1,0:T(8,128)(2,1)S(1)}, u32[]{:S(2)}, u32[]{:S(2)}) %collective-permute-start.5) | collective-permute-done | bytes 135200 | tf_op jit(solution)/shard_map/ppermute | solution.py:298
  90.8 4.1 %collective-permute-done.9.refs_3_ = bf16[528,128]{1,0:T(8,128)(2,1)S(1)} collective-permute-done((bf16[528,128]{1,0:T(8,128)(2,1)S(1)}, bf16[528,128]{1,0:T(8,128)(2,1)S(1)}, u32[]{:S(2)}, u32[]{:S(2)}) %collective-permute-start.9) | collective-permute-done | bytes 135200 | tf_op jit(solution)/shard_map/ppermute | solution.py:298
  95.7 2.8 %collective-permute-start.7 = (bf16[1584,128]{1,0:T(8,128)(2,1)S(1)}, bf16[1584,128]{1,0:T(8,128)(2,1)S(1)}, u32[]{:S(2)}, u32[]{:S(2)}) collective-permute-start(bf16[1584,128]{1,0:T(8,128)(2,1)S(1)} %get-tuple-element.24), channel_id=1, source_target_pairs={{32,0},{64,32},{96,64},{128,96},{160,128},{192,160},{224,192},{256... | collective-permute-start | bytes 1216520 | tf_op jit(solution)/shard_map/ppermute | solution.py:298
  98.5 2.9 %collective-permute-start.10 = (bf16[1584,128]{1,0:T(8,128)(2,1)}, bf16[1584,128]{1,0:T(8,128)(2,1)S(1)}, u32[]{:S(2)}, u32[]{:S(2)}) collective-permute-start(bf16[1584,128]{1,0:T(8,128)(2,1)} %get-tuple-element.23), channel_id=1, source_target_pairs={{480,0},{0,32},{32,64},{64,96},{96,128},{128,160},{160,192},{192,2... | collective-permute-start | bytes 1216520 | tf_op jit(solution)/shard_map/ppermute | solution.py:298
  103.0 3.5 %all-to-all-start.2 = ((bf16[4,128,512]{2,1,0:T(8,128)(2,1)}), bf16[4,128,512]{2,1,0:T(8,128)(2,1)S(1)}, u32[]{:S(2)}, u32[]{:S(2)}) async-start(bf16[4,128,512]{2,1,0:T(8,128)(2,1)} %query.1), calls=%async_computation.2 | async-start | bytes 1048576 | tf_op jit(solution)/shard_map/all_to_all | solution.py:369
  107.9 4.1 %collective-permute-start.8 = (bf16[1584,128]{1,0:T(8,128)(2,1)S(1)}, bf16[1584,128]{1,0:T(8,128)(2,1)S(1)}, u32[]{:S(2)}, u32[]{:S(2)}) collective-permute-start(bf16[1584,128]{1,0:T(8,128)(2,1)S(1)} %collective-permute-done.7.refs_1_), channel_id=1, source_target_pairs={{32,0},{64,32},{96,64},{128,96},{160,128},{192,160},{224,192},{256... | collective-permute-start | bytes 1216520 | tf_op jit(solution)/shard_map/ppermute | solution.py:298
  112.0 2.1 %collective-permute-start.11 = (bf16[1056,128]{1,0:T(8,128)(2,1)S(1)}, bf16[1056,128]{1,0:T(8,128)(2,1)S(1)}, u32[]{:S(2)}, u32[]{:S(2)}) collective-permute-start(bf16[1056,128]{1,0:T(8,128)(2,1)S(1)} %slice.4), channel_id=1, source_target_pairs={{480,0},{0,32},{32,64},{64,96},{96,128},{128,160},{160,192},{192,2... | collective-permute-start | bytes 811016 | tf_op jit(solution)/shard_map/ppermute | solution.py:298
  114.1 4.2 %attend.3 = (f32[4,1,512]{2,1,0:T(1,128)S(1)}, f32[4,1,512]{2,1,0:T(1,128)S(1)}, f32[4,128,512]{2,1,0:T(8,128)S(1)}) custom-call(bf16[4,128,512]{2,1,0:T(8,128)(2,1)S(1)} %all-to-all-done.2.refs_0_, bf16[528,128]{1,0:T(8,128)(2,1)S(1)} %get-tuple-element.16.refs_1_, bf16[528,128]{1,0:T(8,128)(2,1)S(1)} %collective-permute-done.4.refs_2_, ...), custom_call_target="tpu_custom_call" | custom-call | flops 1384120320 | bytes 2097152 | tf_op jit(solution)/shard_map/attend/pallas_call | solution.py:223
  118.3 4.9 %attend.4 = (f32[4,1,512]{2,1,0:T(1,128)S(1)}, f32[4,1,512]{2,1,0:T(1,128)S(1)}, f32[4,128,512]{2,1,0:T(8,128)S(1)}) custom-call(bf16[4,128,512]{2,1,0:T(8,128)(2,1)S(1)} %all-to-all-done.2.refs_0_, bf16[1584,128]{1,0:T(8,128)(2,1)S(1)} %collective-permute-done.7.refs_1_, bf16[1584,128]{1,0:T(8,128)(2,1)S(1)} %collective-permute-done.10.refs_2_, ...), custom_call_target="tpu_custom_call" | custom-call | flops 1660944384 | bytes 2097152 | tf_op jit(solution)/shard_map/attend/pallas_call | solution.py:223
  123.3 4.3 %attend.5 = bf16[4,144,512]{2,1,0:T(8,128)(2,1)S(1)} custom-call(bf16[4,128,512]{2,1,0:T(8,128)(2,1)S(1)} %all-to-all-done.2.refs_0_, bf16[1584,128]{1,0:T(8,128)(2,1)S(1)} %collective-permute-done.8.refs_1_, bf16[1056,128]{1,0:T(8,128)(2,1)S(1)} %collective-permute-done.11.refs_2_, f32[4,1,512]{2,1,0:T(1,128)S(1)} %get-tuple-element.20.refs_3_, ...), custom_call_target="tpu_custom_call" | custom-call | flops 1384120320 | bytes 2097152 | tf_op jit(solution)/shard_map/attend/pallas_call | solution.py:223
  127.6 9.8 %all_to_all.25.parts = bf16[4,144,512]{2,1,0:T(8,128)(2,1)S(1)} all-to-all(bf16[4,144,512]{2,1,0:T(8,128)(2,1)S(1)} %attend.5), channel_id=1, replica_groups=mesh['z'=16,'y'=4,'x'=4,'c'=2] {'y'}, dimensions={0} | all-to-all | bytes 1179648 | tf_op jit(solution)/shard_map/all_to_all | solution.py:378
  137.9 21.4 %all_to_all.26 = bf16[8,32,2048]{2,1,0:T(8,128)(2,1)S(1)} all-to-all(bf16[8,32,2048]{2,1,0:T(8,128)(2,1)S(1)} %bitcast.9), channel_id=1, replica_groups=mesh['z'=16,'y'=4,'x'=4,'c'=2] {'x','c'}, dimensions={0} | all-to-all | bytes 2097152 | tf_op jit(solution)/shard_map/all_to_all | solution.py:392
  (59 shorter events, 14.9 us)
Async XLA Ops:
  0.0 29.4 %collective-permute-start = (bf16[32,2048]{1,0:T(8,128)(2,1)}, bf16[32,2048]{1,0:T(8,128)(2,1)S(1)}, u32[]{:S(2)}, u32[]{:S(2)}) collective-permute-start(bf16[32,2048]{1,0:T(8,128)(2,1)} %refs_0_.1), channel_id=1, source_target_pairs={{2,0},{4,2},{6,4},{0,6},{3,1},{5,3},{7,5},{1,7},{10,8},{12,10},{14... | collective-permute-start | bytes 393224 | tf_op jit(solution)/shard_map/ppermute | solution.py:298
  5.2 24.3 %collective-permute-start.1 = (bf16[32,2048]{1,0:T(8,128)(2,1)}, bf16[32,2048]{1,0:T(8,128)(2,1)S(1)}, u32[]{:S(2)}, u32[]{:S(2)}) collective-permute-start(bf16[32,2048]{1,0:T(8,128)(2,1)} %refs_0_.1), channel_id=1, source_target_pairs={{4,0},{6,2},{0,4},{2,6},{5,1},{7,3},{1,5},{3,7},{12,8},{14,10},{8,... | collective-permute-start | bytes 393224 | tf_op jit(solution)/shard_map/ppermute | solution.py:298
  7.6 21.8 %collective-permute-start.2 = (bf16[32,2048]{1,0:T(8,128)(2,1)}, bf16[32,2048]{1,0:T(8,128)(2,1)S(1)}, u32[]{:S(2)}, u32[]{:S(2)}) collective-permute-start(bf16[32,2048]{1,0:T(8,128)(2,1)} %refs_0_.1), channel_id=1, source_target_pairs={{6,0},{0,2},{2,4},{4,6},{7,1},{1,3},{3,5},{5,7},{14,8},{8,10},{10,... | collective-permute-start | bytes 393224 | tf_op jit(solution)/shard_map/ppermute | solution.py:298
  14.4 26.9 %all-to-all-start = ((f32[16,5,256]{2,1,0:T(8,128)}), f32[16,5,256]{2,1,0:T(8,128)S(1)}, u32[]{:S(2)}, u32[]{:S(2)}) async-start(f32[16,5,256]{2,1,0:T(8,128)} %modulation.1), calls=%async_computation | async-start | bytes 262144 | tf_op jit(solution)/shard_map/all_to_all | solution.py:309
  29.4 31.9 %copy-start = (bf16[32,2048]{1,0:T(8,128)(2,1)S(1)}, bf16[32,2048]{1,0:T(8,128)(2,1)}, u32[]{:S(2)}) copy-start(bf16[32,2048]{1,0:T(8,128)(2,1)} %refs_0_.1) | copy-start | bytes 393220
  29.4 31.9 %copy-start.3 = (bf16[2048,128]{1,0:T(8,128)(2,1)S(1)}, bf16[2048,128]{1,0:T(8,128)(2,1)}, u32[]{:S(2)}) copy-start(bf16[2048,128]{1,0:T(8,128)(2,1)} %refs_8_.1) | copy-start | bytes 1572868
  29.4 31.9 %copy-start.4 = (bf16[2048,128]{1,0:T(8,128)(2,1)S(1)}, bf16[2048,128]{1,0:T(8,128)(2,1)}, u32[]{:S(2)}) copy-start(bf16[2048,128]{1,0:T(8,128)(2,1)} %refs_9_.1) | copy-start | bytes 1572868
  29.4 31.9 %copy-start.5 = (bf16[8,2048]{1,0:T(8,128)(2,1)S(1)}, bf16[8,2048]{1,0:T(8,128)(2,1)}, u32[]{:S(2)}) copy-start(bf16[8,2048]{1,0:T(8,128)(2,1)} %refs_6_.1) | copy-start | bytes 98308
  29.4 31.9 %copy-start.9 = (f32[2048]{0:T(1024)S(1)}, f32[2048]{0:T(1024)}, u32[]{:S(2)}) copy-start(f32[2048]{0:T(1024)} %param.22) | copy-start | bytes 24580
  29.4 31.9 %copy-start.12 = (f32[128]{0:T(128)S(1)}, f32[128]{0:T(128)}, u32[]{:S(2)}) copy-start(f32[128]{0:T(128)} %param.25) | copy-start | bytes 1540
  30.5 30.7 %collective-permute-start.3 = (bf16[128,2048]{1,0:T(8,128)(2,1)S(1)}, bf16[128,2048]{1,0:T(8,128)(2,1)S(1)}, u32[]{:S(2)}, u32[]{:S(2)}) collective-permute-start(bf16[128,2048]{1,0:T(8,128)(2,1)S(1)} %pad_maximum_fusion), channel_id=1, source_target_pairs={{1,0},{0,1},{3,2},{2,3},{5,4},{4,5},{7,6},{6,7},{9,8},{8,9},{11,10... | collective-permute-start | bytes 1572872 | tf_op jit(solution)/shard_map/ppermute | solution.py:298
  42.1 19.2 %all-to-all-start.1 = ((f32[32,5,256]{2,1,0:T(8,128)}), f32[32,5,256]{2,1,0:T(8,128)S(1)}, u32[]{:S(2)}, u32[]{:S(2)}) async-start(f32[32,5,256]{2,1,0:T(8,128)} %broadcast_in_dim.76), calls=%async_computation.1 | async-start | bytes 524288 | tf_op jit(solution)/shard_map/all_to_all | solution.py:30
  63.1 38.3 %copy-start.1 = (bf16[2048,256]{1,0:T(8,128)(2,1)S(1)}, bf16[2048,256]{1,0:T(8,128)(2,1)}, u32[]{:S(2)}) copy-start(bf16[2048,256]{1,0:T(8,128)(2,1)} %wq.1) | copy-start | bytes 3145732
  63.1 38.3 %copy-start.13 = (f32[128]{0:T(128)S(1)}, f32[128]{0:T(128)}, u32[]{:S(2)}) copy-start(f32[128]{0:T(128)} %param.24) | copy-start | bytes 1540
  63.1 17.1 %collective-permute-start.4 = (bf16[528,128]{1,0:T(8,128)(2,1)S(1)}, bf16[528,128]{1,0:T(8,128)(2,1)S(1)}, u32[]{:S(2)}, u32[]{:S(2)}) collective-permute-start(bf16[528,128]{1,0:T(8,128)(2,1)S(1)} %get-tuple-element.16.refs_1_), channel_id=1, source_target_pairs={{32,0},{64,32},{96,64},{128,96},{160,128},{192,160},{224,192},{256... | collective-permute-start | bytes 405512 | tf_op jit(solution)/shard_map/ppermute | solution.py:298
  67.0 23.2 %collective-permute-start.5 = (bf16[528,128]{1,0:T(8,128)(2,1)S(1)}, bf16[528,128]{1,0:T(8,128)(2,1)S(1)}, u32[]{:S(2)}, u32[]{:S(2)}) collective-permute-start(bf16[528,128]{1,0:T(8,128)(2,1)S(1)} %get-tuple-element.16.refs_1_), channel_id=1, source_target_pairs={{192,0},{224,32},{256,64},{288,96},{320,128},{352,160},{384,192},{... | collective-permute-start | bytes 405512 | tf_op jit(solution)/shard_map/ppermute | solution.py:298
  69.1 21.7 %collective-permute-start.6 = (bf16[528,128]{1,0:T(8,128)(2,1)S(1)}, bf16[528,128]{1,0:T(8,128)(2,1)S(1)}, u32[]{:S(2)}, u32[]{:S(2)}) collective-permute-start(bf16[528,128]{1,0:T(8,128)(2,1)S(1)} %get-tuple-element.16.refs_1_), channel_id=1, source_target_pairs={{352,0},{384,32},{416,64},{448,96},{480,128},{0,160},{32,192},{64,... | collective-permute-start | bytes 405512 | tf_op jit(solution)/shard_map/ppermute | solution.py:298
  76.9 18.0 %collective-permute-start.9 = (bf16[528,128]{1,0:T(8,128)(2,1)S(1)}, bf16[528,128]{1,0:T(8,128)(2,1)S(1)}, u32[]{:S(2)}, u32[]{:S(2)}) collective-permute-start(bf16[528,128]{1,0:T(8,128)(2,1)S(1)} %get-tuple-element.16.refs_1_), channel_id=1, source_target_pairs={{480,0},{0,32},{32,64},{64,96},{96,128},{128,160},{160,192},{192,2... | collective-permute-start | bytes 405512 | tf_op jit(solution)/shard_map/ppermute | solution.py:298
  95.7 12.1 %collective-permute-start.7 = (bf16[1584,128]{1,0:T(8,128)(2,1)S(1)}, bf16[1584,128]{1,0:T(8,128)(2,1)S(1)}, u32[]{:S(2)}, u32[]{:S(2)}) collective-permute-start(bf16[1584,128]{1,0:T(8,128)(2,1)S(1)} %get-tuple-element.24), channel_id=1, source_target_pairs={{32,0},{64,32},{96,64},{128,96},{160,128},{192,160},{224,192},{256... | collective-permute-start | bytes 1216520 | tf_op jit(solution)/shard_map/ppermute | solution.py:298
  98.5 13.4 %collective-permute-start.10 = (bf16[1584,128]{1,0:T(8,128)(2,1)}, bf16[1584,128]{1,0:T(8,128)(2,1)S(1)}, u32[]{:S(2)}, u32[]{:S(2)}) collective-permute-start(bf16[1584,128]{1,0:T(8,128)(2,1)} %get-tuple-element.23), channel_id=1, source_target_pairs={{480,0},{0,32},{32,64},{64,96},{96,128},{128,160},{160,192},{192,2... | collective-permute-start | bytes 1216520 | tf_op jit(solution)/shard_map/ppermute | solution.py:298
  103.0 11.1 %all-to-all-start.2 = ((bf16[4,128,512]{2,1,0:T(8,128)(2,1)}), bf16[4,128,512]{2,1,0:T(8,128)(2,1)S(1)}, u32[]{:S(2)}, u32[]{:S(2)}) async-start(bf16[4,128,512]{2,1,0:T(8,128)(2,1)} %query.1), calls=%async_computation.2 | async-start | bytes 1048576 | tf_op jit(solution)/shard_map/all_to_all | solution.py:369
  107.9 15.4 %collective-permute-start.8 = (bf16[1584,128]{1,0:T(8,128)(2,1)S(1)}, bf16[1584,128]{1,0:T(8,128)(2,1)S(1)}, u32[]{:S(2)}, u32[]{:S(2)}) collective-permute-start(bf16[1584,128]{1,0:T(8,128)(2,1)S(1)} %collective-permute-done.7.refs_1_), channel_id=1, source_target_pairs={{32,0},{64,32},{96,64},{128,96},{160,128},{192,160},{224,192},{256... | collective-permute-start | bytes 1216520 | tf_op jit(solution)/shard_map/ppermute | solution.py:298
  112.0 11.3 %collective-permute-start.11 = (bf16[1056,128]{1,0:T(8,128)(2,1)S(1)}, bf16[1056,128]{1,0:T(8,128)(2,1)S(1)}, u32[]{:S(2)}, u32[]{:S(2)}) collective-permute-start(bf16[1056,128]{1,0:T(8,128)(2,1)S(1)} %slice.4), channel_id=1, source_target_pairs={{480,0},{0,32},{32,64},{64,96},{96,128},{128,160},{160,192},{192,2... | collective-permute-start | bytes 811016 | tf_op jit(solution)/shard_map/ppermute | solution.py:298
  127.6 9.8 %copy-start.2 = (bf16[256,2048]{1,0:T(8,128)(2,1)S(1)}, bf16[256,2048]{1,0:T(8,128)(2,1)}, u32[]{:S(2)}) copy-start(bf16[256,2048]{1,0:T(8,128)(2,1)} %w_out.1) | copy-start | bytes 3145732
  (6 other events, 4.2 us)

commit v4 on v3

--- a/solution.py
+++ b/solution.py
@@ -25,6 +25,10 @@
     return [pltpu.with_memory_space_constraint(a, pltpu.VMEM) for a in arrays]
 
 
+def far(*arrays):
+    return [pltpu.with_memory_space_constraint(a, pltpu.HBM) for a in arrays]
+
+
 def from_everyone(value, axes):
     devices = lax.axis_size(axes)
     return lax.all_to_all(
@@ -34,11 +38,6 @@
 
 def rms_rows(values):
     return values * lax.rsqrt(jnp.mean(values * values, axis=-1, keepdims=True) + 1e-06)
-
-
-def rms(values, gain):
-    values = values.astype(F32)
-    return rms_rows(values) * gain
 
 
 def rotation_tables(positions, grid_width, head_dim):
@@ -126,6 +125,30 @@
         qt = jnp.transpose(qh).astype(BF16)
         for i in range(q_out.shape[0]):
             q_out[i, :, h * rows : (h + 1) * rows] = qt
+
+
+def bundle_kernel(*refs, groups):
+    outs = refs[-len(groups) :]
+    for out, group in zip(outs, groups):
+        at = 0
+        for k in group:
+            rows = min(refs[k].shape[0], out.shape[0] - at)
+            out[at : at + rows] = refs[k][0:rows]
+            at += rows
+
+
+def bundled(arrays, groups, rows):
+    whole = pl.BlockSpec(memory_space=pltpu.VMEM)
+    return pl.pallas_call(
+        functools.partial(bundle_kernel, groups=groups),
+        in_specs=[whole] * len(arrays),
+        out_specs=tuple([whole] * len(groups)),
+        out_shape=tuple(
+            jax.ShapeDtypeStruct((rows, arrays[0].shape[1]), arrays[0].dtype) for _ in groups
+        ),
+        compiler_params=room(4),
+        name="bundle",
+    )(*near(*arrays))
 
 
 def attend_kernel(*refs, counts, keys, extra, first, last, factor, lift):
@@ -244,8 +267,8 @@
     )(*near(*operands))
 
 
-def merge_kernel(parts, w_out, out):
-    count, rows, width = parts.shape
+def merge_kernel(parts, out):
+    count, rows, _ = parts.shape
     dim = rows - 16
     tail = [parts[i, dim : dim + 16].astype(F32) for i in range(count)]
     lse = [t[0:1] + t[1:2] + t[2:3] for t in tail]
@@ -255,15 +278,35 @@
     merged = functools.reduce(
         jnp.add, [parts[i, 0:dim].astype(F32) * share[i] for i in range(count)]
     )
-    merged = (merged / whole).astype(BF16)
-    heads = w_out.shape[0] // dim
-    rows = width // heads
-    stacked = jnp.concatenate(
-        [merged[:, h * rows : (h + 1) * rows] for h in range(heads)], axis=0
-    )
-    out[...] = lax.dot_general(
-        stacked, w_out[...], (((0,), (0,)), ((), ())), preferred_element_type=F32
-    ).astype(BF16)
+    merged = merged / whole
+    heads = out.shape[2] // dim
+    chips, part = out.shape[0], out.shape[1]
+    for h in range(heads):
+        turn = jnp.transpose(merged[:, h * chips * part : (h + 1) * chips * part]).astype(BF16)
+        for i in range(chips):
+            out[i, :, h * dim : (h + 1) * dim] = turn[i * part : (i + 1) * part]
+
+
+def out_kernel(place, attended, w0, w1, w2, w3, mine, other, both, held, done):
+    copies = [
+        pltpu.make_async_copy(w, held.at[h], done.at[h]) for h, w in enumerate((w0, w1, w2, w3))
+    ]
+    for copy in copies:
+        copy.start()
+    for h, copy in enumerate(copies):
+        chip = jax.lax.rem(place[0] + h, 4)
+        copy.wait()
+        partial = jnp.dot(attended[chip], held[h], preferred_element_type=F32)
+        partial = partial.astype(BF16).astype(F32)
+        both[...] = partial if h == 0 else both[...] + partial
+    rows = mine.shape[0]
+    mine[...] = both[pl.ds(pl.multiple_of(place[1] * rows, rows), rows)]
+    other[...] = both[pl.ds(pl.multiple_of((1 - place[1]) * rows, rows), rows)]
+
+
+def final_kernel(latent, mine, other, gate, gain, out):
+    mixed = mine[...] + other[...]
+    out[...] = (latent[...].astype(F32) + gate[...] * (rms_rows(mixed) * gain[...])).astype(BF16)
 
 
 def body(
@@ -305,7 +348,7 @@
         out_shape=jax.ShapeDtypeStruct((lax.axis_size("z"), 5, w_shift.shape[1]), F32),
         compiler_params=room(16),
         name="modulation",
-    )(condition[None], context_condition[None], w_shift, w_scale, w_gate)
+    )(*far(condition[None], context_condition[None], w_shift, w_scale, w_gate))
     partial_mod = lax.all_to_all(partial_mod, "z", 0, 0, tiled=True)
     partial_mod = partial_mod.sum(axis=0)
     pieces = from_everyone(partial_mod, ("y", *TP))
@@ -367,32 +410,62 @@
     far_up, far_down = receive(message, "z", 6), receive(message, "z", -5)
     up, down = receive(message, "z", 1), receive(message, "z", -1)
     q_all = lax.all_to_all(query, "y", 0, 0, tiled=True)
-    ups = receive(jnp.concatenate([up, far_up, far_down], axis=0), "z", 1)
-    downs = receive(jnp.concatenate([far_up, far_down, down], axis=0), "z", -1)
+    w_outs = [w_out] + [receive(w_out, "x", h) for h in (1, 2, 3)]
+    to_down, to_up = bundled(
+        [up, far_up, far_down, down], ((0, 1, 2), (1, 2, 3)), 3 * msg_rows
+    )
+    ups, downs = receive(to_down, "z", 1), receive(to_up, "z", -1)
     last_ups = receive(ups, "z", 1)
-    last_downs = receive(downs[: 2 * msg_rows], "z", -1)
+    (to_up,) = bundled([downs], ((0,),), 2 * msg_rows)
+    last_downs = receive(to_up, "z", -1)
     shared = (tok_dev, ctx_dev, factor, lift)
     carry = attend(q_all, [message, up, down, far_up, far_down], None, False, *shared)
     carry = attend(q_all, [ups, downs], carry, False, *shared)
     (partials,) = attend(q_all, [last_ups, last_downs], carry, True, *shared)
     returned = lax.all_to_all(partials, "y", 0, 0, tiled=True)
-    mixed = pl.pallas_call(
+    attended = pl.pallas_call(
         merge_kernel,
-        out_shape=jax.ShapeDtypeStruct((tok_dev, model), BF16),
+        in_specs=[whole],
+        out_specs=whole,
+        out_shape=jax.ShapeDtypeStruct(
+            (lax.axis_size("x"), tok_dev // lax.axis_size("x"), heads_dev * head_dim), BF16
+        ),
+        compiler_params=room(16),
+        name="merge",
+    )(*near(returned))
+    attended = lax.all_to_all(attended, "x", 0, 0, tiled=True)
+    rows = latent.shape[0]
+    sums, others = pl.pallas_call(
+        out_kernel,
+        in_specs=[pl.BlockSpec(memory_space=pltpu.SMEM), whole]
+        + [pl.BlockSpec(memory_space=pltpu.HBM)] * 4,
+        out_specs=(whole, whole),
+        out_shape=(
+            jax.ShapeDtypeStruct((rows, model), F32),
+            jax.ShapeDtypeStruct((rows, model), F32),
+        ),
+        scratch_shapes=[
+            pltpu.VMEM((2 * rows, model), F32),
+            pltpu.VMEM((4, *w_out.shape), BF16),
+            pltpu.SemaphoreType.DMA((4,)),
+        ],
+        compiler_params=room(16),
         cost_estimate=pl.CostEstimate(
             flops=2 * tok_dev * model * heads_dev * head_dim,
             bytes_accessed=4 * tok_dev * model,
             transcendentals=0,
         ),
-        in_specs=[whole, whole],
+        name="out",
+    )(place, *near(attended), *far(*w_outs))
+    others = receive(others, "c", 1)
+    return pl.pallas_call(
+        final_kernel,
+        in_specs=[whole] * 5,
         out_specs=whole,
+        out_shape=jax.ShapeDtypeStruct((rows, model), BF16),
         compiler_params=room(16),
-        name="merge",
-    )(*near(returned, w_out))
-    arrived = lax.all_to_all(mixed.reshape(tp_count, -1, model), TP, 0, 0, tiled=True)
-    mixed = arrived.astype(F32).sum(axis=0)
-    updated = latent.astype(F32) + gate * rms(mixed, post_gain)
-    return updated.astype(BF16)
+        name="final",
+    )(*near(latent, sums, others, gate, post_gain[None]))
 
 
 def solution(mesh):
@@ -415,6 +488,4 @@
         P(None, TP),
         P(TP, None),
     )
-    return jax.shard_map(
-        body, mesh=torus, in_specs=placed, out_specs=P(ALL, None), check_vma=False
-    )
+    return jax.shard_map(body, mesh=torus, in_specs=placed, out_specs=P(ALL, None), check_vma=False)

time: 162 us -> 174 us (1.074)
  blocking collectives: 31.2 us -> 10.5 us
  waiting for transfers between devices: 31.3 us -> 49.2 us
  starting transfers between devices: 71.5 us -> 86.3 us
  Pallas kernels: 18.1 us -> 24 us
  other arithmetic: 3.57 us -> 0.72 us
  local copies, waits for them, and re-layouts: 4.67 us -> 2.01 us
    all_to_all x1 -> x0, blocking collectives: 21.4 us -> none  [body(): lax.all_to_all(mixed.reshape(tp_count, -1, model), TP, 0, 0, tiled=True)]
    ppermute x12 -> x16, waiting for transfers between devices: 16 us -> 32.3 us  [receive(): lax.ppermute(value, axis, [((i + hop) % size, i) for i in range(size)])]
    ppermute x12 -> x16, starting transfers between devices: 42.8 us -> 53.5 us  [receive(): lax.ppermute(value, axis, [((i + hop) % size, i) for i in range(size)])]
    pallas_call x1 -> x5, Pallas kernels: 0.55 us -> 5.59 us  [the longest x1 3.08 us: body(): pl.pallas_call(out_kernel, in_specs=[pl.BlockSpec(memory_space=pltpu.SMEM...]
    all_to_all x0 -> x1, starting transfers between devices: none -> 3.93 us  [body(): attended = lax.all_to_all(attended, 'x', 0, 0, tiled=True)]
    unnamed x30 -> x18, local copies, waits for them, and re-layouts: 3.93 us -> 1.29 us
  transfers between devices with their start and end apart: 15 -> 20, of which waited for: 6 -> 9; matrix products, arithmetic and copies ran while one was open for 2% -> 1% of each run, Pallas kernels for 7% -> 10%
where the time goes in v4:
time: 174 us; the launch traced here: 173 us
  starting transfers between devices  86.3 us (50%)
  waiting for transfers between devices  49.2 us (28%)
  Pallas kernels  24 us (14%)
  blocking collectives  10.5 us (6%)
  local copies, waits for them, and re-layouts  2.01 us (1%)
    ppermute x16, starting transfers between devices, receive(): lax.ppermute(value, axis, [((i + hop) % size, i) for i in range(size)])  53.5 us
    ppermute x16, waiting for transfers between devices, receive(): lax.ppermute(value, axis, [((i + hop) % size, i) for i in range(size)])  32.3 us
    all_to_all x1, starting transfers between devices, body(): partial_mod = lax.all_to_all(partial_mod, 'z', 0, 0, tiled=True)  15 us
    pallas_call x3, Pallas kernels, attend(): pl.pallas_call(functools.partial(attend_kernel, counts=counts, keys=keys,...  13.5 us
    all_to_all x1, blocking collectives, body(): returned = lax.all_to_all(partials, 'y', 0, 0, tiled=True)  10.5 us
    all_to_all x1, starting transfers between devices, from_everyone(): lax.all_to_all(jnp.broadcast_to(value[None], (devices, *value.shape)), ax...  10.4 us
    all_to_all x1, waiting for transfers between devices, from_everyone(): lax.all_to_all(jnp.broadcast_to(value[None], (devices, *value.shape)), ax...  8.21 us
    all_to_all x1, waiting for transfers between devices, body(): partial_mod = lax.all_to_all(partial_mod, 'z', 0, 0, tiled=True)  8.11 us
  transfers between devices with their start and end apart: 20, of which 9 were waited for; matrix products, arithmetic and copies ran while one was open for 1% of the time, Pallas kernels for 10%

profile of v4, /device:TPU:1, one launch (start us, length us, event | category | flops | bytes accessed | tf_op | source)
XLA Modules:
  0.0 173.1 jit_solution(10451828531922937823)
XLA Ops:
  0.0 5.2 %collective-permute-start = (bf16[32,2048]{1,0:T(8,128)(2,1)}, bf16[32,2048]{1,0:T(8,128)(2,1)S(1)}, u32[]{:S(2)}, u32[]{:S(2)}) collective-permute-start(bf16[32,2048]{1,0:T(8,128)(2,1)} %latent.1), channel_id=1, source_target_pairs={{2,0},{4,2},{6,4},{0,6},{3,1},{5,3},{7,5},{1,7},{10,8},{12,10},{14... | collective-permute-start | bytes 393224 | tf_op jit(solution)/shard_map/ppermute | solution.py:341
  11.8 15.0 %all-to-all-start = ((f32[16,5,256]{2,1,0:T(8,128)}), f32[16,5,256]{2,1,0:T(8,128)S(1)}, u32[]{:S(2)}, u32[]{:S(2)}) async-start(f32[16,5,256]{2,1,0:T(8,128)} %modulation.1), calls=%async_computation | async-start | bytes 262144 | tf_op jit(solution)/shard_map/all_to_all | solution.py:352
  26.9 3.7 %collective-permute-start.3 = (bf16[128,2048]{1,0:T(8,128)(2,1)S(1)}, bf16[128,2048]{1,0:T(8,128)(2,1)S(1)}, u32[]{:S(2)}, u32[]{:S(2)}) collective-permute-start(bf16[128,2048]{1,0:T(8,128)(2,1)S(1)} %pad_maximum_fusion), channel_id=1, source_target_pairs={{1,0},{0,1},{3,2},{2,3},{5,4},{4,5},{7,6},{6,7},{9,8},{8,9},{11,10... | collective-permute-start | bytes 1572872 | tf_op jit(solution)/shard_map/ppermute | solution.py:341
  30.7 8.1 %all-to-all-done = f32[16,5,256]{2,1,0:T(8,128)S(1)} async-done(((f32[16,5,256]{2,1,0:T(8,128)}), f32[16,5,256]{2,1,0:T(8,128)S(1)}, u32[]{:S(2)}, u32[]{:S(2)}) %all-to-all-start) | async-done | bytes 81952 | tf_op jit(solution)/shard_map/all_to_all | solution.py:352
  39.5 10.4 %all-to-all-start.1 = ((f32[32,5,256]{2,1,0:T(8,128)}), f32[32,5,256]{2,1,0:T(8,128)S(1)}, u32[]{:S(2)}, u32[]{:S(2)}) async-start(f32[32,5,256]{2,1,0:T(8,128)} %broadcast_in_dim.77), calls=%async_computation.1 | async-start | bytes 524288 | tf_op jit(solution)/shard_map/all_to_all | solution.py:34
  50.6 8.2 %all-to-all-done.1.refs_5_ = f32[32,5,256]{2,1,0:T(8,128)S(1)} async-done(((f32[32,5,256]{2,1,0:T(8,128)}), f32[32,5,256]{2,1,0:T(8,128)S(1)}, u32[]{:S(2)}, u32[]{:S(2)}) %all-to-all-start.1) | async-done | bytes 163872 | tf_op jit(solution)/shard_map/all_to_all | solution.py:34
  61.3 3.8 %collective-permute-start.4 = (bf16[528,128]{1,0:T(8,128)(2,1)S(1)}, bf16[528,128]{1,0:T(8,128)(2,1)S(1)}, u32[]{:S(2)}, u32[]{:S(2)}) collective-permute-start(bf16[528,128]{1,0:T(8,128)(2,1)S(1)} %get-tuple-element.19.refs_1_), channel_id=1, source_target_pairs={{32,0},{64,32},{96,64},{128,96},{160,128},{192,160},{224,192},{256... | collective-permute-start | bytes 405512 | tf_op jit(solution)/shard_map/ppermute | solution.py:341
  67.1 7.8 %collective-permute-start.6 = (bf16[528,128]{1,0:T(8,128)(2,1)S(1)}, bf16[528,128]{1,0:T(8,128)(2,1)S(1)}, u32[]{:S(2)}, u32[]{:S(2)}) collective-permute-start(bf16[528,128]{1,0:T(8,128)(2,1)S(1)} %get-tuple-element.19.refs_1_), channel_id=1, source_target_pairs={{352,0},{384,32},{416,64},{448,96},{480,128},{0,160},{32,192},{64,... | collective-permute-start | bytes 405512 | tf_op jit(solution)/shard_map/ppermute | solution.py:341
  74.9 3.4 %collective-permute-start.7 = (bf16[528,128]{1,0:T(8,128)(2,1)S(1)}, bf16[528,128]{1,0:T(8,128)(2,1)S(1)}, u32[]{:S(2)}, u32[]{:S(2)}) collective-permute-start(bf16[528,128]{1,0:T(8,128)(2,1)S(1)} %get-tuple-element.19.refs_1_), channel_id=1, source_target_pairs={{480,0},{0,32},{32,64},{64,96},{96,128},{128,160},{160,192},{192,2... | collective-permute-start | bytes 405512 | tf_op jit(solution)/shard_map/ppermute | solution.py:341
  78.3 10.0 %collective-permute-done.5.refs_1_.refs_4_ = bf16[528,128]{1,0:T(8,128)(2,1)S(1)} collective-permute-done((bf16[528,128]{1,0:T(8,128)(2,1)S(1)}, bf16[528,128]{1,0:T(8,128)(2,1)S(1)}, u32[]{:S(2)}, u32[]{:S(2)}) %collective-permute-start.5) | collective-permute-done | bytes 135200 | tf_op jit(solution)/shard_map/ppermute | solution.py:341
  88.7 4.3 %collective-permute-done.7.refs_3_ = bf16[528,128]{1,0:T(8,128)(2,1)S(1)} collective-permute-done((bf16[528,128]{1,0:T(8,128)(2,1)S(1)}, bf16[528,128]{1,0:T(8,128)(2,1)S(1)}, u32[]{:S(2)}, u32[]{:S(2)}) %collective-permute-start.7) | collective-permute-done | bytes 135200 | tf_op jit(solution)/shard_map/ppermute | solution.py:341
  96.5 2.9 %collective-permute-start.10 = (bf16[1584,128]{1,0:T(8,128)(2,1)}, bf16[1584,128]{1,0:T(8,128)(2,1)S(1)}, u32[]{:S(2)}, u32[]{:S(2)}) collective-permute-start(bf16[1584,128]{1,0:T(8,128)(2,1)} %get-tuple-element.21), channel_id=1, source_target_pairs={{480,0},{0,32},{32,64},{64,96},{96,128},{128,160},{160,192},{192,2... | collective-permute-start | bytes 1216520 | tf_op jit(solution)/shard_map/ppermute | solution.py:341
  101.7 3.5 %all-to-all-start.2 = ((bf16[4,128,512]{2,1,0:T(8,128)(2,1)}), bf16[4,128,512]{2,1,0:T(8,128)(2,1)S(1)}, u32[]{:S(2)}, u32[]{:S(2)}) async-start(bf16[4,128,512]{2,1,0:T(8,128)(2,1)} %query.1), calls=%async_computation.2 | async-start | bytes 1048576 | tf_op jit(solution)/shard_map/all_to_all | solution.py:412
  105.9 4.1 %collective-permute-start.9 = (bf16[1584,128]{1,0:T(8,128)(2,1)S(1)}, bf16[1584,128]{1,0:T(8,128)(2,1)S(1)}, u32[]{:S(2)}, u32[]{:S(2)}) collective-permute-start(bf16[1584,128]{1,0:T(8,128)(2,1)S(1)} %collective-permute-done.8.refs_1_), channel_id=1, source_target_pairs={{32,0},{64,32},{96,64},{128,96},{160,128},{192,160},{224,192},{256... | collective-permute-start | bytes 1216520 | tf_op jit(solution)/shard_map/ppermute | solution.py:341
  110.0 3.0 %collective-permute-start.12 = (bf16[256,2048]{1,0:T(8,128)(2,1)}, bf16[256,2048]{1,0:T(8,128)(2,1)}, u32[]{:S(2)}, u32[]{:S(2)}) collective-permute-start(bf16[256,2048]{1,0:T(8,128)(2,1)} %w0.1), channel_id=1, source_target_pairs={{2,0},{4,2},{6,4},{0,6},{3,1},{5,3},{7,5},{1,7},{10,8},{12,10},{14... | collective-permute-start | bytes 3145736 | tf_op jit(solution)/shard_map/ppermute | solution.py:341
  113.0 3.0 %collective-permute-start.13 = (bf16[256,2048]{1,0:T(8,128)(2,1)}, bf16[256,2048]{1,0:T(8,128)(2,1)}, u32[]{:S(2)}, u32[]{:S(2)}) collective-permute-start(bf16[256,2048]{1,0:T(8,128)(2,1)} %w0.1), channel_id=1, source_target_pairs={{4,0},{6,2},{0,4},{2,6},{5,1},{7,3},{1,5},{3,7},{12,8},{14,10},{8,... | collective-permute-start | bytes 3145736 | tf_op jit(solution)/shard_map/ppermute | solution.py:341
  120.2 4.2 %attend.3 = (f32[4,1,512]{2,1,0:T(1,128)S(1)}, f32[4,1,512]{2,1,0:T(1,128)S(1)}, f32[4,128,512]{2,1,0:T(8,128)S(1)}) custom-call(bf16[4,128,512]{2,1,0:T(8,128)(2,1)S(1)} %all-to-all-done.2.refs_0_, bf16[528,128]{1,0:T(8,128)(2,1)S(1)} %get-tuple-element.19.refs_1_, bf16[528,128]{1,0:T(8,128)(2,1)S(1)} %collective-permute-done.4.refs_0_.refs_2_, ...), custom_call_target="tpu_custom_call" | custom-call | flops 1384120320 | bytes 2097152 | tf_op jit(solution)/shard_map/attend/pallas_call | solution.py:246
  124.4 5.0 %attend.4 = (f32[4,1,512]{2,1,0:T(1,128)S(1)}, f32[4,1,512]{2,1,0:T(1,128)S(1)}, f32[4,128,512]{2,1,0:T(8,128)S(1)}) custom-call(bf16[4,128,512]{2,1,0:T(8,128)(2,1)S(1)} %all-to-all-done.2.refs_0_, bf16[1584,128]{1,0:T(8,128)(2,1)S(1)} %collective-permute-done.8.refs_1_, bf16[1584,128]{1,0:T(8,128)(2,1)S(1)} %collective-permute-done.10.refs_0_.refs_2_, ...), custom_call_target="tpu_custom_call" | custom-call | flops 1660944384 | bytes 2097152 | tf_op jit(solution)/shard_map/attend/pallas_call | solution.py:246
  129.4 4.3 %attend.5 = bf16[4,144,512]{2,1,0:T(8,128)(2,1)S(1)} custom-call(bf16[4,128,512]{2,1,0:T(8,128)(2,1)S(1)} %all-to-all-done.2.refs_0_, bf16[1584,128]{1,0:T(8,128)(2,1)S(1)} %collective-permute-done.9.refs_1_, bf16[1056,128]{1,0:T(8,128)(2,1)S(1)} %collective-permute-done.11.refs_2_, f32[4,1,512]{2,1,0:T(1,128)S(1)} %get-tuple-element.25.refs_3_, ...), custom_call_target="tpu_custom_call" | custom-call | flops 1384120320 | bytes 2097152 | tf_op jit(solution)/shard_map/attend/pallas_call | solution.py:246
  133.7 10.5 %all_to_all.25.parts = bf16[4,144,512]{2,1,0:T(8,128)(2,1)S(1)} all-to-all(bf16[4,144,512]{2,1,0:T(8,128)(2,1)S(1)} %attend.5), channel_id=1, replica_groups=mesh['z'=16,'y'=4,'x'=4,'c'=2] {'y'}, dimensions={0} | all-to-all | bytes 1179648 | tf_op jit(solution)/shard_map/all_to_all | solution.py:425
  145.0 3.9 %all-to-all-start.4 = ((bf16[4,64,256]{2,1,0:T(8,128)(2,1)}), bf16[4,64,256]{2,1,0:T(8,128)(2,1)S(1)}, u32[]{:S(2)}, u32[]{:S(2)}) async-start(bf16[4,64,256]{2,1,0:T(8,128)(2,1)} %merge.1), calls=%async_computation.4 | async-start | bytes 262144 | tf_op jit(solution)/shard_map/all_to_all | solution.py:436
  149.0 15.7 %collective-permute-done.14.w3 = bf16[256,2048]{1,0:T(8,128)(2,1)} collective-permute-done((bf16[256,2048]{1,0:T(8,128)(2,1)}, bf16[256,2048]{1,0:T(8,128)(2,1)}, u32[]{:S(2)}, u32[]{:S(2)}) %collective-permute-start.14) | collective-permute-done | bytes 1048608 | tf_op jit(solution)/shard_map/ppermute | solution.py:341
  165.3 3.1 %out.1 = (f32[32,2048]{1,0:T(8,128)S(1)}, f32[32,2048]{1,0:T(8,128)S(1)}) custom-call(s32[2]{0:T(128)S(1)} %pad_add_fusion.place, bf16[4,64,256]{2,1,0:T(8,128)(2,1)S(1)} %all-to-all-done.4.attended, bf16[256,2048]{1,0:T(8,128)(2,1)} %w0.1, bf16[256,2048]{1,0:T(8,128)(2,1)} %collective-permute-done.12.w1, bf16[256,2048]{1,0:T(8,128)(2,1)} %collective-permute-done.13.w2, ...), custom_call_target="tpu_custom_call" | custom-call | flops 268435456 | bytes 2097152 | tf_op jit(solution)/shard_map/out/pallas_call | solution.py:438
  168.3 2.8 %collective-permute-start.15 = (f32[32,2048]{1,0:T(8,128)S(1)}, f32[32,2048]{1,0:T(8,128)S(1)}, u32[]{:S(2)}, u32[]{:S(2)}) collective-permute-start(f32[32,2048]{1,0:T(8,128)S(1)} %get-tuple-element.29), channel_id=1, source_target_pairs={{1,0},{0,1},{3,2},{2,3},{5,4},{4,5},{7,6},{6,7},{9,8},{8,9},{11,10... | collective-permute-start | bytes 786440 | tf_op jit(solution)/shard_map/ppermute | solution.py:341
  (54 shorter events, 26.8 us)
Async XLA Ops:
  0.0 26.8 %collective-permute-start = (bf16[32,2048]{1,0:T(8,128)(2,1)}, bf16[32,2048]{1,0:T(8,128)(2,1)S(1)}, u32[]{:S(2)}, u32[]{:S(2)}) collective-permute-start(bf16[32,2048]{1,0:T(8,128)(2,1)} %latent.1), channel_id=1, source_target_pairs={{2,0},{4,2},{6,4},{0,6},{3,1},{5,3},{7,5},{1,7},{10,8},{12,10},{14... | collective-permute-start | bytes 393224 | tf_op jit(solution)/shard_map/ppermute | solution.py:341
  5.2 21.6 %collective-permute-start.1 = (bf16[32,2048]{1,0:T(8,128)(2,1)}, bf16[32,2048]{1,0:T(8,128)(2,1)S(1)}, u32[]{:S(2)}, u32[]{:S(2)}) collective-permute-start(bf16[32,2048]{1,0:T(8,128)(2,1)} %latent.1), channel_id=1, source_target_pairs={{4,0},{6,2},{0,4},{2,6},{5,1},{7,3},{1,5},{3,7},{12,8},{14,10},{8,... | collective-permute-start | bytes 393224 | tf_op jit(solution)/shard_map/ppermute | solution.py:341
  7.6 19.2 %collective-permute-start.2 = (bf16[32,2048]{1,0:T(8,128)(2,1)}, bf16[32,2048]{1,0:T(8,128)(2,1)S(1)}, u32[]{:S(2)}, u32[]{:S(2)}) collective-permute-start(bf16[32,2048]{1,0:T(8,128)(2,1)} %latent.1), channel_id=1, source_target_pairs={{6,0},{0,2},{2,4},{4,6},{7,1},{1,3},{3,5},{5,7},{14,8},{8,10},{10,... | collective-permute-start | bytes 393224 | tf_op jit(solution)/shard_map/ppermute | solution.py:341
  11.7 15.1 %copy-start = (bf16[32,2048]{1,0:T(8,128)(2,1)S(1)}, bf16[32,2048]{1,0:T(8,128)(2,1)}, u32[]{:S(2)}) copy-start(bf16[32,2048]{1,0:T(8,128)(2,1)} %latent.1) | copy-start | bytes 393220
  11.8 27.0 %all-to-all-start = ((f32[16,5,256]{2,1,0:T(8,128)}), f32[16,5,256]{2,1,0:T(8,128)S(1)}, u32[]{:S(2)}, u32[]{:S(2)}) async-start(f32[16,5,256]{2,1,0:T(8,128)} %modulation.1), calls=%async_computation | async-start | bytes 262144 | tf_op jit(solution)/shard_map/all_to_all | solution.py:352
  26.9 31.9 %collective-permute-start.3 = (bf16[128,2048]{1,0:T(8,128)(2,1)S(1)}, bf16[128,2048]{1,0:T(8,128)(2,1)S(1)}, u32[]{:S(2)}, u32[]{:S(2)}) collective-permute-start(bf16[128,2048]{1,0:T(8,128)(2,1)S(1)} %pad_maximum_fusion), channel_id=1, source_target_pairs={{1,0},{0,1},{3,2},{2,3},{5,4},{4,5},{7,6},{6,7},{9,8},{8,9},{11,10... | collective-permute-start | bytes 1572872 | tf_op jit(solution)/shard_map/ppermute | solution.py:341
  38.8 20.0 %copy-start.3 = (bf16[2048,128]{1,0:T(8,128)(2,1)S(1)}, bf16[2048,128]{1,0:T(8,128)(2,1)}, u32[]{:S(2)}) copy-start(bf16[2048,128]{1,0:T(8,128)(2,1)} %refs_9_.1) | copy-start | bytes 1572868
  39.5 19.3 %copy-start.2 = (bf16[2048,128]{1,0:T(8,128)(2,1)S(1)}, bf16[2048,128]{1,0:T(8,128)(2,1)}, u32[]{:S(2)}) copy-start(bf16[2048,128]{1,0:T(8,128)(2,1)} %refs_8_.1) | copy-start | bytes 1572868
  39.5 19.3 %all-to-all-start.1 = ((f32[32,5,256]{2,1,0:T(8,128)}), f32[32,5,256]{2,1,0:T(8,128)S(1)}, u32[]{:S(2)}, u32[]{:S(2)}) async-start(f32[32,5,256]{2,1,0:T(8,128)} %broadcast_in_dim.77), calls=%async_computation.1 | async-start | bytes 524288 | tf_op jit(solution)/shard_map/all_to_all | solution.py:34
  59.5 40.0 %copy-start.1 = (bf16[2048,256]{1,0:T(8,128)(2,1)S(1)}, bf16[2048,256]{1,0:T(8,128)(2,1)}, u32[]{:S(2)}) copy-start(bf16[2048,256]{1,0:T(8,128)(2,1)} %wq.1) | copy-start | bytes 3145732
  61.3 17.0 %collective-permute-start.4 = (bf16[528,128]{1,0:T(8,128)(2,1)S(1)}, bf16[528,128]{1,0:T(8,128)(2,1)S(1)}, u32[]{:S(2)}, u32[]{:S(2)}) collective-permute-start(bf16[528,128]{1,0:T(8,128)(2,1)S(1)} %get-tuple-element.19.refs_1_), channel_id=1, source_target_pairs={{32,0},{64,32},{96,64},{128,96},{160,128},{192,160},{224,192},{256... | collective-permute-start | bytes 405512 | tf_op jit(solution)/shard_map/ppermute | solution.py:341
  65.1 23.2 %collective-permute-start.5 = (bf16[528,128]{1,0:T(8,128)(2,1)S(1)}, bf16[528,128]{1,0:T(8,128)(2,1)S(1)}, u32[]{:S(2)}, u32[]{:S(2)}) collective-permute-start(bf16[528,128]{1,0:T(8,128)(2,1)S(1)} %get-tuple-element.19.refs_1_), channel_id=1, source_target_pairs={{192,0},{224,32},{256,64},{288,96},{320,128},{352,160},{384,192},{... | collective-permute-start | bytes 405512 | tf_op jit(solution)/shard_map/ppermute | solution.py:341
  67.1 21.6 %collective-permute-start.6 = (bf16[528,128]{1,0:T(8,128)(2,1)S(1)}, bf16[528,128]{1,0:T(8,128)(2,1)S(1)}, u32[]{:S(2)}, u32[]{:S(2)}) collective-permute-start(bf16[528,128]{1,0:T(8,128)(2,1)S(1)} %get-tuple-element.19.refs_1_), channel_id=1, source_target_pairs={{352,0},{384,32},{416,64},{448,96},{480,128},{0,160},{32,192},{64,... | collective-permute-start | bytes 405512 | tf_op jit(solution)/shard_map/ppermute | solution.py:341
  74.9 18.1 %collective-permute-start.7 = (bf16[528,128]{1,0:T(8,128)(2,1)S(1)}, bf16[528,128]{1,0:T(8,128)(2,1)S(1)}, u32[]{:S(2)}, u32[]{:S(2)}) collective-permute-start(bf16[528,128]{1,0:T(8,128)(2,1)S(1)} %get-tuple-element.19.refs_1_), channel_id=1, source_target_pairs={{480,0},{0,32},{32,64},{64,96},{96,128},{128,160},{160,192},{192,2... | collective-permute-start | bytes 405512 | tf_op jit(solution)/shard_map/ppermute | solution.py:341
  93.8 12.1 %collective-permute-start.8 = (bf16[1584,128]{1,0:T(8,128)(2,1)S(1)}, bf16[1584,128]{1,0:T(8,128)(2,1)S(1)}, u32[]{:S(2)}, u32[]{:S(2)}) collective-permute-start(bf16[1584,128]{1,0:T(8,128)(2,1)S(1)} %get-tuple-element.20), channel_id=1, source_target_pairs={{32,0},{64,32},{96,64},{128,96},{160,128},{192,160},{224,192},{256... | collective-permute-start | bytes 1216520 | tf_op jit(solution)/shard_map/ppermute | solution.py:341
  96.5 21.5 %collective-permute-start.10 = (bf16[1584,128]{1,0:T(8,128)(2,1)}, bf16[1584,128]{1,0:T(8,128)(2,1)S(1)}, u32[]{:S(2)}, u32[]{:S(2)}) collective-permute-start(bf16[1584,128]{1,0:T(8,128)(2,1)} %get-tuple-element.21), channel_id=1, source_target_pairs={{480,0},{0,32},{32,64},{64,96},{96,128},{128,160},{160,192},{192,2... | collective-permute-start | bytes 1216520 | tf_op jit(solution)/shard_map/ppermute | solution.py:341
  101.7 18.5 %all-to-all-start.2 = ((bf16[4,128,512]{2,1,0:T(8,128)(2,1)}), bf16[4,128,512]{2,1,0:T(8,128)(2,1)S(1)}, u32[]{:S(2)}, u32[]{:S(2)}) async-start(bf16[4,128,512]{2,1,0:T(8,128)(2,1)} %query.1), calls=%async_computation.2 | async-start | bytes 1048576 | tf_op jit(solution)/shard_map/all_to_all | solution.py:412
  105.9 23.5 %collective-permute-start.9 = (bf16[1584,128]{1,0:T(8,128)(2,1)S(1)}, bf16[1584,128]{1,0:T(8,128)(2,1)S(1)}, u32[]{:S(2)}, u32[]{:S(2)}) collective-permute-start(bf16[1584,128]{1,0:T(8,128)(2,1)S(1)} %collective-permute-done.8.refs_1_), channel_id=1, source_target_pairs={{32,0},{64,32},{96,64},{128,96},{160,128},{192,160},{224,192},{256... | collective-permute-start | bytes 1216520 | tf_op jit(solution)/shard_map/ppermute | solution.py:341
  110.0 39.0 %collective-permute-start.12 = (bf16[256,2048]{1,0:T(8,128)(2,1)}, bf16[256,2048]{1,0:T(8,128)(2,1)}, u32[]{:S(2)}, u32[]{:S(2)}) collective-permute-start(bf16[256,2048]{1,0:T(8,128)(2,1)} %w0.1), channel_id=1, source_target_pairs={{2,0},{4,2},{6,4},{0,6},{3,1},{5,3},{7,5},{1,7},{10,8},{12,10},{14... | collective-permute-start | bytes 3145736 | tf_op jit(solution)/shard_map/ppermute | solution.py:341
  113.0 35.9 %collective-permute-start.13 = (bf16[256,2048]{1,0:T(8,128)(2,1)}, bf16[256,2048]{1,0:T(8,128)(2,1)}, u32[]{:S(2)}, u32[]{:S(2)}) collective-permute-start(bf16[256,2048]{1,0:T(8,128)(2,1)} %w0.1), channel_id=1, source_target_pairs={{4,0},{6,2},{0,4},{2,6},{5,1},{7,3},{1,5},{3,7},{12,8},{14,10},{8,... | collective-permute-start | bytes 3145736 | tf_op jit(solution)/shard_map/ppermute | solution.py:341
  116.1 48.6 %collective-permute-start.14 = (bf16[256,2048]{1,0:T(8,128)(2,1)}, bf16[256,2048]{1,0:T(8,128)(2,1)}, u32[]{:S(2)}, u32[]{:S(2)}) collective-permute-start(bf16[256,2048]{1,0:T(8,128)(2,1)} %w0.1), channel_id=1, source_target_pairs={{6,0},{0,2},{2,4},{4,6},{7,1},{1,3},{3,5},{5,7},{14,8},{8,10},{10,... | collective-permute-start | bytes 3145736 | tf_op jit(solution)/shard_map/ppermute | solution.py:341
  118.0 11.3 %collective-permute-start.11 = (bf16[1056,128]{1,0:T(8,128)(2,1)S(1)}, bf16[1056,128]{1,0:T(8,128)(2,1)S(1)}, u32[]{:S(2)}, u32[]{:S(2)}) collective-permute-start(bf16[1056,128]{1,0:T(8,128)(2,1)S(1)} %bundle.3), channel_id=1, source_target_pairs={{480,0},{0,32},{32,64},{64,96},{96,128},{128,160},{160,192},{192,2... | collective-permute-start | bytes 811016 | tf_op jit(solution)/shard_map/ppermute | solution.py:341
  145.0 20.2 %all-to-all-start.4 = ((bf16[4,64,256]{2,1,0:T(8,128)(2,1)}), bf16[4,64,256]{2,1,0:T(8,128)(2,1)S(1)}, u32[]{:S(2)}, u32[]{:S(2)}) async-start(bf16[4,64,256]{2,1,0:T(8,128)(2,1)} %merge.1), calls=%async_computation.4 | async-start | bytes 262144 | tf_op jit(solution)/shard_map/all_to_all | solution.py:436
  168.3 3.9 %collective-permute-start.15 = (f32[32,2048]{1,0:T(8,128)S(1)}, f32[32,2048]{1,0:T(8,128)S(1)}, u32[]{:S(2)}, u32[]{:S(2)}) collective-permute-start(f32[32,2048]{1,0:T(8,128)S(1)} %get-tuple-element.29), channel_id=1, source_target_pairs={{1,0},{0,1},{3,2},{2,3},{5,4},{4,5},{7,6},{6,7},{9,8},{8,9},{11,10... | collective-permute-start | bytes 786440 | tf_op jit(solution)/shard_map/ppermute | solution.py:341
  (5 other events, 25.6 us)

commit v5 on v4

--- a/solution.py
+++ b/solution.py
@@ -27,13 +27,6 @@
 
 def far(*arrays):
     return [pltpu.with_memory_space_constraint(a, pltpu.HBM) for a in arrays]
-
-
-def from_everyone(value, axes):
-    devices = lax.axis_size(axes)
-    return lax.all_to_all(
-        jnp.broadcast_to(value[None], (devices, *value.shape)), axes, 0, 0, tiled=True
-    )
 
 
 def rms_rows(values):
@@ -80,7 +73,7 @@
 
 def project_kernel(place, *refs):
     mine, other = refs[:4], refs[4]
-    pieces, ctx, gain, wk, wv, kg, cos, sa, sb, msg, normed, gate, lat = refs[5:]
+    pieces, ctx, gain, wk, wv, gains, cos, sa, sb, msg, normed, gate, lat = refs[5:]
     rows = lat.shape[0]
     part = mine[0].shape[0]
     for h in range(4):
@@ -110,21 +103,30 @@
     both = jnp.concatenate([x, c], axis=0)
     k = jnp.dot(both, wk[...], preferred_element_type=F32)
     v = jnp.dot(both, wv[...], preferred_element_type=F32)
-    msg[0:rows] = turned(k[:rows], kg[...], cos, sa, sb).astype(BF16)
+    msg[0:rows] = turned(k[:rows], gains[1:2], cos, sa, sb).astype(BF16)
     msg[rows : 2 * rows] = v[:rows].astype(BF16)
-    tail = jnp.concatenate([rms_rows(k[rows:]) * kg[...], v[rows:]], axis=0)
+    tail = jnp.concatenate([rms_rows(k[rows:]) * gains[1:2], v[rows:]], axis=0)
     msg[2 * rows : 2 * rows + 2 * ctx_rows] = tail.astype(BF16)
 
 
-def query_kernel(normed, wq, qg, cos, sa, sb, q_out):
-    rows = normed.shape[0]
-    head_dim = qg.shape[1]
+def query_kernel(normed, wq, gains, cos, sa, sb, q_out, *, chips):
+    head_dim = gains.shape[1]
     q = jnp.dot(normed[...], wq[...], preferred_element_type=F32)
-    for h in range(q.shape[1] // head_dim):
-        qh = turned(q[:, h * head_dim : (h + 1) * head_dim], qg[...], cos, sa, sb)
-        qt = jnp.transpose(qh).astype(BF16)
-        for i in range(q_out.shape[0]):
-            q_out[i, :, h * rows : (h + 1) * rows] = qt
+    heads = [
+        turned(q[:, h : h + head_dim], gains[0:1], cos, sa, sb)
+        for h in range(0, q.shape[1], head_dim)
+    ]
+    part = q.shape[0] // chips
+    rows = [v[i * part : (i + 1) * part] for i in range(chips) for v in heads]
+    qt = jnp.transpose(jnp.concatenate(rows, axis=0)).astype(BF16)
+    for i in range(q_out.shape[0]):
+        q_out[i] = qt
+
+
+def spread_kernel(blocks, out):
+    total = functools.reduce(jnp.add, [blocks[i] for i in range(blocks.shape[0])])
+    for i in range(out.shape[0]):
+        out[i] = total
 
 
 def bundle_kernel(*refs, groups):
@@ -209,9 +211,12 @@
             at = slice(w * width, (w + 1) * width)
             if last:
                 (out,) = refs
-                dim = acc.shape[0]
-                out[wide * i + w, 0:dim] = acc[:, at].astype(BF16)
-                out[wide * i + w, dim : dim + 16] = packed[:, at].astype(BF16)
+                dim, lanes = acc.shape[0], out.shape[2]
+                for n in range(width // lanes):
+                    at = slice(w * width + n * lanes, w * width + (n + 1) * lanes)
+                    to = (wide * i + w) * (width // lanes) + n
+                    out[to, 0:dim] = acc[:, at].astype(BF16)
+                    out[to, dim : dim + 16] = packed[:, at].astype(BF16)
             else:
                 m_out, l_out, acc_out = refs
                 m_out[wide * i + w] = largest[:, at]
@@ -228,13 +233,13 @@
     )
 
 
-def attend(q_all, bundles, carry, last, keys, extra, factor, lift):
+def attend(q_all, bundles, carry, last, keys, extra, factor, lift, chips):
     parts, dim, width = q_all.shape
     first = carry is None
     counts = tuple(b.shape[0] // (2 * (keys + extra)) for b in bundles)
     operands = [q_all, *bundles] + ([] if first else list(carry))
     if last:
-        out_shape = (jax.ShapeDtypeStruct((parts, dim + 16, width), BF16),)
+        out_shape = (jax.ShapeDtypeStruct((parts * chips, dim + 16, width // chips), BF16),)
     else:
         out_shape = (
             pltpu.VMEM((parts, 1, width), F32),
@@ -267,39 +272,34 @@
     )(*near(*operands))
 
 
-def merge_kernel(parts, out):
-    count, rows, _ = parts.shape
-    dim = rows - 16
-    tail = [parts[i, dim : dim + 16].astype(F32) for i in range(count)]
-    lse = [t[0:1] + t[1:2] + t[2:3] for t in tail]
-    top = functools.reduce(jnp.maximum, lse)
-    share = [jnp.exp2(v - top) for v in lse]
-    whole = functools.reduce(jnp.add, share)
-    merged = functools.reduce(
-        jnp.add, [parts[i, 0:dim].astype(F32) * share[i] for i in range(count)]
-    )
-    merged = merged / whole
-    heads = out.shape[2] // dim
-    chips, part = out.shape[0], out.shape[1]
-    for h in range(heads):
-        turn = jnp.transpose(merged[:, h * chips * part : (h + 1) * chips * part]).astype(BF16)
-        for i in range(chips):
-            out[i, :, h * dim : (h + 1) * dim] = turn[i * part : (i + 1) * part]
-
-
-def out_kernel(place, attended, w0, w1, w2, w3, mine, other, both, held, done):
+def out_kernel(place, parts, w0, w1, w2, w3, mine, other, both, held, done):
     copies = [
         pltpu.make_async_copy(w, held.at[h], done.at[h]) for h, w in enumerate((w0, w1, w2, w3))
     ]
     for copy in copies:
         copy.start()
+    chips = len(copies)
+    dim = parts.shape[1] - 16
+    rows = mine.shape[0]
     for h, copy in enumerate(copies):
-        chip = jax.lax.rem(place[0] + h, 4)
+        chip = jax.lax.rem(place[0] + h, chips)
+        group = [y * chips + chip for y in range(parts.shape[0] // chips)]
+        tail = [parts[i, dim : dim + 16].astype(F32) for i in group]
+        lse = [t[0:1] + t[1:2] + t[2:3] for t in tail]
+        top = functools.reduce(jnp.maximum, lse)
+        share = [jnp.exp2(v - top) for v in lse]
+        whole = functools.reduce(jnp.add, share)
+        merged = functools.reduce(
+            jnp.add, [parts[i, 0:dim].astype(F32) * s for i, s in zip(group, share)]
+        )
+        turn = jnp.transpose(merged / whole)
+        attended = jnp.concatenate(
+            [turn[at : at + 2 * rows] for at in range(0, turn.shape[0], 2 * rows)], axis=1
+        ).astype(BF16)
         copy.wait()
-        partial = jnp.dot(attended[chip], held[h], preferred_element_type=F32)
+        partial = jnp.dot(attended, held[h], preferred_element_type=F32)
         partial = partial.astype(BF16).astype(F32)
         both[...] = partial if h == 0 else both[...] + partial
-    rows = mine.shape[0]
     mine[...] = both[pl.ds(pl.multiple_of(place[1] * rows, rows), rows)]
     other[...] = both[pl.ds(pl.multiple_of((1 - place[1]) * rows, rows), rows)]
 
@@ -340,7 +340,9 @@
         size = lax.axis_size(axis)
         return lax.ppermute(value, axis, [((i + hop) % size, i) for i in range(size)])
 
+    chips = lax.axis_size("x")
     whole = pl.BlockSpec(memory_space=pltpu.VMEM)
+    gains = jnp.stack([query_gain, key_gain])
     partial_mod = pl.pallas_call(
         modulation_kernel,
         in_specs=[whole] * 5,
@@ -350,8 +352,15 @@
         name="modulation",
     )(*far(condition[None], context_condition[None], w_shift, w_scale, w_gate))
     partial_mod = lax.all_to_all(partial_mod, "z", 0, 0, tiled=True)
-    partial_mod = partial_mod.sum(axis=0)
-    pieces = from_everyone(partial_mod, ("y", *TP))
+    partial_mod = pl.pallas_call(
+        spread_kernel,
+        in_specs=[whole],
+        out_specs=whole,
+        out_shape=jax.ShapeDtypeStruct((y_count * tp_count, *partial_mod.shape[1:]), F32),
+        compiler_params=room(4),
+        name="spread",
+    )(*near(partial_mod))
+    pieces = lax.all_to_all(partial_mod, ("y", *TP), 0, 0, tiled=True)
     mine = [latent] + [receive(latent, "x", h) for h in (1, 2, 3)]
     other = jnp.concatenate(mine, axis=0)
     other = receive(other, "c", 1)
@@ -387,14 +396,14 @@
             pre_gain[None],
             w_key,
             w_value,
-            key_gain[None],
+            gains,
             cos,
             sa,
             sb,
         ),
     )
     query = pl.pallas_call(
-        query_kernel,
+        functools.partial(query_kernel, chips=chips),
         in_specs=[whole] * 6,
         out_specs=whole,
         out_shape=jax.ShapeDtypeStruct((y_count, head_dim, heads_dev * tok_dev), BF16),
@@ -405,7 +414,7 @@
         ),
         compiler_params=room(16),
         name="query",
-    )(*near(normed, w_query, query_gain[None], cos, sa, sb))
+    )(*near(normed, w_query, gains, cos, sa, sb))
 
     far_up, far_down = receive(message, "z", 6), receive(message, "z", -5)
     up, down = receive(message, "z", 1), receive(message, "z", -1)
@@ -418,22 +427,11 @@
     last_ups = receive(ups, "z", 1)
     (to_up,) = bundled([downs], ((0,),), 2 * msg_rows)
     last_downs = receive(to_up, "z", -1)
-    shared = (tok_dev, ctx_dev, factor, lift)
+    shared = (tok_dev, ctx_dev, factor, lift, chips)
     carry = attend(q_all, [message, up, down, far_up, far_down], None, False, *shared)
     carry = attend(q_all, [ups, downs], carry, False, *shared)
     (partials,) = attend(q_all, [last_ups, last_downs], carry, True, *shared)
-    returned = lax.all_to_all(partials, "y", 0, 0, tiled=True)
-    attended = pl.pallas_call(
-        merge_kernel,
-        in_specs=[whole],
-        out_specs=whole,
-        out_shape=jax.ShapeDtypeStruct(
-            (lax.axis_size("x"), tok_dev // lax.axis_size("x"), heads_dev * head_dim), BF16
-        ),
-        compiler_params=room(16),
-        name="merge",
-    )(*near(returned))
-    attended = lax.all_to_all(attended, "x", 0, 0, tiled=True)
+    returned = lax.all_to_all(partials, ("y", "x"), 0, 0, tiled=True)
     rows = latent.shape[0]
     sums, others = pl.pallas_call(
         out_kernel,
@@ -456,7 +454,7 @@
             transcendentals=0,
         ),
         name="out",
-    )(place, *near(attended), *far(*w_outs))
+    )(place, *near(returned), *far(*w_outs))
     others = receive(others, "c", 1)
     return pl.pallas_call(
         final_kernel,

time: 174 us -> 180 us (1.034)
  waiting for transfers between devices: 49.2 us -> 63.8 us
  blocking collectives: 10.5 us -> 0 us
  starting transfers between devices: 86.3 us -> 90.3 us
  local copies, waits for them, and re-layouts: 2.01 us -> 0.04 us
    ppermute x16, waiting for transfers between devices: 32.3 us -> 42.9 us  [receive(): lax.ppermute(value, axis, [((i + hop) % size, i) for i in range(size)])]
    all_to_all x1 -> x0, blocking collectives: 10.5 us -> none  [body(): returned = lax.all_to_all(partials, 'y', 0, 0, tiled=True)]
    ppermute x16, starting transfers between devices: 53.5 us -> 58.3 us  [receive(): lax.ppermute(value, axis, [((i + hop) % size, i) for i in range(size)])]
    all_to_all x2, waiting for transfers between devices: 8.8 us -> 13.4 us  [the longest x1 8.77 us: body(): pieces = lax.all_to_all(partial_mod, ('y', *TP), 0, 0, tiled=True)]
  transfers between devices with their start and end apart: 20 -> 20, of which waited for: 9 -> 10; matrix products, arithmetic and copies ran while one was open for 1% -> 0% of each run, Pallas kernels for 10% -> 10%
where the time goes in v5:
time: 180 us; the launch traced here: 179 us
  starting transfers between devices  90.3 us (50%)
  waiting for transfers between devices  63.8 us (35%)
  Pallas kernels  23.9 us (13%)
    ppermute x16, starting transfers between devices, receive(): lax.ppermute(value, axis, [((i + hop) % size, i) for i in range(size)])  58.3 us
    ppermute x16, waiting for transfers between devices, receive(): lax.ppermute(value, axis, [((i + hop) % size, i) for i in range(size)])  42.9 us
    all_to_all x1, starting transfers between devices, body(): partial_mod = lax.all_to_all(partial_mod, 'z', 0, 0, tiled=True)  15 us
    pallas_call x3, Pallas kernels, attend(): pl.pallas_call(functools.partial(attend_kernel, counts=counts, keys=keys,...  14.2 us
    all_to_all x1, waiting for transfers between devices, body(): pieces = lax.all_to_all(partial_mod, ('y', *TP), 0, 0, tiled=True)  8.77 us
    all_to_all x1, starting transfers between devices, body(): pieces = lax.all_to_all(partial_mod, ('y', *TP), 0, 0, tiled=True)  8.67 us
    all_to_all x1, waiting for transfers between devices, body(): partial_mod = lax.all_to_all(partial_mod, 'z', 0, 0, tiled=True)  7.53 us
    all_to_all x1, starting transfers between devices, body(): returned = lax.all_to_all(partials, ('y', 'x'), 0, 0, tiled=True)  4.8 us
  transfers between devices with their start and end apart: 20, of which 10 were waited for; matrix products, arithmetic and copies ran while one was open for 0% of the time, Pallas kernels for 10%

profile of v5, /device:TPU:1, one launch (start us, length us, event | category | flops | bytes accessed | tf_op | source)
XLA Modules:
  0.0 179.1 jit_solution(8752548695371376907)
XLA Ops:
  0.0 3.9 %collective-permute-start.2 = (bf16[32,2048]{1,0:T(8,128)(2,1)}, bf16[32,2048]{1,0:T(8,128)(2,1)S(1)}, u32[]{:S(2)}, u32[]{:S(2)}) collective-permute-start(bf16[32,2048]{1,0:T(8,128)(2,1)} %latent.1), channel_id=1, source_target_pairs={{6,0},{0,2},{2,4},{4,6},{7,1},{1,3},{3,5},{5,7},{14,8},{8,10},{10,... | collective-permute-start | bytes 393224 | tf_op jit(solution)/shard_map/ppermute | solution.py:341
  3.9 4.4 %collective-permute-start.1 = (bf16[32,2048]{1,0:T(8,128)(2,1)}, bf16[32,2048]{1,0:T(8,128)(2,1)S(1)}, u32[]{:S(2)}, u32[]{:S(2)}) collective-permute-start(bf16[32,2048]{1,0:T(8,128)(2,1)} %latent.1), channel_id=1, source_target_pairs={{4,0},{6,2},{0,4},{2,6},{5,1},{7,3},{1,5},{3,7},{12,8},{14,10},{8,... | collective-permute-start | bytes 393224 | tf_op jit(solution)/shard_map/ppermute | solution.py:341
  8.3 3.1 %collective-permute-start = (bf16[32,2048]{1,0:T(8,128)(2,1)}, bf16[32,2048]{1,0:T(8,128)(2,1)S(1)}, u32[]{:S(2)}, u32[]{:S(2)}) collective-permute-start(bf16[32,2048]{1,0:T(8,128)(2,1)} %latent.1), channel_id=1, source_target_pairs={{2,0},{4,2},{6,4},{0,6},{3,1},{5,3},{7,5},{1,7},{10,8},{12,10},{14... | collective-permute-start | bytes 393224 | tf_op jit(solution)/shard_map/ppermute | solution.py:341
  13.0 15.0 %all-to-all-start = ((f32[16,5,256]{2,1,0:T(8,128)}), f32[16,5,256]{2,1,0:T(8,128)S(1)}, u32[]{:S(2)}, u32[]{:S(2)}) async-start(f32[16,5,256]{2,1,0:T(8,128)} %modulation.1), calls=%async_computation | async-start | bytes 262144 | tf_op jit(solution)/shard_map/all_to_all | solution.py:354
  28.1 3.7 %collective-permute-start.3 = (bf16[128,2048]{1,0:T(8,128)(2,1)S(1)}, bf16[128,2048]{1,0:T(8,128)(2,1)S(1)}, u32[]{:S(2)}, u32[]{:S(2)}) collective-permute-start(bf16[128,2048]{1,0:T(8,128)(2,1)S(1)} %pad_maximum_fusion), channel_id=1, source_target_pairs={{1,0},{0,1},{3,2},{2,3},{5,4},{4,5},{7,6},{6,7},{9,8},{8,9},{11,10... | collective-permute-start | bytes 1572872 | tf_op jit(solution)/shard_map/ppermute | solution.py:341
  32.5 7.5 %all-to-all-done.blocks = f32[16,5,256]{2,1,0:T(8,128)S(1)} async-done(((f32[16,5,256]{2,1,0:T(8,128)}), f32[16,5,256]{2,1,0:T(8,128)S(1)}, u32[]{:S(2)}, u32[]{:S(2)}) %all-to-all-start) | async-done | bytes 81952 | tf_op jit(solution)/shard_map/all_to_all | solution.py:354
  40.7 8.7 %all-to-all-start.1 = ((f32[32,5,256]{2,1,0:T(8,128)}), f32[32,5,256]{2,1,0:T(8,128)S(1)}, u32[]{:S(2)}, u32[]{:S(2)}) async-start(f32[32,5,256]{2,1,0:T(8,128)} %spread.1), calls=%async_computation.1 | async-start | bytes 524288 | tf_op jit(solution)/shard_map/all_to_all | solution.py:363
  49.5 8.8 %all-to-all-done.1.refs_5_ = f32[32,5,256]{2,1,0:T(8,128)S(1)} async-done(((f32[32,5,256]{2,1,0:T(8,128)}), f32[32,5,256]{2,1,0:T(8,128)S(1)}, u32[]{:S(2)}, u32[]{:S(2)}) %all-to-all-start.1) | async-done | bytes 163872 | tf_op jit(solution)/shard_map/all_to_all | solution.py:363
  62.6 3.5 %collective-permute-start.6 = (bf16[528,128]{1,0:T(8,128)(2,1)S(1)}, bf16[528,128]{1,0:T(8,128)(2,1)S(1)}, u32[]{:S(2)}, u32[]{:S(2)}) collective-permute-start(bf16[528,128]{1,0:T(8,128)(2,1)S(1)} %get-tuple-element.19.refs_1_), channel_id=1, source_target_pairs={{352,0},{384,32},{416,64},{448,96},{480,128},{0,160},{32,192},{64,... | collective-permute-start | bytes 405512 | tf_op jit(solution)/shard_map/ppermute | solution.py:341
  66.1 8.4 %collective-permute-start.5 = (bf16[528,128]{1,0:T(8,128)(2,1)S(1)}, bf16[528,128]{1,0:T(8,128)(2,1)S(1)}, u32[]{:S(2)}, u32[]{:S(2)}) collective-permute-start(bf16[528,128]{1,0:T(8,128)(2,1)S(1)} %get-tuple-element.19.refs_1_), channel_id=1, source_target_pairs={{192,0},{224,32},{256,64},{288,96},{320,128},{352,160},{384,192},{... | collective-permute-start | bytes 405512 | tf_op jit(solution)/shard_map/ppermute | solution.py:341
  77.1 5.9 %collective-permute-done.6.refs_2_.refs_5_ = bf16[528,128]{1,0:T(8,128)(2,1)S(1)} collective-permute-done((bf16[528,128]{1,0:T(8,128)(2,1)S(1)}, bf16[528,128]{1,0:T(8,128)(2,1)S(1)}, u32[]{:S(2)}, u32[]{:S(2)}) %collective-permute-start.6) | collective-permute-done | bytes 135200 | tf_op jit(solution)/shard_map/ppermute | solution.py:341
  83.1 9.2 %collective-permute-done.5.refs_1_.refs_4_ = bf16[528,128]{1,0:T(8,128)(2,1)S(1)} collective-permute-done((bf16[528,128]{1,0:T(8,128)(2,1)S(1)}, bf16[528,128]{1,0:T(8,128)(2,1)S(1)}, u32[]{:S(2)}, u32[]{:S(2)}) %collective-permute-start.5) | collective-permute-done | bytes 135200 | tf_op jit(solution)/shard_map/ppermute | solution.py:341
  95.1 4.9 %collective-permute-start.8 = (bf16[1584,128]{1,0:T(8,128)(2,1)S(1)}, bf16[1584,128]{1,0:T(8,128)(2,1)S(1)}, u32[]{:S(2)}, u32[]{:S(2)}) collective-permute-start(bf16[1584,128]{1,0:T(8,128)(2,1)S(1)} %get-tuple-element.20), channel_id=1, source_target_pairs={{32,0},{64,32},{96,64},{128,96},{160,128},{192,160},{224,192},{256... | collective-permute-start | bytes 1216520 | tf_op jit(solution)/shard_map/ppermute | solution.py:341
  103.6 3.5 %all-to-all-start.2 = ((bf16[4,128,512]{2,1,0:T(8,128)(2,1)}), bf16[4,128,512]{2,1,0:T(8,128)(2,1)S(1)}, u32[]{:S(2)}, u32[]{:S(2)}) async-start(bf16[4,128,512]{2,1,0:T(8,128)(2,1)} %query.1), calls=%async_computation.2 | async-start | bytes 1048576 | tf_op jit(solution)/shard_map/all_to_all | solution.py:421
  108.2 5.3 %collective-permute-start.9 = (bf16[1584,128]{1,0:T(8,128)(2,1)S(1)}, bf16[1584,128]{1,0:T(8,128)(2,1)S(1)}, u32[]{:S(2)}, u32[]{:S(2)}) collective-permute-start(bf16[1584,128]{1,0:T(8,128)(2,1)S(1)} %collective-permute-done.8.refs_1_), channel_id=1, source_target_pairs={{32,0},{64,32},{96,64},{128,96},{160,128},{192,160},{224,192},{256... | collective-permute-start | bytes 1216520 | tf_op jit(solution)/shard_map/ppermute | solution.py:341
  116.1 4.1 %collective-permute-start.12 = (bf16[256,2048]{1,0:T(8,128)(2,1)}, bf16[256,2048]{1,0:T(8,128)(2,1)}, u32[]{:S(2)}, u32[]{:S(2)}) collective-permute-start(bf16[256,2048]{1,0:T(8,128)(2,1)} %w0.1), channel_id=1, source_target_pairs={{2,0},{4,2},{6,4},{0,6},{3,1},{5,3},{7,5},{1,7},{10,8},{12,10},{14... | collective-permute-start | bytes 3145736 | tf_op jit(solution)/shard_map/ppermute | solution.py:341
  124.3 4.2 %attend.3 = (f32[4,1,512]{2,1,0:T(1,128)S(1)}, f32[4,1,512]{2,1,0:T(1,128)S(1)}, f32[4,128,512]{2,1,0:T(8,128)S(1)}) custom-call(bf16[4,128,512]{2,1,0:T(8,128)(2,1)S(1)} %all-to-all-done.2.refs_0_, bf16[528,128]{1,0:T(8,128)(2,1)S(1)} %get-tuple-element.19.refs_1_, bf16[528,128]{1,0:T(8,128)(2,1)S(1)} %collective-permute-done.4.refs_0_.refs_2_, ...), custom_call_target="tpu_custom_call" | custom-call | flops 1384120320 | bytes 2097152 | tf_op jit(solution)/shard_map/attend/pallas_call | solution.py:251
  128.5 4.9 %attend.4 = (f32[4,1,512]{2,1,0:T(1,128)S(1)}, f32[4,1,512]{2,1,0:T(1,128)S(1)}, f32[4,128,512]{2,1,0:T(8,128)S(1)}) custom-call(bf16[4,128,512]{2,1,0:T(8,128)(2,1)S(1)} %all-to-all-done.2.refs_0_, bf16[1584,128]{1,0:T(8,128)(2,1)S(1)} %collective-permute-done.8.refs_1_, bf16[1584,128]{1,0:T(8,128)(2,1)S(1)} %collective-permute-done.10.refs_0_.refs_2_, ...), custom_call_target="tpu_custom_call" | custom-call | flops 1660944384 | bytes 2097152 | tf_op jit(solution)/shard_map/attend/pallas_call | solution.py:251
  133.5 5.0 %attend.5 = bf16[16,144,128]{2,1,0:T(8,128)(2,1)} custom-call(bf16[4,128,512]{2,1,0:T(8,128)(2,1)S(1)} %all-to-all-done.2.refs_0_, bf16[1584,128]{1,0:T(8,128)(2,1)S(1)} %collective-permute-done.9.refs_1_, bf16[1056,128]{1,0:T(8,128)(2,1)S(1)} %collective-permute-done.11.refs_2_, f32[4,1,512]{2,1,0:T(1,128)S(1)} %get-tuple-element.25.refs_3_, ...), custom_call_target="tpu_custom_call" | custom-call | flops 1384120320 | bytes 2097152 | tf_op jit(solution)/shard_map/attend/pallas_call | solution.py:251
  138.5 4.8 %all-to-all-start.3 = ((bf16[16,144,128]{2,1,0:T(8,128)(2,1)}), bf16[16,144,128]{2,1,0:T(8,128)(2,1)S(1)}, u32[]{:S(2)}, u32[]{:S(2)}) async-start(bf16[16,144,128]{2,1,0:T(8,128)(2,1)} %attend.5), calls=%async_computation.3 | async-start | bytes 1179648 | tf_op jit(solution)/shard_map/all_to_all | solution.py:434
  143.3 20.2 %collective-permute-done.12.w1 = bf16[256,2048]{1,0:T(8,128)(2,1)} collective-permute-done((bf16[256,2048]{1,0:T(8,128)(2,1)}, bf16[256,2048]{1,0:T(8,128)(2,1)}, u32[]{:S(2)}, u32[]{:S(2)}) %collective-permute-start.12) | collective-permute-done | bytes 1048608 | tf_op jit(solution)/shard_map/ppermute | solution.py:341
  166.0 4.6 %all-to-all-done.3.parts = bf16[16,144,128]{2,1,0:T(8,128)(2,1)S(1)} async-done(((bf16[16,144,128]{2,1,0:T(8,128)(2,1)}), bf16[16,144,128]{2,1,0:T(8,128)(2,1)S(1)}, u32[]{:S(2)}, u32[]{:S(2)}) %all-to-all-start.3) | async-done | bytes 589856 | tf_op jit(solution)/shard_map/all_to_all | solution.py:434
  170.6 3.1 %out.1 = (f32[32,2048]{1,0:T(8,128)S(1)}, f32[32,2048]{1,0:T(8,128)S(1)}) custom-call(s32[2]{0:T(128)S(1)} %pad_add_fusion.place, bf16[16,144,128]{2,1,0:T(8,128)(2,1)S(1)} %all-to-all-done.3.parts, bf16[256,2048]{1,0:T(8,128)(2,1)} %w0.1, bf16[256,2048]{1,0:T(8,128)(2,1)} %collective-permute-done.12.w1, bf16[256,2048]{1,0:T(8,128)(2,1)} %collective-permute-done.13.w2, ...), custom_call_target="tpu_custom_call" | custom-call | flops 268435456 | bytes 2097152 | tf_op jit(solution)/shard_map/out/pallas_call | solution.py:436
  173.7 3.5 %collective-permute-start.15 = (f32[32,2048]{1,0:T(8,128)S(1)}, f32[32,2048]{1,0:T(8,128)S(1)}, u32[]{:S(2)}, u32[]{:S(2)}) collective-permute-start(f32[32,2048]{1,0:T(8,128)S(1)} %get-tuple-element.29), channel_id=1, source_target_pairs={{1,0},{0,1},{3,2},{2,3},{5,4},{4,5},{7,6},{6,7},{9,8},{8,9},{11,10... | collective-permute-start | bytes 786440 | tf_op jit(solution)/shard_map/ppermute | solution.py:341
  (52 shorter events, 28.5 us)
Async XLA Ops:
  0.0 28.1 %collective-permute-start.2 = (bf16[32,2048]{1,0:T(8,128)(2,1)}, bf16[32,2048]{1,0:T(8,128)(2,1)S(1)}, u32[]{:S(2)}, u32[]{:S(2)}) collective-permute-start(bf16[32,2048]{1,0:T(8,128)(2,1)} %latent.1), channel_id=1, source_target_pairs={{6,0},{0,2},{2,4},{4,6},{7,1},{1,3},{3,5},{5,7},{14,8},{8,10},{10,... | collective-permute-start | bytes 393224 | tf_op jit(solution)/shard_map/ppermute | solution.py:341
  3.9 24.1 %collective-permute-start.1 = (bf16[32,2048]{1,0:T(8,128)(2,1)}, bf16[32,2048]{1,0:T(8,128)(2,1)S(1)}, u32[]{:S(2)}, u32[]{:S(2)}) collective-permute-start(bf16[32,2048]{1,0:T(8,128)(2,1)} %latent.1), channel_id=1, source_target_pairs={{4,0},{6,2},{0,4},{2,6},{5,1},{7,3},{1,5},{3,7},{12,8},{14,10},{8,... | collective-permute-start | bytes 393224 | tf_op jit(solution)/shard_map/ppermute | solution.py:341
  8.3 19.8 %collective-permute-start = (bf16[32,2048]{1,0:T(8,128)(2,1)}, bf16[32,2048]{1,0:T(8,128)(2,1)S(1)}, u32[]{:S(2)}, u32[]{:S(2)}) collective-permute-start(bf16[32,2048]{1,0:T(8,128)(2,1)} %latent.1), channel_id=1, source_target_pairs={{2,0},{4,2},{6,4},{0,6},{3,1},{5,3},{7,5},{1,7},{10,8},{12,10},{14... | collective-permute-start | bytes 393224 | tf_op jit(solution)/shard_map/ppermute | solution.py:341
  13.0 27.0 %all-to-all-start = ((f32[16,5,256]{2,1,0:T(8,128)}), f32[16,5,256]{2,1,0:T(8,128)S(1)}, u32[]{:S(2)}, u32[]{:S(2)}) async-start(f32[16,5,256]{2,1,0:T(8,128)} %modulation.1), calls=%async_computation | async-start | bytes 262144 | tf_op jit(solution)/shard_map/all_to_all | solution.py:354
  28.1 30.1 %collective-permute-start.3 = (bf16[128,2048]{1,0:T(8,128)(2,1)S(1)}, bf16[128,2048]{1,0:T(8,128)(2,1)S(1)}, u32[]{:S(2)}, u32[]{:S(2)}) collective-permute-start(bf16[128,2048]{1,0:T(8,128)(2,1)S(1)} %pad_maximum_fusion), channel_id=1, source_target_pairs={{1,0},{0,1},{3,2},{2,3},{5,4},{4,5},{7,6},{6,7},{9,8},{8,9},{11,10... | collective-permute-start | bytes 1572872 | tf_op jit(solution)/shard_map/ppermute | solution.py:341
  31.9 26.4 %copy-start.3 = (bf16[2048,128]{1,0:T(8,128)(2,1)S(1)}, bf16[2048,128]{1,0:T(8,128)(2,1)}, u32[]{:S(2)}) copy-start(bf16[2048,128]{1,0:T(8,128)(2,1)} %refs_9_.1) | copy-start | bytes 1572868
  32.4 25.8 %copy-start.2 = (bf16[2048,128]{1,0:T(8,128)(2,1)S(1)}, bf16[2048,128]{1,0:T(8,128)(2,1)}, u32[]{:S(2)}) copy-start(bf16[2048,128]{1,0:T(8,128)(2,1)} %refs_8_.1) | copy-start | bytes 1572868
  40.7 17.6 %copy-start.4 = (bf16[8,2048]{1,0:T(8,128)(2,1)S(1)}, bf16[8,2048]{1,0:T(8,128)(2,1)}, u32[]{:S(2)}) copy-start(bf16[8,2048]{1,0:T(8,128)(2,1)} %refs_6_.1) | copy-start | bytes 98308
  40.7 17.6 %all-to-all-start.1 = ((f32[32,5,256]{2,1,0:T(8,128)}), f32[32,5,256]{2,1,0:T(8,128)S(1)}, u32[]{:S(2)}, u32[]{:S(2)}) async-start(f32[32,5,256]{2,1,0:T(8,128)} %spread.1), calls=%async_computation.1 | async-start | bytes 524288 | tf_op jit(solution)/shard_map/all_to_all | solution.py:363
  58.3 43.7 %copy-start.1 = (bf16[2048,256]{1,0:T(8,128)(2,1)S(1)}, bf16[2048,256]{1,0:T(8,128)(2,1)}, u32[]{:S(2)}) copy-start(bf16[2048,256]{1,0:T(8,128)(2,1)} %wq.1) | copy-start | bytes 3145732
  60.1 17.0 %collective-permute-start.7 = (bf16[528,128]{1,0:T(8,128)(2,1)S(1)}, bf16[528,128]{1,0:T(8,128)(2,1)S(1)}, u32[]{:S(2)}, u32[]{:S(2)}) collective-permute-start(bf16[528,128]{1,0:T(8,128)(2,1)S(1)} %get-tuple-element.19.refs_1_), channel_id=1, source_target_pairs={{480,0},{0,32},{32,64},{64,96},{96,128},{128,160},{160,192},{192,2... | collective-permute-start | bytes 405512 | tf_op jit(solution)/shard_map/ppermute | solution.py:341
  62.6 20.4 %collective-permute-start.6 = (bf16[528,128]{1,0:T(8,128)(2,1)S(1)}, bf16[528,128]{1,0:T(8,128)(2,1)S(1)}, u32[]{:S(2)}, u32[]{:S(2)}) collective-permute-start(bf16[528,128]{1,0:T(8,128)(2,1)S(1)} %get-tuple-element.19.refs_1_), channel_id=1, source_target_pairs={{352,0},{384,32},{416,64},{448,96},{480,128},{0,160},{32,192},{64,... | collective-permute-start | bytes 405512 | tf_op jit(solution)/shard_map/ppermute | solution.py:341
  66.1 26.1 %collective-permute-start.5 = (bf16[528,128]{1,0:T(8,128)(2,1)S(1)}, bf16[528,128]{1,0:T(8,128)(2,1)S(1)}, u32[]{:S(2)}, u32[]{:S(2)}) collective-permute-start(bf16[528,128]{1,0:T(8,128)(2,1)S(1)} %get-tuple-element.19.refs_1_), channel_id=1, source_target_pairs={{192,0},{224,32},{256,64},{288,96},{320,128},{352,160},{384,192},{... | collective-permute-start | bytes 405512 | tf_op jit(solution)/shard_map/ppermute | solution.py:341
  74.5 20.5 %collective-permute-start.4 = (bf16[528,128]{1,0:T(8,128)(2,1)S(1)}, bf16[528,128]{1,0:T(8,128)(2,1)S(1)}, u32[]{:S(2)}, u32[]{:S(2)}) collective-permute-start(bf16[528,128]{1,0:T(8,128)(2,1)S(1)} %get-tuple-element.19.refs_1_), channel_id=1, source_target_pairs={{32,0},{64,32},{96,64},{128,96},{160,128},{192,160},{224,192},{256... | collective-permute-start | bytes 405512 | tf_op jit(solution)/shard_map/ppermute | solution.py:341
  95.1 13.1 %collective-permute-start.8 = (bf16[1584,128]{1,0:T(8,128)(2,1)S(1)}, bf16[1584,128]{1,0:T(8,128)(2,1)S(1)}, u32[]{:S(2)}, u32[]{:S(2)}) collective-permute-start(bf16[1584,128]{1,0:T(8,128)(2,1)S(1)} %get-tuple-element.20), channel_id=1, source_target_pairs={{32,0},{64,32},{96,64},{128,96},{160,128},{192,160},{224,192},{256... | collective-permute-start | bytes 1216520 | tf_op jit(solution)/shard_map/ppermute | solution.py:341
  100.1 22.1 %collective-permute-start.10 = (bf16[1584,128]{1,0:T(8,128)(2,1)S(1)}, bf16[1584,128]{1,0:T(8,128)(2,1)S(1)}, u32[]{:S(2)}, u32[]{:S(2)}) collective-permute-start(bf16[1584,128]{1,0:T(8,128)(2,1)S(1)} %get-tuple-element.21), channel_id=1, source_target_pairs={{480,0},{0,32},{32,64},{64,96},{96,128},{128,160},{160,192},{192,2... | collective-permute-start | bytes 1216520 | tf_op jit(solution)/shard_map/ppermute | solution.py:341
  103.6 20.7 %all-to-all-start.2 = ((bf16[4,128,512]{2,1,0:T(8,128)(2,1)}), bf16[4,128,512]{2,1,0:T(8,128)(2,1)S(1)}, u32[]{:S(2)}, u32[]{:S(2)}) async-start(bf16[4,128,512]{2,1,0:T(8,128)(2,1)} %query.1), calls=%async_computation.2 | async-start | bytes 1048576 | tf_op jit(solution)/shard_map/all_to_all | solution.py:421
  108.2 25.3 %collective-permute-start.9 = (bf16[1584,128]{1,0:T(8,128)(2,1)S(1)}, bf16[1584,128]{1,0:T(8,128)(2,1)S(1)}, u32[]{:S(2)}, u32[]{:S(2)}) collective-permute-start(bf16[1584,128]{1,0:T(8,128)(2,1)S(1)} %collective-permute-done.8.refs_1_), channel_id=1, source_target_pairs={{32,0},{64,32},{96,64},{128,96},{160,128},{192,160},{224,192},{256... | collective-permute-start | bytes 1216520 | tf_op jit(solution)/shard_map/ppermute | solution.py:341
  113.5 29.8 %collective-permute-start.13 = (bf16[256,2048]{1,0:T(8,128)(2,1)}, bf16[256,2048]{1,0:T(8,128)(2,1)}, u32[]{:S(2)}, u32[]{:S(2)}) collective-permute-start(bf16[256,2048]{1,0:T(8,128)(2,1)} %w0.1), channel_id=1, source_target_pairs={{4,0},{6,2},{0,4},{2,6},{5,1},{7,3},{1,5},{3,7},{12,8},{14,10},{8,... | collective-permute-start | bytes 3145736 | tf_op jit(solution)/shard_map/ppermute | solution.py:341
  116.1 47.5 %collective-permute-start.12 = (bf16[256,2048]{1,0:T(8,128)(2,1)}, bf16[256,2048]{1,0:T(8,128)(2,1)}, u32[]{:S(2)}, u32[]{:S(2)}) collective-permute-start(bf16[256,2048]{1,0:T(8,128)(2,1)} %w0.1), channel_id=1, source_target_pairs={{2,0},{4,2},{6,4},{0,6},{3,1},{5,3},{7,5},{1,7},{10,8},{12,10},{14... | collective-permute-start | bytes 3145736 | tf_op jit(solution)/shard_map/ppermute | solution.py:341
  120.2 45.8 %collective-permute-start.14 = (bf16[256,2048]{1,0:T(8,128)(2,1)}, bf16[256,2048]{1,0:T(8,128)(2,1)}, u32[]{:S(2)}, u32[]{:S(2)}) collective-permute-start(bf16[256,2048]{1,0:T(8,128)(2,1)} %w0.1), channel_id=1, source_target_pairs={{6,0},{0,2},{2,4},{4,6},{7,1},{1,3},{3,5},{5,7},{14,8},{8,10},{10,... | collective-permute-start | bytes 3145736 | tf_op jit(solution)/shard_map/ppermute | solution.py:341
  122.2 11.3 %collective-permute-start.11 = (bf16[1056,128]{1,0:T(8,128)(2,1)S(1)}, bf16[1056,128]{1,0:T(8,128)(2,1)S(1)}, u32[]{:S(2)}, u32[]{:S(2)}) collective-permute-start(bf16[1056,128]{1,0:T(8,128)(2,1)S(1)} %bundle.3), channel_id=1, source_target_pairs={{480,0},{0,32},{32,64},{64,96},{96,128},{128,160},{160,192},{192,2... | collective-permute-start | bytes 811016 | tf_op jit(solution)/shard_map/ppermute | solution.py:341
  138.5 32.1 %all-to-all-start.3 = ((bf16[16,144,128]{2,1,0:T(8,128)(2,1)}), bf16[16,144,128]{2,1,0:T(8,128)(2,1)S(1)}, u32[]{:S(2)}, u32[]{:S(2)}) async-start(bf16[16,144,128]{2,1,0:T(8,128)(2,1)} %attend.5), calls=%async_computation.3 | async-start | bytes 1179648 | tf_op jit(solution)/shard_map/all_to_all | solution.py:434
  173.7 4.6 %collective-permute-start.15 = (f32[32,2048]{1,0:T(8,128)S(1)}, f32[32,2048]{1,0:T(8,128)S(1)}, u32[]{:S(2)}, u32[]{:S(2)}) collective-permute-start(f32[32,2048]{1,0:T(8,128)S(1)} %get-tuple-element.29), channel_id=1, source_target_pairs={{1,0},{0,1},{3,2},{2,3},{5,4},{4,5},{7,6},{6,7},{9,8},{8,9},{11,10... | collective-permute-start | bytes 786440 | tf_op jit(solution)/shard_map/ppermute | solution.py:341
  (5 other events, 49.3 us)

commit v6 on v5

--- a/solution.py
+++ b/solution.py
@@ -8,6 +8,7 @@
 from jax.experimental.pallas import tpu as pltpu
 from jax.sharding import Mesh
 from jax.sharding import PartitionSpec as P
+
 
 GRID_W = 64
 LOG2E = math.log2(math.e)
@@ -416,10 +417,14 @@
         name="query",
     )(*near(normed, w_query, gains, cos, sa, sb))
 
-    far_up, far_down = receive(message, "z", 6), receive(message, "z", -5)
+    far_up = receive(message, "z", 6)
+    far_down = receive(message, "z", -5)
     up, down = receive(message, "z", 1), receive(message, "z", -1)
     q_all = lax.all_to_all(query, "y", 0, 0, tiled=True)
-    w_outs = [w_out] + [receive(w_out, "x", h) for h in (1, 2, 3)]
+    across = receive(w_out, "x", 2)
+    after = receive(w_out, "x", 1)
+    before = receive(w_out, "x", 3)
+    w_outs = [w_out, after, across, before]
     to_down, to_up = bundled(
         [up, far_up, far_down, down], ((0, 1, 2), (1, 2, 3)), 3 * msg_rows
     )

time: 180 us -> 180 us (level)
  no operation moved by 1% of the time
where the time goes in v6:
time: 180 us; the launch traced here: 179 us
  starting transfers between devices  90.3 us (50%)
  waiting for transfers between devices  63.8 us (35%)
  Pallas kernels  23.9 us (13%)
    ppermute x16, starting transfers between devices, receive(): lax.ppermute(value, axis, [((i + hop) % size, i) for i in range(size)])  58.3 us
    ppermute x16, waiting for transfers between devices, receive(): lax.ppermute(value, axis, [((i + hop) % size, i) for i in range(size)])  42.9 us
    all_to_all x1, starting transfers between devices, body(): partial_mod = lax.all_to_all(partial_mod, 'z', 0, 0, tiled=True)  15 us
    pallas_call x3, Pallas kernels, attend(): pl.pallas_call(functools.partial(attend_kernel, counts=counts, keys=keys,...  14.2 us
    all_to_all x1, waiting for transfers between devices, body(): pieces = lax.all_to_all(partial_mod, ('y', *TP), 0, 0, tiled=True)  8.77 us
    all_to_all x1, starting transfers between devices, body(): pieces = lax.all_to_all(partial_mod, ('y', *TP), 0, 0, tiled=True)  8.67 us
    all_to_all x1, waiting for transfers between devices, body(): partial_mod = lax.all_to_all(partial_mod, 'z', 0, 0, tiled=True)  7.53 us
    all_to_all x1, starting transfers between devices, body(): returned = lax.all_to_all(partials, ('y', 'x'), 0, 0, tiled=True)  4.8 us
  transfers between devices with their start and end apart: 20, of which 10 were waited for; matrix products, arithmetic and copies ran while one was open for 0% of the time, Pallas kernels for 10%

profile of v6, /device:TPU:1, one launch (start us, length us, event | category | flops | bytes accessed | tf_op | source)
XLA Modules:
  0.0 179.1 jit_solution(8752548695371376907)
XLA Ops:
  0.0 3.9 %collective-permute-start.2 = (bf16[32,2048]{1,0:T(8,128)(2,1)}, bf16[32,2048]{1,0:T(8,128)(2,1)S(1)}, u32[]{:S(2)}, u32[]{:S(2)}) collective-permute-start(bf16[32,2048]{1,0:T(8,128)(2,1)} %latent.1), channel_id=1, source_target_pairs={{6,0},{0,2},{2,4},{4,6},{7,1},{1,3},{3,5},{5,7},{14,8},{8,10},{10,... | collective-permute-start | bytes 393224 | tf_op jit(solution)/shard_map/ppermute | solution.py:342
  3.9 4.4 %collective-permute-start.1 = (bf16[32,2048]{1,0:T(8,128)(2,1)}, bf16[32,2048]{1,0:T(8,128)(2,1)S(1)}, u32[]{:S(2)}, u32[]{:S(2)}) collective-permute-start(bf16[32,2048]{1,0:T(8,128)(2,1)} %latent.1), channel_id=1, source_target_pairs={{4,0},{6,2},{0,4},{2,6},{5,1},{7,3},{1,5},{3,7},{12,8},{14,10},{8,... | collective-permute-start | bytes 393224 | tf_op jit(solution)/shard_map/ppermute | solution.py:342
  8.3 3.1 %collective-permute-start = (bf16[32,2048]{1,0:T(8,128)(2,1)}, bf16[32,2048]{1,0:T(8,128)(2,1)S(1)}, u32[]{:S(2)}, u32[]{:S(2)}) collective-permute-start(bf16[32,2048]{1,0:T(8,128)(2,1)} %latent.1), channel_id=1, source_target_pairs={{2,0},{4,2},{6,4},{0,6},{3,1},{5,3},{7,5},{1,7},{10,8},{12,10},{14... | collective-permute-start | bytes 393224 | tf_op jit(solution)/shard_map/ppermute | solution.py:342
  13.0 15.0 %all-to-all-start = ((f32[16,5,256]{2,1,0:T(8,128)}), f32[16,5,256]{2,1,0:T(8,128)S(1)}, u32[]{:S(2)}, u32[]{:S(2)}) async-start(f32[16,5,256]{2,1,0:T(8,128)} %modulation.1), calls=%async_computation | async-start | bytes 262144 | tf_op jit(solution)/shard_map/all_to_all | solution.py:355
  28.1 3.7 %collective-permute-start.3 = (bf16[128,2048]{1,0:T(8,128)(2,1)S(1)}, bf16[128,2048]{1,0:T(8,128)(2,1)S(1)}, u32[]{:S(2)}, u32[]{:S(2)}) collective-permute-start(bf16[128,2048]{1,0:T(8,128)(2,1)S(1)} %pad_maximum_fusion), channel_id=1, source_target_pairs={{1,0},{0,1},{3,2},{2,3},{5,4},{4,5},{7,6},{6,7},{9,8},{8,9},{11,10... | collective-permute-start | bytes 1572872 | tf_op jit(solution)/shard_map/ppermute | solution.py:342
  32.5 7.5 %all-to-all-done.blocks = f32[16,5,256]{2,1,0:T(8,128)S(1)} async-done(((f32[16,5,256]{2,1,0:T(8,128)}), f32[16,5,256]{2,1,0:T(8,128)S(1)}, u32[]{:S(2)}, u32[]{:S(2)}) %all-to-all-start) | async-done | bytes 81952 | tf_op jit(solution)/shard_map/all_to_all | solution.py:355
  40.7 8.7 %all-to-all-start.1 = ((f32[32,5,256]{2,1,0:T(8,128)}), f32[32,5,256]{2,1,0:T(8,128)S(1)}, u32[]{:S(2)}, u32[]{:S(2)}) async-start(f32[32,5,256]{2,1,0:T(8,128)} %spread.1), calls=%async_computation.1 | async-start | bytes 524288 | tf_op jit(solution)/shard_map/all_to_all | solution.py:364
  49.5 8.8 %all-to-all-done.1.refs_5_ = f32[32,5,256]{2,1,0:T(8,128)S(1)} async-done(((f32[32,5,256]{2,1,0:T(8,128)}), f32[32,5,256]{2,1,0:T(8,128)S(1)}, u32[]{:S(2)}, u32[]{:S(2)}) %all-to-all-start.1) | async-done | bytes 163872 | tf_op jit(solution)/shard_map/all_to_all | solution.py:364
  62.6 3.5 %collective-permute-start.6 = (bf16[528,128]{1,0:T(8,128)(2,1)S(1)}, bf16[528,128]{1,0:T(8,128)(2,1)S(1)}, u32[]{:S(2)}, u32[]{:S(2)}) collective-permute-start(bf16[528,128]{1,0:T(8,128)(2,1)S(1)} %get-tuple-element.19.refs_1_), channel_id=1, source_target_pairs={{352,0},{384,32},{416,64},{448,96},{480,128},{0,160},{32,192},{64,... | collective-permute-start | bytes 405512 | tf_op jit(solution)/shard_map/ppermute | solution.py:342
  66.1 8.4 %collective-permute-start.5 = (bf16[528,128]{1,0:T(8,128)(2,1)S(1)}, bf16[528,128]{1,0:T(8,128)(2,1)S(1)}, u32[]{:S(2)}, u32[]{:S(2)}) collective-permute-start(bf16[528,128]{1,0:T(8,128)(2,1)S(1)} %get-tuple-element.19.refs_1_), channel_id=1, source_target_pairs={{192,0},{224,32},{256,64},{288,96},{320,128},{352,160},{384,192},{... | collective-permute-start | bytes 405512 | tf_op jit(solution)/shard_map/ppermute | solution.py:342
  77.1 5.9 %collective-permute-done.6.refs_2_.refs_5_ = bf16[528,128]{1,0:T(8,128)(2,1)S(1)} collective-permute-done((bf16[528,128]{1,0:T(8,128)(2,1)S(1)}, bf16[528,128]{1,0:T(8,128)(2,1)S(1)}, u32[]{:S(2)}, u32[]{:S(2)}) %collective-permute-start.6) | collective-permute-done | bytes 135200 | tf_op jit(solution)/shard_map/ppermute | solution.py:342
  83.1 9.2 %collective-permute-done.5.refs_1_.refs_4_ = bf16[528,128]{1,0:T(8,128)(2,1)S(1)} collective-permute-done((bf16[528,128]{1,0:T(8,128)(2,1)S(1)}, bf16[528,128]{1,0:T(8,128)(2,1)S(1)}, u32[]{:S(2)}, u32[]{:S(2)}) %collective-permute-start.5) | collective-permute-done | bytes 135200 | tf_op jit(solution)/shard_map/ppermute | solution.py:342
  95.1 4.9 %collective-permute-start.8 = (bf16[1584,128]{1,0:T(8,128)(2,1)S(1)}, bf16[1584,128]{1,0:T(8,128)(2,1)S(1)}, u32[]{:S(2)}, u32[]{:S(2)}) collective-permute-start(bf16[1584,128]{1,0:T(8,128)(2,1)S(1)} %get-tuple-element.20), channel_id=1, source_target_pairs={{32,0},{64,32},{96,64},{128,96},{160,128},{192,160},{224,192},{256... | collective-permute-start | bytes 1216520 | tf_op jit(solution)/shard_map/ppermute | solution.py:342
  103.6 3.5 %all-to-all-start.2 = ((bf16[4,128,512]{2,1,0:T(8,128)(2,1)}), bf16[4,128,512]{2,1,0:T(8,128)(2,1)S(1)}, u32[]{:S(2)}, u32[]{:S(2)}) async-start(bf16[4,128,512]{2,1,0:T(8,128)(2,1)} %query.1), calls=%async_computation.2 | async-start | bytes 1048576 | tf_op jit(solution)/shard_map/all_to_all | solution.py:423
  108.2 5.3 %collective-permute-start.9 = (bf16[1584,128]{1,0:T(8,128)(2,1)S(1)}, bf16[1584,128]{1,0:T(8,128)(2,1)S(1)}, u32[]{:S(2)}, u32[]{:S(2)}) collective-permute-start(bf16[1584,128]{1,0:T(8,128)(2,1)S(1)} %collective-permute-done.8.refs_1_), channel_id=1, source_target_pairs={{32,0},{64,32},{96,64},{128,96},{160,128},{192,160},{224,192},{256... | collective-permute-start | bytes 1216520 | tf_op jit(solution)/shard_map/ppermute | solution.py:342
  116.1 4.1 %collective-permute-start.12 = (bf16[256,2048]{1,0:T(8,128)(2,1)}, bf16[256,2048]{1,0:T(8,128)(2,1)}, u32[]{:S(2)}, u32[]{:S(2)}) collective-permute-start(bf16[256,2048]{1,0:T(8,128)(2,1)} %w0.1), channel_id=1, source_target_pairs={{2,0},{4,2},{6,4},{0,6},{3,1},{5,3},{7,5},{1,7},{10,8},{12,10},{14... | collective-permute-start | bytes 3145736 | tf_op jit(solution)/shard_map/ppermute | solution.py:342
  124.3 4.2 %attend.3 = (f32[4,1,512]{2,1,0:T(1,128)S(1)}, f32[4,1,512]{2,1,0:T(1,128)S(1)}, f32[4,128,512]{2,1,0:T(8,128)S(1)}) custom-call(bf16[4,128,512]{2,1,0:T(8,128)(2,1)S(1)} %all-to-all-done.2.refs_0_, bf16[528,128]{1,0:T(8,128)(2,1)S(1)} %get-tuple-element.19.refs_1_, bf16[528,128]{1,0:T(8,128)(2,1)S(1)} %collective-permute-done.4.refs_0_.refs_2_, ...), custom_call_target="tpu_custom_call" | custom-call | flops 1384120320 | bytes 2097152 | tf_op jit(solution)/shard_map/attend/pallas_call | solution.py:252
  128.5 4.9 %attend.4 = (f32[4,1,512]{2,1,0:T(1,128)S(1)}, f32[4,1,512]{2,1,0:T(1,128)S(1)}, f32[4,128,512]{2,1,0:T(8,128)S(1)}) custom-call(bf16[4,128,512]{2,1,0:T(8,128)(2,1)S(1)} %all-to-all-done.2.refs_0_, bf16[1584,128]{1,0:T(8,128)(2,1)S(1)} %collective-permute-done.8.refs_1_, bf16[1584,128]{1,0:T(8,128)(2,1)S(1)} %collective-permute-done.10.refs_0_.refs_2_, ...), custom_call_target="tpu_custom_call" | custom-call | flops 1660944384 | bytes 2097152 | tf_op jit(solution)/shard_map/attend/pallas_call | solution.py:252
  133.5 5.0 %attend.5 = bf16[16,144,128]{2,1,0:T(8,128)(2,1)} custom-call(bf16[4,128,512]{2,1,0:T(8,128)(2,1)S(1)} %all-to-all-done.2.refs_0_, bf16[1584,128]{1,0:T(8,128)(2,1)S(1)} %collective-permute-done.9.refs_1_, bf16[1056,128]{1,0:T(8,128)(2,1)S(1)} %collective-permute-done.11.refs_2_, f32[4,1,512]{2,1,0:T(1,128)S(1)} %get-tuple-element.25.refs_3_, ...), custom_call_target="tpu_custom_call" | custom-call | flops 1384120320 | bytes 2097152 | tf_op jit(solution)/shard_map/attend/pallas_call | solution.py:252
  138.5 4.8 %all-to-all-start.3 = ((bf16[16,144,128]{2,1,0:T(8,128)(2,1)}), bf16[16,144,128]{2,1,0:T(8,128)(2,1)S(1)}, u32[]{:S(2)}, u32[]{:S(2)}) async-start(bf16[16,144,128]{2,1,0:T(8,128)(2,1)} %attend.5), calls=%async_computation.3 | async-start | bytes 1179648 | tf_op jit(solution)/shard_map/all_to_all | solution.py:439
  143.3 20.2 %collective-permute-done.12.w1 = bf16[256,2048]{1,0:T(8,128)(2,1)} collective-permute-done((bf16[256,2048]{1,0:T(8,128)(2,1)}, bf16[256,2048]{1,0:T(8,128)(2,1)}, u32[]{:S(2)}, u32[]{:S(2)}) %collective-permute-start.12) | collective-permute-done | bytes 1048608 | tf_op jit(solution)/shard_map/ppermute | solution.py:342
  166.0 4.6 %all-to-all-done.3.parts = bf16[16,144,128]{2,1,0:T(8,128)(2,1)S(1)} async-done(((bf16[16,144,128]{2,1,0:T(8,128)(2,1)}), bf16[16,144,128]{2,1,0:T(8,128)(2,1)S(1)}, u32[]{:S(2)}, u32[]{:S(2)}) %all-to-all-start.3) | async-done | bytes 589856 | tf_op jit(solution)/shard_map/all_to_all | solution.py:439
  170.6 3.1 %out.1 = (f32[32,2048]{1,0:T(8,128)S(1)}, f32[32,2048]{1,0:T(8,128)S(1)}) custom-call(s32[2]{0:T(128)S(1)} %pad_add_fusion.place, bf16[16,144,128]{2,1,0:T(8,128)(2,1)S(1)} %all-to-all-done.3.parts, bf16[256,2048]{1,0:T(8,128)(2,1)} %w0.1, bf16[256,2048]{1,0:T(8,128)(2,1)} %collective-permute-done.12.w1, bf16[256,2048]{1,0:T(8,128)(2,1)} %collective-permute-done.13.w2, ...), custom_call_target="tpu_custom_call" | custom-call | flops 268435456 | bytes 2097152 | tf_op jit(solution)/shard_map/out/pallas_call | solution.py:441
  173.7 3.5 %collective-permute-start.15 = (f32[32,2048]{1,0:T(8,128)S(1)}, f32[32,2048]{1,0:T(8,128)S(1)}, u32[]{:S(2)}, u32[]{:S(2)}) collective-permute-start(f32[32,2048]{1,0:T(8,128)S(1)} %get-tuple-element.29), channel_id=1, source_target_pairs={{1,0},{0,1},{3,2},{2,3},{5,4},{4,5},{7,6},{6,7},{9,8},{8,9},{11,10... | collective-permute-start | bytes 786440 | tf_op jit(solution)/shard_map/ppermute | solution.py:342
  (52 shorter events, 28.5 us)
Async XLA Ops:
  0.0 28.1 %collective-permute-start.2 = (bf16[32,2048]{1,0:T(8,128)(2,1)}, bf16[32,2048]{1,0:T(8,128)(2,1)S(1)}, u32[]{:S(2)}, u32[]{:S(2)}) collective-permute-start(bf16[32,2048]{1,0:T(8,128)(2,1)} %latent.1), channel_id=1, source_target_pairs={{6,0},{0,2},{2,4},{4,6},{7,1},{1,3},{3,5},{5,7},{14,8},{8,10},{10,... | collective-permute-start | bytes 393224 | tf_op jit(solution)/shard_map/ppermute | solution.py:342
  3.9 24.1 %collective-permute-start.1 = (bf16[32,2048]{1,0:T(8,128)(2,1)}, bf16[32,2048]{1,0:T(8,128)(2,1)S(1)}, u32[]{:S(2)}, u32[]{:S(2)}) collective-permute-start(bf16[32,2048]{1,0:T(8,128)(2,1)} %latent.1), channel_id=1, source_target_pairs={{4,0},{6,2},{0,4},{2,6},{5,1},{7,3},{1,5},{3,7},{12,8},{14,10},{8,... | collective-permute-start | bytes 393224 | tf_op jit(solution)/shard_map/ppermute | solution.py:342
  8.3 19.8 %collective-permute-start = (bf16[32,2048]{1,0:T(8,128)(2,1)}, bf16[32,2048]{1,0:T(8,128)(2,1)S(1)}, u32[]{:S(2)}, u32[]{:S(2)}) collective-permute-start(bf16[32,2048]{1,0:T(8,128)(2,1)} %latent.1), channel_id=1, source_target_pairs={{2,0},{4,2},{6,4},{0,6},{3,1},{5,3},{7,5},{1,7},{10,8},{12,10},{14... | collective-permute-start | bytes 393224 | tf_op jit(solution)/shard_map/ppermute | solution.py:342
  13.0 27.0 %all-to-all-start = ((f32[16,5,256]{2,1,0:T(8,128)}), f32[16,5,256]{2,1,0:T(8,128)S(1)}, u32[]{:S(2)}, u32[]{:S(2)}) async-start(f32[16,5,256]{2,1,0:T(8,128)} %modulation.1), calls=%async_computation | async-start | bytes 262144 | tf_op jit(solution)/shard_map/all_to_all | solution.py:355
  28.1 30.1 %collective-permute-start.3 = (bf16[128,2048]{1,0:T(8,128)(2,1)S(1)}, bf16[128,2048]{1,0:T(8,128)(2,1)S(1)}, u32[]{:S(2)}, u32[]{:S(2)}) collective-permute-start(bf16[128,2048]{1,0:T(8,128)(2,1)S(1)} %pad_maximum_fusion), channel_id=1, source_target_pairs={{1,0},{0,1},{3,2},{2,3},{5,4},{4,5},{7,6},{6,7},{9,8},{8,9},{11,10... | collective-permute-start | bytes 1572872 | tf_op jit(solution)/shard_map/ppermute | solution.py:342
  31.9 26.4 %copy-start.3 = (bf16[2048,128]{1,0:T(8,128)(2,1)S(1)}, bf16[2048,128]{1,0:T(8,128)(2,1)}, u32[]{:S(2)}) copy-start(bf16[2048,128]{1,0:T(8,128)(2,1)} %refs_9_.1) | copy-start | bytes 1572868
  32.4 25.8 %copy-start.2 = (bf16[2048,128]{1,0:T(8,128)(2,1)S(1)}, bf16[2048,128]{1,0:T(8,128)(2,1)}, u32[]{:S(2)}) copy-start(bf16[2048,128]{1,0:T(8,128)(2,1)} %refs_8_.1) | copy-start | bytes 1572868
  40.7 17.6 %copy-start.4 = (bf16[8,2048]{1,0:T(8,128)(2,1)S(1)}, bf16[8,2048]{1,0:T(8,128)(2,1)}, u32[]{:S(2)}) copy-start(bf16[8,2048]{1,0:T(8,128)(2,1)} %refs_6_.1) | copy-start | bytes 98308
  40.7 17.6 %all-to-all-start.1 = ((f32[32,5,256]{2,1,0:T(8,128)}), f32[32,5,256]{2,1,0:T(8,128)S(1)}, u32[]{:S(2)}, u32[]{:S(2)}) async-start(f32[32,5,256]{2,1,0:T(8,128)} %spread.1), calls=%async_computation.1 | async-start | bytes 524288 | tf_op jit(solution)/shard_map/all_to_all | solution.py:364
  58.3 43.7 %copy-start.1 = (bf16[2048,256]{1,0:T(8,128)(2,1)S(1)}, bf16[2048,256]{1,0:T(8,128)(2,1)}, u32[]{:S(2)}) copy-start(bf16[2048,256]{1,0:T(8,128)(2,1)} %wq.1) | copy-start | bytes 3145732
  60.1 17.0 %collective-permute-start.7 = (bf16[528,128]{1,0:T(8,128)(2,1)S(1)}, bf16[528,128]{1,0:T(8,128)(2,1)S(1)}, u32[]{:S(2)}, u32[]{:S(2)}) collective-permute-start(bf16[528,128]{1,0:T(8,128)(2,1)S(1)} %get-tuple-element.19.refs_1_), channel_id=1, source_target_pairs={{480,0},{0,32},{32,64},{64,96},{96,128},{128,160},{160,192},{192,2... | collective-permute-start | bytes 405512 | tf_op jit(solution)/shard_map/ppermute | solution.py:342
  62.6 20.4 %collective-permute-start.6 = (bf16[528,128]{1,0:T(8,128)(2,1)S(1)}, bf16[528,128]{1,0:T(8,128)(2,1)S(1)}, u32[]{:S(2)}, u32[]{:S(2)}) collective-permute-start(bf16[528,128]{1,0:T(8,128)(2,1)S(1)} %get-tuple-element.19.refs_1_), channel_id=1, source_target_pairs={{352,0},{384,32},{416,64},{448,96},{480,128},{0,160},{32,192},{64,... | collective-permute-start | bytes 405512 | tf_op jit(solution)/shard_map/ppermute | solution.py:342
  66.1 26.1 %collective-permute-start.5 = (bf16[528,128]{1,0:T(8,128)(2,1)S(1)}, bf16[528,128]{1,0:T(8,128)(2,1)S(1)}, u32[]{:S(2)}, u32[]{:S(2)}) collective-permute-start(bf16[528,128]{1,0:T(8,128)(2,1)S(1)} %get-tuple-element.19.refs_1_), channel_id=1, source_target_pairs={{192,0},{224,32},{256,64},{288,96},{320,128},{352,160},{384,192},{... | collective-permute-start | bytes 405512 | tf_op jit(solution)/shard_map/ppermute | solution.py:342
  74.5 20.5 %collective-permute-start.4 = (bf16[528,128]{1,0:T(8,128)(2,1)S(1)}, bf16[528,128]{1,0:T(8,128)(2,1)S(1)}, u32[]{:S(2)}, u32[]{:S(2)}) collective-permute-start(bf16[528,128]{1,0:T(8,128)(2,1)S(1)} %get-tuple-element.19.refs_1_), channel_id=1, source_target_pairs={{32,0},{64,32},{96,64},{128,96},{160,128},{192,160},{224,192},{256... | collective-permute-start | bytes 405512 | tf_op jit(solution)/shard_map/ppermute | solution.py:342
  95.1 13.1 %collective-permute-start.8 = (bf16[1584,128]{1,0:T(8,128)(2,1)S(1)}, bf16[1584,128]{1,0:T(8,128)(2,1)S(1)}, u32[]{:S(2)}, u32[]{:S(2)}) collective-permute-start(bf16[1584,128]{1,0:T(8,128)(2,1)S(1)} %get-tuple-element.20), channel_id=1, source_target_pairs={{32,0},{64,32},{96,64},{128,96},{160,128},{192,160},{224,192},{256... | collective-permute-start | bytes 1216520 | tf_op jit(solution)/shard_map/ppermute | solution.py:342
  100.1 22.1 %collective-permute-start.10 = (bf16[1584,128]{1,0:T(8,128)(2,1)S(1)}, bf16[1584,128]{1,0:T(8,128)(2,1)S(1)}, u32[]{:S(2)}, u32[]{:S(2)}) collective-permute-start(bf16[1584,128]{1,0:T(8,128)(2,1)S(1)} %get-tuple-element.21), channel_id=1, source_target_pairs={{480,0},{0,32},{32,64},{64,96},{96,128},{128,160},{160,192},{192,2... | collective-permute-start | bytes 1216520 | tf_op jit(solution)/shard_map/ppermute | solution.py:342
  103.6 20.7 %all-to-all-start.2 = ((bf16[4,128,512]{2,1,0:T(8,128)(2,1)}), bf16[4,128,512]{2,1,0:T(8,128)(2,1)S(1)}, u32[]{:S(2)}, u32[]{:S(2)}) async-start(bf16[4,128,512]{2,1,0:T(8,128)(2,1)} %query.1), calls=%async_computation.2 | async-start | bytes 1048576 | tf_op jit(solution)/shard_map/all_to_all | solution.py:423
  108.2 25.3 %collective-permute-start.9 = (bf16[1584,128]{1,0:T(8,128)(2,1)S(1)}, bf16[1584,128]{1,0:T(8,128)(2,1)S(1)}, u32[]{:S(2)}, u32[]{:S(2)}) collective-permute-start(bf16[1584,128]{1,0:T(8,128)(2,1)S(1)} %collective-permute-done.8.refs_1_), channel_id=1, source_target_pairs={{32,0},{64,32},{96,64},{128,96},{160,128},{192,160},{224,192},{256... | collective-permute-start | bytes 1216520 | tf_op jit(solution)/shard_map/ppermute | solution.py:342
  113.5 29.8 %collective-permute-start.13 = (bf16[256,2048]{1,0:T(8,128)(2,1)}, bf16[256,2048]{1,0:T(8,128)(2,1)}, u32[]{:S(2)}, u32[]{:S(2)}) collective-permute-start(bf16[256,2048]{1,0:T(8,128)(2,1)} %w0.1), channel_id=1, source_target_pairs={{4,0},{6,2},{0,4},{2,6},{5,1},{7,3},{1,5},{3,7},{12,8},{14,10},{8,... | collective-permute-start | bytes 3145736 | tf_op jit(solution)/shard_map/ppermute | solution.py:342
  116.1 47.5 %collective-permute-start.12 = (bf16[256,2048]{1,0:T(8,128)(2,1)}, bf16[256,2048]{1,0:T(8,128)(2,1)}, u32[]{:S(2)}, u32[]{:S(2)}) collective-permute-start(bf16[256,2048]{1,0:T(8,128)(2,1)} %w0.1), channel_id=1, source_target_pairs={{2,0},{4,2},{6,4},{0,6},{3,1},{5,3},{7,5},{1,7},{10,8},{12,10},{14... | collective-permute-start | bytes 3145736 | tf_op jit(solution)/shard_map/ppermute | solution.py:342
  120.2 45.8 %collective-permute-start.14 = (bf16[256,2048]{1,0:T(8,128)(2,1)}, bf16[256,2048]{1,0:T(8,128)(2,1)}, u32[]{:S(2)}, u32[]{:S(2)}) collective-permute-start(bf16[256,2048]{1,0:T(8,128)(2,1)} %w0.1), channel_id=1, source_target_pairs={{6,0},{0,2},{2,4},{4,6},{7,1},{1,3},{3,5},{5,7},{14,8},{8,10},{10,... | collective-permute-start | bytes 3145736 | tf_op jit(solution)/shard_map/ppermute | solution.py:342
  122.2 11.3 %collective-permute-start.11 = (bf16[1056,128]{1,0:T(8,128)(2,1)S(1)}, bf16[1056,128]{1,0:T(8,128)(2,1)S(1)}, u32[]{:S(2)}, u32[]{:S(2)}) collective-permute-start(bf16[1056,128]{1,0:T(8,128)(2,1)S(1)} %bundle.3), channel_id=1, source_target_pairs={{480,0},{0,32},{32,64},{64,96},{96,128},{128,160},{160,192},{192,2... | collective-permute-start | bytes 811016 | tf_op jit(solution)/shard_map/ppermute | solution.py:342
  138.5 32.1 %all-to-all-start.3 = ((bf16[16,144,128]{2,1,0:T(8,128)(2,1)}), bf16[16,144,128]{2,1,0:T(8,128)(2,1)S(1)}, u32[]{:S(2)}, u32[]{:S(2)}) async-start(bf16[16,144,128]{2,1,0:T(8,128)(2,1)} %attend.5), calls=%async_computation.3 | async-start | bytes 1179648 | tf_op jit(solution)/shard_map/all_to_all | solution.py:439
  173.7 4.6 %collective-permute-start.15 = (f32[32,2048]{1,0:T(8,128)S(1)}, f32[32,2048]{1,0:T(8,128)S(1)}, u32[]{:S(2)}, u32[]{:S(2)}) collective-permute-start(f32[32,2048]{1,0:T(8,128)S(1)} %get-tuple-element.29), channel_id=1, source_target_pairs={{1,0},{0,1},{3,2},{2,3},{5,4},{4,5},{7,6},{6,7},{9,8},{8,9},{11,10... | collective-permute-start | bytes 786440 | tf_op jit(solution)/shard_map/ppermute | solution.py:342
  (5 other events, 49.3 us)

commit v7 on v6

--- a/solution.py
+++ b/solution.py
@@ -10,6 +10,8 @@
 from jax.sharding import PartitionSpec as P
 
 
+RESIDENT = (3, 1)
+FETCHED = (0, 2)
 GRID_W = 64
 LOG2E = math.log2(math.e)
 TP = ("x", "c")
@@ -274,15 +276,16 @@
 
 
 def out_kernel(place, parts, w0, w1, w2, w3, mine, other, both, held, done):
-    copies = [
-        pltpu.make_async_copy(w, held.at[h], done.at[h]) for h, w in enumerate((w0, w1, w2, w3))
-    ]
-    for copy in copies:
+    weights = (w0, w1, w2, w3)
+    copies = {
+        h: pltpu.make_async_copy(weights[h], held.at[n], done.at[n]) for n, h in enumerate(FETCHED)
+    }
+    for copy in copies.values():
         copy.start()
-    chips = len(copies)
+    chips = len(weights)
     dim = parts.shape[1] - 16
     rows = mine.shape[0]
-    for h, copy in enumerate(copies):
+    for h in (*RESIDENT, *FETCHED):
         chip = jax.lax.rem(place[0] + h, chips)
         group = [y * chips + chip for y in range(parts.shape[0] // chips)]
         tail = [parts[i, dim : dim + 16].astype(F32) for i in group]
@@ -297,10 +300,12 @@
         attended = jnp.concatenate(
             [turn[at : at + 2 * rows] for at in range(0, turn.shape[0], 2 * rows)], axis=1
         ).astype(BF16)
-        copy.wait()
-        partial = jnp.dot(attended, held[h], preferred_element_type=F32)
+        if h in copies:
+            copies[h].wait()
+        rows_out = held[FETCHED.index(h)] if h in copies else weights[h][...]
+        partial = jnp.dot(attended, rows_out, preferred_element_type=F32)
         partial = partial.astype(BF16).astype(F32)
-        both[...] = partial if h == 0 else both[...] + partial
+        both[...] = partial if h == (*RESIDENT, *FETCHED)[0] else both[...] + partial
     mine[...] = both[pl.ds(pl.multiple_of(place[1] * rows, rows), rows)]
     other[...] = both[pl.ds(pl.multiple_of((1 - place[1]) * rows, rows), rows)]
 
@@ -441,7 +446,7 @@
     sums, others = pl.pallas_call(
         out_kernel,
         in_specs=[pl.BlockSpec(memory_space=pltpu.SMEM), whole]
-        + [pl.BlockSpec(memory_space=pltpu.HBM)] * 4,
+        + [whole if h in RESIDENT else pl.BlockSpec(memory_space=pltpu.HBM) for h in range(4)],
         out_specs=(whole, whole),
         out_shape=(
             jax.ShapeDtypeStruct((rows, model), F32),
@@ -449,8 +454,8 @@
         ),
         scratch_shapes=[
             pltpu.VMEM((2 * rows, model), F32),
-            pltpu.VMEM((4, *w_out.shape), BF16),
-            pltpu.SemaphoreType.DMA((4,)),
+            pltpu.VMEM((len(FETCHED), *w_out.shape), BF16),
+            pltpu.SemaphoreType.DMA((len(FETCHED),)),
         ],
         compiler_params=room(16),
         cost_estimate=pl.CostEstimate(
@@ -459,7 +464,7 @@
             transcendentals=0,
         ),
         name="out",
-    )(place, *near(returned), *far(*w_outs))
+    )(place, *near(returned), *[(near if h in RESIDENT else far)(w)[0] for h, w in enumerate(w_outs)])
     others = receive(others, "c", 1)
     return pl.pallas_call(
         final_kernel,

time: 180 us -> 181 us (level)
  waiting for transfers between devices: 63.8 us -> 56.6 us
  local copies, waits for them, and re-layouts: 0.04 us -> 5.21 us
  Pallas kernels: 23.9 us -> 26.5 us
    ppermute x16, waiting for transfers between devices: 42.9 us -> 35.5 us  [receive(): lax.ppermute(value, axis, [((i + hop) % size, i) for i in range(size)])]
    unnamed x18 -> x38, local copies, waits for them, and re-layouts: 0.04 us -> 5.21 us
    pallas_call x3, Pallas kernels: 14.2 us -> 16.2 us  [attend(): pl.pallas_call(functools.partial(attend_kernel, counts=counts, keys=keys,...]
  transfers between devices with their start and end apart: 20 -> 20, of which waited for: 10 -> 10; matrix products, arithmetic and copies ran while one was open for 0% -> 0% of each run, Pallas kernels for 10% -> 11%
where the time goes in v7:
time: 181 us; the launch traced here: 180 us
  starting transfers between devices  90.4 us (50%)
  waiting for transfers between devices  56.6 us (31%)
  Pallas kernels  26.5 us (15%)
  local copies, waits for them, and re-layouts  5.21 us (3%)
    ppermute x16, starting transfers between devices, receive(): lax.ppermute(value, axis, [((i + hop) % size, i) for i in range(size)])  58.4 us
    ppermute x16, waiting for transfers between devices, receive(): lax.ppermute(value, axis, [((i + hop) % size, i) for i in range(size)])  35.5 us
    pallas_call x3, Pallas kernels, attend(): pl.pallas_call(functools.partial(attend_kernel, counts=counts, keys=keys,...  16.2 us
    all_to_all x1, starting transfers between devices, body(): partial_mod = lax.all_to_all(partial_mod, 'z', 0, 0, tiled=True)  15 us
    all_to_all x1, waiting for transfers between devices, body(): pieces = lax.all_to_all(partial_mod, ('y', *TP), 0, 0, tiled=True)  8.77 us
    all_to_all x1, starting transfers between devices, body(): pieces = lax.all_to_all(partial_mod, ('y', *TP), 0, 0, tiled=True)  8.67 us
    all_to_all x1, waiting for transfers between devices, body(): partial_mod = lax.all_to_all(partial_mod, 'z', 0, 0, tiled=True)  7.52 us
    unnamed x38, local copies, waits for them, and re-layouts  5.21 us
  transfers between devices with their start and end apart: 20, of which 10 were waited for; matrix products, arithmetic and copies ran while one was open for 0% of the time, Pallas kernels for 11%

profile of v7, /device:TPU:1, one launch (start us, length us, event | category | flops | bytes accessed | tf_op | source)
XLA Modules:
  0.0 179.7 jit_solution(15327447762133238686)
XLA Ops:
  0.0 3.9 %collective-permute-start.2 = (bf16[32,2048]{1,0:T(8,128)(2,1)}, bf16[32,2048]{1,0:T(8,128)(2,1)S(1)}, u32[]{:S(2)}, u32[]{:S(2)}) collective-permute-start(bf16[32,2048]{1,0:T(8,128)(2,1)} %latent.1), channel_id=1, source_target_pairs={{6,0},{0,2},{2,4},{4,6},{7,1},{1,3},{3,5},{5,7},{14,8},{8,10},{10,... | collective-permute-start | bytes 393224 | tf_op jit(solution)/shard_map/ppermute | solution.py:347
  3.9 4.4 %collective-permute-start.1 = (bf16[32,2048]{1,0:T(8,128)(2,1)}, bf16[32,2048]{1,0:T(8,128)(2,1)S(1)}, u32[]{:S(2)}, u32[]{:S(2)}) collective-permute-start(bf16[32,2048]{1,0:T(8,128)(2,1)} %latent.1), channel_id=1, source_target_pairs={{4,0},{6,2},{0,4},{2,6},{5,1},{7,3},{1,5},{3,7},{12,8},{14,10},{8,... | collective-permute-start | bytes 393224 | tf_op jit(solution)/shard_map/ppermute | solution.py:347
  8.3 3.1 %collective-permute-start = (bf16[32,2048]{1,0:T(8,128)(2,1)}, bf16[32,2048]{1,0:T(8,128)(2,1)S(1)}, u32[]{:S(2)}, u32[]{:S(2)}) collective-permute-start(bf16[32,2048]{1,0:T(8,128)(2,1)} %latent.1), channel_id=1, source_target_pairs={{2,0},{4,2},{6,4},{0,6},{3,1},{5,3},{7,5},{1,7},{10,8},{12,10},{14... | collective-permute-start | bytes 393224 | tf_op jit(solution)/shard_map/ppermute | solution.py:347
  13.0 15.0 %all-to-all-start = ((f32[16,5,256]{2,1,0:T(8,128)}), f32[16,5,256]{2,1,0:T(8,128)S(1)}, u32[]{:S(2)}, u32[]{:S(2)}) async-start(f32[16,5,256]{2,1,0:T(8,128)} %modulation.1), calls=%async_computation | async-start | bytes 262144 | tf_op jit(solution)/shard_map/all_to_all | solution.py:360
  28.1 3.7 %collective-permute-start.3 = (bf16[128,2048]{1,0:T(8,128)(2,1)S(1)}, bf16[128,2048]{1,0:T(8,128)(2,1)S(1)}, u32[]{:S(2)}, u32[]{:S(2)}) collective-permute-start(bf16[128,2048]{1,0:T(8,128)(2,1)S(1)} %pad_maximum_fusion), channel_id=1, source_target_pairs={{1,0},{0,1},{3,2},{2,3},{5,4},{4,5},{7,6},{6,7},{9,8},{8,9},{11,10... | collective-permute-start | bytes 1572872 | tf_op jit(solution)/shard_map/ppermute | solution.py:347
  32.5 7.5 %all-to-all-done.blocks = f32[16,5,256]{2,1,0:T(8,128)S(1)} async-done(((f32[16,5,256]{2,1,0:T(8,128)}), f32[16,5,256]{2,1,0:T(8,128)S(1)}, u32[]{:S(2)}, u32[]{:S(2)}) %all-to-all-start) | async-done | bytes 81952 | tf_op jit(solution)/shard_map/all_to_all | solution.py:360
  40.7 8.7 %all-to-all-start.1 = ((f32[32,5,256]{2,1,0:T(8,128)}), f32[32,5,256]{2,1,0:T(8,128)S(1)}, u32[]{:S(2)}, u32[]{:S(2)}) async-start(f32[32,5,256]{2,1,0:T(8,128)} %spread.1), calls=%async_computation.1 | async-start | bytes 524288 | tf_op jit(solution)/shard_map/all_to_all | solution.py:369
  49.5 8.8 %all-to-all-done.1.refs_5_ = f32[32,5,256]{2,1,0:T(8,128)S(1)} async-done(((f32[32,5,256]{2,1,0:T(8,128)}), f32[32,5,256]{2,1,0:T(8,128)S(1)}, u32[]{:S(2)}, u32[]{:S(2)}) %all-to-all-start.1) | async-done | bytes 163872 | tf_op jit(solution)/shard_map/all_to_all | solution.py:369
  62.6 3.5 %collective-permute-start.6 = (bf16[528,128]{1,0:T(8,128)(2,1)S(1)}, bf16[528,128]{1,0:T(8,128)(2,1)S(1)}, u32[]{:S(2)}, u32[]{:S(2)}) collective-permute-start(bf16[528,128]{1,0:T(8,128)(2,1)S(1)} %get-tuple-element.19.refs_1_), channel_id=1, source_target_pairs={{352,0},{384,32},{416,64},{448,96},{480,128},{0,160},{32,192},{64,... | collective-permute-start | bytes 405512 | tf_op jit(solution)/shard_map/ppermute | solution.py:347
  66.1 8.4 %collective-permute-start.5 = (bf16[528,128]{1,0:T(8,128)(2,1)S(1)}, bf16[528,128]{1,0:T(8,128)(2,1)S(1)}, u32[]{:S(2)}, u32[]{:S(2)}) collective-permute-start(bf16[528,128]{1,0:T(8,128)(2,1)S(1)} %get-tuple-element.19.refs_1_), channel_id=1, source_target_pairs={{192,0},{224,32},{256,64},{288,96},{320,128},{352,160},{384,192},{... | collective-permute-start | bytes 405512 | tf_op jit(solution)/shard_map/ppermute | solution.py:347
  77.7 5.3 %collective-permute-done.6.refs_2_.refs_5_ = bf16[528,128]{1,0:T(8,128)(2,1)S(1)} collective-permute-done((bf16[528,128]{1,0:T(8,128)(2,1)S(1)}, bf16[528,128]{1,0:T(8,128)(2,1)S(1)}, u32[]{:S(2)}, u32[]{:S(2)}) %collective-permute-start.6) | collective-permute-done | bytes 135200 | tf_op jit(solution)/shard_map/ppermute | solution.py:347
  83.1 9.1 %collective-permute-done.5.refs_1_.refs_4_ = bf16[528,128]{1,0:T(8,128)(2,1)S(1)} collective-permute-done((bf16[528,128]{1,0:T(8,128)(2,1)S(1)}, bf16[528,128]{1,0:T(8,128)(2,1)S(1)}, u32[]{:S(2)}, u32[]{:S(2)}) %collective-permute-start.5) | collective-permute-done | bytes 135200 | tf_op jit(solution)/shard_map/ppermute | solution.py:347
  92.2 2.9 %collective-permute-done.4.refs_0_.refs_2_ = bf16[528,128]{1,0:T(8,128)(2,1)S(1)} collective-permute-done((bf16[528,128]{1,0:T(8,128)(2,1)S(1)}, bf16[528,128]{1,0:T(8,128)(2,1)S(1)}, u32[]{:S(2)}, u32[]{:S(2)}) %collective-permute-start.4) | collective-permute-done | bytes 135200 | tf_op jit(solution)/shard_map/ppermute | solution.py:347
  95.9 4.9 %collective-permute-start.8 = (bf16[1584,128]{1,0:T(8,128)(2,1)S(1)}, bf16[1584,128]{1,0:T(8,128)(2,1)}, u32[]{:S(2)}, u32[]{:S(2)}) collective-permute-start(bf16[1584,128]{1,0:T(8,128)(2,1)S(1)} %get-tuple-element.20), channel_id=1, source_target_pairs={{32,0},{64,32},{96,64},{128,96},{160,128},{192,160},{224,192},{256... | collective-permute-start | bytes 1216520 | tf_op jit(solution)/shard_map/ppermute | solution.py:347
  104.3 3.5 %all-to-all-start.2 = ((bf16[4,128,512]{2,1,0:T(8,128)(2,1)}), bf16[4,128,512]{2,1,0:T(8,128)(2,1)S(1)}, u32[]{:S(2)}, u32[]{:S(2)}) async-start(bf16[4,128,512]{2,1,0:T(8,128)(2,1)} %query.1), calls=%async_computation.2 | async-start | bytes 1048576 | tf_op jit(solution)/shard_map/all_to_all | solution.py:428
  108.9 5.4 %collective-permute-start.9 = (bf16[1584,128]{1,0:T(8,128)(2,1)}, bf16[1584,128]{1,0:T(8,128)(2,1)}, u32[]{:S(2)}, u32[]{:S(2)}) collective-permute-start(bf16[1584,128]{1,0:T(8,128)(2,1)} %collective-permute-done.8.refs_1_), channel_id=1, source_target_pairs={{32,0},{64,32},{96,64},{128,96},{160,128},{192,160},{224,192},{256... | collective-permute-start | bytes 1216520 | tf_op jit(solution)/shard_map/ppermute | solution.py:347
  116.9 4.1 %collective-permute-start.12 = (bf16[256,2048]{1,0:T(8,128)(2,1)}, bf16[256,2048]{1,0:T(8,128)(2,1)S(1)}, u32[]{:S(2)}, u32[]{:S(2)}) collective-permute-start(bf16[256,2048]{1,0:T(8,128)(2,1)} %w0.1), channel_id=1, source_target_pairs={{2,0},{4,2},{6,4},{0,6},{3,1},{5,3},{7,5},{1,7},{10,8},{12,10},{14... | collective-permute-start | bytes 3145736 | tf_op jit(solution)/shard_map/ppermute | solution.py:347
  129.7 4.2 %attend.3 = (f32[4,1,512]{2,1,0:T(1,128)S(1)}, f32[4,1,512]{2,1,0:T(1,128)S(1)}, f32[4,128,512]{2,1,0:T(8,128)S(1)}) custom-call(bf16[4,128,512]{2,1,0:T(8,128)(2,1)S(1)} %all-to-all-done.2.refs_0_, bf16[528,128]{1,0:T(8,128)(2,1)S(1)} %copy-done.16, bf16[528,128]{1,0:T(8,128)(2,1)S(1)} %copy-done.11, bf16[528,128]{1,0:T(8,128)(2,1)S(1)} %copy-done.5, ...), custom_call_target="tpu_custom_call" | custom-call | flops 1384120320 | bytes 2097152 | tf_op jit(solution)/shard_map/attend/pallas_call | solution.py:254
  133.9 5.9 %attend.4 = (f32[4,1,512]{2,1,0:T(1,128)S(1)}, f32[4,1,512]{2,1,0:T(1,128)S(1)}, f32[4,128,512]{2,1,0:T(8,128)S(1)}) custom-call(bf16[4,128,512]{2,1,0:T(8,128)(2,1)S(1)} %all-to-all-done.2.refs_0_, bf16[1584,128]{1,0:T(8,128)(2,1)} %collective-permute-done.8.refs_1_, bf16[1584,128]{1,0:T(8,128)(2,1)S(1)} %collective-permute-done.10.refs_0_.refs_2_, ...), custom_call_target="tpu_custom_call" | custom-call | flops 1660944384 | bytes 2097152 | tf_op jit(solution)/shard_map/attend/pallas_call | solution.py:254
  139.8 6.1 %attend.5 = bf16[16,144,128]{2,1,0:T(8,128)(2,1)} custom-call(bf16[4,128,512]{2,1,0:T(8,128)(2,1)S(1)} %all-to-all-done.2.refs_0_, bf16[1584,128]{1,0:T(8,128)(2,1)} %collective-permute-done.9.refs_1_, bf16[1056,128]{1,0:T(8,128)(2,1)} %collective-permute-done.11.refs_2_, f32[4,1,512]{2,1,0:T(1,128)S(1)} %get-tuple-element.25.refs_3_, ...), custom_call_target="tpu_custom_call" | custom-call | flops 1384120320 | bytes 2097152 | tf_op jit(solution)/shard_map/attend/pallas_call | solution.py:254
  145.9 4.8 %all-to-all-start.3 = ((bf16[16,144,128]{2,1,0:T(8,128)(2,1)}), bf16[16,144,128]{2,1,0:T(8,128)(2,1)S(1)}, u32[]{:S(2)}, u32[]{:S(2)}) async-start(bf16[16,144,128]{2,1,0:T(8,128)(2,1)} %attend.5), calls=%async_computation.3 | async-start | bytes 1179648 | tf_op jit(solution)/shard_map/all_to_all | solution.py:444
  150.7 13.6 %collective-permute-done.12.w1 = bf16[256,2048]{1,0:T(8,128)(2,1)S(1)} collective-permute-done((bf16[256,2048]{1,0:T(8,128)(2,1)}, bf16[256,2048]{1,0:T(8,128)(2,1)S(1)}, u32[]{:S(2)}, u32[]{:S(2)}) %collective-permute-start.12) | collective-permute-done | bytes 1048608 | tf_op jit(solution)/shard_map/ppermute | solution.py:347
  166.7 4.7 %all-to-all-done.3.parts = bf16[16,144,128]{2,1,0:T(8,128)(2,1)S(1)} async-done(((bf16[16,144,128]{2,1,0:T(8,128)(2,1)}), bf16[16,144,128]{2,1,0:T(8,128)(2,1)S(1)}, u32[]{:S(2)}, u32[]{:S(2)}) %all-to-all-start.3) | async-done | bytes 589856 | tf_op jit(solution)/shard_map/all_to_all | solution.py:444
  174.3 3.5 %collective-permute-start.15 = (f32[32,2048]{1,0:T(8,128)S(1)}, f32[32,2048]{1,0:T(8,128)S(1)}, u32[]{:S(2)}, u32[]{:S(2)}) collective-permute-start(f32[32,2048]{1,0:T(8,128)S(1)} %get-tuple-element.29), channel_id=1, source_target_pairs={{1,0},{0,1},{3,2},{2,3},{5,4},{4,5},{7,6},{6,7},{9,8},{8,9},{11,10... | collective-permute-start | bytes 786440 | tf_op jit(solution)/shard_map/ppermute | solution.py:347
  (72 shorter events, 34.3 us)
Async XLA Ops:
  0.0 28.1 %collective-permute-start.2 = (bf16[32,2048]{1,0:T(8,128)(2,1)}, bf16[32,2048]{1,0:T(8,128)(2,1)S(1)}, u32[]{:S(2)}, u32[]{:S(2)}) collective-permute-start(bf16[32,2048]{1,0:T(8,128)(2,1)} %latent.1), channel_id=1, source_target_pairs={{6,0},{0,2},{2,4},{4,6},{7,1},{1,3},{3,5},{5,7},{14,8},{8,10},{10,... | collective-permute-start | bytes 393224 | tf_op jit(solution)/shard_map/ppermute | solution.py:347
  3.9 24.1 %collective-permute-start.1 = (bf16[32,2048]{1,0:T(8,128)(2,1)}, bf16[32,2048]{1,0:T(8,128)(2,1)S(1)}, u32[]{:S(2)}, u32[]{:S(2)}) collective-permute-start(bf16[32,2048]{1,0:T(8,128)(2,1)} %latent.1), channel_id=1, source_target_pairs={{4,0},{6,2},{0,4},{2,6},{5,1},{7,3},{1,5},{3,7},{12,8},{14,10},{8,... | collective-permute-start | bytes 393224 | tf_op jit(solution)/shard_map/ppermute | solution.py:347
  8.3 19.8 %collective-permute-start = (bf16[32,2048]{1,0:T(8,128)(2,1)}, bf16[32,2048]{1,0:T(8,128)(2,1)S(1)}, u32[]{:S(2)}, u32[]{:S(2)}) collective-permute-start(bf16[32,2048]{1,0:T(8,128)(2,1)} %latent.1), channel_id=1, source_target_pairs={{2,0},{4,2},{6,4},{0,6},{3,1},{5,3},{7,5},{1,7},{10,8},{12,10},{14... | collective-permute-start | bytes 393224 | tf_op jit(solution)/shard_map/ppermute | solution.py:347
  13.0 27.0 %all-to-all-start = ((f32[16,5,256]{2,1,0:T(8,128)}), f32[16,5,256]{2,1,0:T(8,128)S(1)}, u32[]{:S(2)}, u32[]{:S(2)}) async-start(f32[16,5,256]{2,1,0:T(8,128)} %modulation.1), calls=%async_computation | async-start | bytes 262144 | tf_op jit(solution)/shard_map/all_to_all | solution.py:360
  28.1 30.1 %collective-permute-start.3 = (bf16[128,2048]{1,0:T(8,128)(2,1)S(1)}, bf16[128,2048]{1,0:T(8,128)(2,1)S(1)}, u32[]{:S(2)}, u32[]{:S(2)}) collective-permute-start(bf16[128,2048]{1,0:T(8,128)(2,1)S(1)} %pad_maximum_fusion), channel_id=1, source_target_pairs={{1,0},{0,1},{3,2},{2,3},{5,4},{4,5},{7,6},{6,7},{9,8},{8,9},{11,10... | collective-permute-start | bytes 1572872 | tf_op jit(solution)/shard_map/ppermute | solution.py:347
  31.9 26.4 %copy-start.3 = (bf16[2048,128]{1,0:T(8,128)(2,1)S(1)}, bf16[2048,128]{1,0:T(8,128)(2,1)}, u32[]{:S(2)}) copy-start(bf16[2048,128]{1,0:T(8,128)(2,1)} %refs_9_.1) | copy-start | bytes 1572868
  32.4 25.8 %copy-start.2 = (bf16[2048,128]{1,0:T(8,128)(2,1)S(1)}, bf16[2048,128]{1,0:T(8,128)(2,1)}, u32[]{:S(2)}) copy-start(bf16[2048,128]{1,0:T(8,128)(2,1)} %refs_8_.1) | copy-start | bytes 1572868
  40.7 17.6 %all-to-all-start.1 = ((f32[32,5,256]{2,1,0:T(8,128)}), f32[32,5,256]{2,1,0:T(8,128)S(1)}, u32[]{:S(2)}, u32[]{:S(2)}) async-start(f32[32,5,256]{2,1,0:T(8,128)} %spread.1), calls=%async_computation.1 | async-start | bytes 524288 | tf_op jit(solution)/shard_map/all_to_all | solution.py:369
  58.3 44.4 %copy-start.1 = (bf16[2048,256]{1,0:T(8,128)(2,1)S(1)}, bf16[2048,256]{1,0:T(8,128)(2,1)}, u32[]{:S(2)}) copy-start(bf16[2048,256]{1,0:T(8,128)(2,1)} %wq.1) | copy-start | bytes 3145732
  60.1 17.6 %collective-permute-start.7 = (bf16[528,128]{1,0:T(8,128)(2,1)S(1)}, bf16[528,128]{1,0:T(8,128)(2,1)S(1)}, u32[]{:S(2)}, u32[]{:S(2)}) collective-permute-start(bf16[528,128]{1,0:T(8,128)(2,1)S(1)} %get-tuple-element.19.refs_1_), channel_id=1, source_target_pairs={{480,0},{0,32},{32,64},{64,96},{96,128},{128,160},{160,192},{192,2... | collective-permute-start | bytes 405512 | tf_op jit(solution)/shard_map/ppermute | solution.py:347
  62.6 20.4 %collective-permute-start.6 = (bf16[528,128]{1,0:T(8,128)(2,1)S(1)}, bf16[528,128]{1,0:T(8,128)(2,1)S(1)}, u32[]{:S(2)}, u32[]{:S(2)}) collective-permute-start(bf16[528,128]{1,0:T(8,128)(2,1)S(1)} %get-tuple-element.19.refs_1_), channel_id=1, source_target_pairs={{352,0},{384,32},{416,64},{448,96},{480,128},{0,160},{32,192},{64,... | collective-permute-start | bytes 405512 | tf_op jit(solution)/shard_map/ppermute | solution.py:347
  66.1 26.1 %collective-permute-start.5 = (bf16[528,128]{1,0:T(8,128)(2,1)S(1)}, bf16[528,128]{1,0:T(8,128)(2,1)S(1)}, u32[]{:S(2)}, u32[]{:S(2)}) collective-permute-start(bf16[528,128]{1,0:T(8,128)(2,1)S(1)} %get-tuple-element.19.refs_1_), channel_id=1, source_target_pairs={{192,0},{224,32},{256,64},{288,96},{320,128},{352,160},{384,192},{... | collective-permute-start | bytes 405512 | tf_op jit(solution)/shard_map/ppermute | solution.py:347
  74.5 20.5 %collective-permute-start.4 = (bf16[528,128]{1,0:T(8,128)(2,1)S(1)}, bf16[528,128]{1,0:T(8,128)(2,1)S(1)}, u32[]{:S(2)}, u32[]{:S(2)}) collective-permute-start(bf16[528,128]{1,0:T(8,128)(2,1)S(1)} %get-tuple-element.19.refs_1_), channel_id=1, source_target_pairs={{32,0},{64,32},{96,64},{128,96},{160,128},{192,160},{224,192},{256... | collective-permute-start | bytes 405512 | tf_op jit(solution)/shard_map/ppermute | solution.py:347
  77.7 18.1 %copy-start.4 = (bf16[528,128]{1,0:T(8,128)(2,1)}, bf16[528,128]{1,0:T(8,128)(2,1)S(1)}, u32[]{:S(2)}) copy-start(bf16[528,128]{1,0:T(8,128)(2,1)S(1)} %collective-permute-done.7.refs_3_) | copy-start | bytes 405508
  95.9 13.0 %collective-permute-start.8 = (bf16[1584,128]{1,0:T(8,128)(2,1)S(1)}, bf16[1584,128]{1,0:T(8,128)(2,1)}, u32[]{:S(2)}, u32[]{:S(2)}) collective-permute-start(bf16[1584,128]{1,0:T(8,128)(2,1)S(1)} %get-tuple-element.20), channel_id=1, source_target_pairs={{32,0},{64,32},{96,64},{128,96},{160,128},{192,160},{224,192},{256... | collective-permute-start | bytes 1216520 | tf_op jit(solution)/shard_map/ppermute | solution.py:347
  100.8 22.2 %collective-permute-start.10 = (bf16[1584,128]{1,0:T(8,128)(2,1)}, bf16[1584,128]{1,0:T(8,128)(2,1)S(1)}, u32[]{:S(2)}, u32[]{:S(2)}) collective-permute-start(bf16[1584,128]{1,0:T(8,128)(2,1)} %get-tuple-element.21), channel_id=1, source_target_pairs={{480,0},{0,32},{32,64},{64,96},{96,128},{128,160},{160,192},{192,2... | collective-permute-start | bytes 1216520 | tf_op jit(solution)/shard_map/ppermute | solution.py:347
  104.3 20.8 %all-to-all-start.2 = ((bf16[4,128,512]{2,1,0:T(8,128)(2,1)}), bf16[4,128,512]{2,1,0:T(8,128)(2,1)S(1)}, u32[]{:S(2)}, u32[]{:S(2)}) async-start(bf16[4,128,512]{2,1,0:T(8,128)(2,1)} %query.1), calls=%async_computation.2 | async-start | bytes 1048576 | tf_op jit(solution)/shard_map/all_to_all | solution.py:428
  108.9 30.9 %collective-permute-start.9 = (bf16[1584,128]{1,0:T(8,128)(2,1)}, bf16[1584,128]{1,0:T(8,128)(2,1)}, u32[]{:S(2)}, u32[]{:S(2)}) collective-permute-start(bf16[1584,128]{1,0:T(8,128)(2,1)} %collective-permute-done.8.refs_1_), channel_id=1, source_target_pairs={{32,0},{64,32},{96,64},{128,96},{160,128},{192,160},{224,192},{256... | collective-permute-start | bytes 1216520 | tf_op jit(solution)/shard_map/ppermute | solution.py:347
  114.3 36.4 %collective-permute-start.13 = (bf16[256,2048]{1,0:T(8,128)(2,1)}, bf16[256,2048]{1,0:T(8,128)(2,1)}, u32[]{:S(2)}, u32[]{:S(2)}) collective-permute-start(bf16[256,2048]{1,0:T(8,128)(2,1)} %w0.1), channel_id=1, source_target_pairs={{4,0},{6,2},{0,4},{2,6},{5,1},{7,3},{1,5},{3,7},{12,8},{14,10},{8,... | collective-permute-start | bytes 3145736 | tf_op jit(solution)/shard_map/ppermute | solution.py:347
  116.9 47.5 %collective-permute-start.12 = (bf16[256,2048]{1,0:T(8,128)(2,1)}, bf16[256,2048]{1,0:T(8,128)(2,1)S(1)}, u32[]{:S(2)}, u32[]{:S(2)}) collective-permute-start(bf16[256,2048]{1,0:T(8,128)(2,1)} %w0.1), channel_id=1, source_target_pairs={{2,0},{4,2},{6,4},{0,6},{3,1},{5,3},{7,5},{1,7},{10,8},{12,10},{14... | collective-permute-start | bytes 3145736 | tf_op jit(solution)/shard_map/ppermute | solution.py:347
  121.0 45.6 %collective-permute-start.14 = (bf16[256,2048]{1,0:T(8,128)(2,1)}, bf16[256,2048]{1,0:T(8,128)(2,1)S(1)}, u32[]{:S(2)}, u32[]{:S(2)}) collective-permute-start(bf16[256,2048]{1,0:T(8,128)(2,1)} %w0.1), channel_id=1, source_target_pairs={{6,0},{0,2},{2,4},{4,6},{7,1},{1,3},{3,5},{5,7},{14,8},{8,10},{10,... | collective-permute-start | bytes 3145736 | tf_op jit(solution)/shard_map/ppermute | solution.py:347
  123.0 16.8 %collective-permute-start.11 = (bf16[1056,128]{1,0:T(8,128)(2,1)S(1)}, bf16[1056,128]{1,0:T(8,128)(2,1)}, u32[]{:S(2)}, u32[]{:S(2)}) collective-permute-start(bf16[1056,128]{1,0:T(8,128)(2,1)S(1)} %bundle.3), channel_id=1, source_target_pairs={{480,0},{0,32},{32,64},{64,96},{96,128},{128,160},{160,192},{192,2... | collective-permute-start | bytes 811016 | tf_op jit(solution)/shard_map/ppermute | solution.py:347
  145.9 25.5 %all-to-all-start.3 = ((bf16[16,144,128]{2,1,0:T(8,128)(2,1)}), bf16[16,144,128]{2,1,0:T(8,128)(2,1)S(1)}, u32[]{:S(2)}, u32[]{:S(2)}) async-start(bf16[16,144,128]{2,1,0:T(8,128)(2,1)} %attend.5), calls=%async_computation.3 | async-start | bytes 1179648 | tf_op jit(solution)/shard_map/all_to_all | solution.py:444
  174.3 4.6 %collective-permute-start.15 = (f32[32,2048]{1,0:T(8,128)S(1)}, f32[32,2048]{1,0:T(8,128)S(1)}, u32[]{:S(2)}, u32[]{:S(2)}) collective-permute-start(f32[32,2048]{1,0:T(8,128)S(1)} %get-tuple-element.29), channel_id=1, source_target_pairs={{1,0},{0,1},{3,2},{2,3},{5,4},{4,5},{7,6},{6,7},{9,8},{8,9},{11,10... | collective-permute-start | bytes 786440 | tf_op jit(solution)/shard_map/ppermute | solution.py:347
  (15 other events, 89.2 us)
